TPU v7x, 128 devices: a 2x2x16 block of a 8x8x16 slice. The times are simulated.
128 devices in a mesh: grp: 4 (over y, x), ep: 32 (over z, core).
Axes of the slice: x: 2, y: 2, z: 16, core: 2. Of those that a mesh axis runs over, the one named last changes fastest.
The devices are a block of a 8x8x16 slice.
Arguments:
- tokens: bfloat16 [256, 2048], P('grp', 'ep'), parts along dimension 0, may hold values from -6 to 6
- w_query: bfloat16 [2048, 1024], P('ep'), may hold values from -0.125 to 0.125
- w_key: bfloat16 [2048, 1024], P('ep'), may hold values from -0.125 to 0.125
- w_value: bfloat16 [2048, 1024], P('ep'), may hold values from -0.125 to 0.125
- w_forget: bfloat16 [2048, 16], P('ep'), may hold values from -0.125 to 0.125
- forget_bias: float32 [16], replicated, may hold values from -1 to 2
- cache_keys: bfloat16 [256, 1024, 1024], P(('grp', 'ep')), parts along dimension 0
- cache_values: bfloat16 [256, 1024, 1024], P(('grp', 'ep')), parts along dimension 0, may hold values from -6 to 6
- cache_gates: float32 [256, 1024, 16], P(('grp', 'ep')), parts along dimension 0, as said below
- lengths: int32 [256], P(('grp', 'ep')), parts along dimension 0, may hold values from 128 to 1024, as said below
- w_out: bfloat16 [1024, 2048], P('ep'), may hold values from -0.1875 to 0.1875
- norm_gain: bfloat16 [2048], replicated, may hold values from 0.099609375 to 1.8984375
- w_router: bfloat16 [2048, 4], replicated, may hold values from -0.125 to 0.125
- routes: int32 [256, 2], P('grp'), parts along dimension 0, may hold values from 0 to 3, all different within a row
- dense_gate: bfloat16 [2048], replicated, may hold values from -0.25 to 0.25
- dense_w_gate: bfloat16 [2048, 8192], P(None, 'ep'), may hold values from -0.125 to 0.125
- dense_w_up: bfloat16 [2048, 8192], P(None, 'ep'), may hold values from -0.125 to 0.125
- dense_w_down: bfloat16 [8192, 2048], P('ep'), may hold values from -0.125 to 0.125
- expert_w_gate: bfloat16 [2048, 16384], P(None, 'ep'), may hold values from -0.125 to 0.125
- expert_w_up: bfloat16 [2048, 16384], P(None, 'ep'), may hold values from -0.125 to 0.125
- expert_w_down: bfloat16 [16384, 2048], P('ep'), may hold values from -0.1875 to 0.1875
- final_gain: bfloat16 [2048], P('ep'), may hold values from 0.099609375 to 1.8984375
Outputs:
- result: bfloat16 [256, 2048], P('grp', 'ep'), parts along dimension 0
There are 4 independent parts, one for each index of `grp`. A program takes and returns all parts, laid end to end along the dimension named above; an argument that names none is the same for every part. Nothing has to cross between parts.
Inputs may be any that keep to these rules, and one draw needn't show every extreme that they name: `routes`: each row names 2 different experts; every expert is named by some row. `lengths`: the first sequence of each part holds 1024 positions. `cache_gates`: never rising along positions.
All inputs are finite; a program needn't handle non-finite values.
Results may differ from a plain program's by a relative error of at most 0.0085.
Values may be sent and summed in bfloat16 or wider, within the bound.
No kernel may reach another device: no remote copies, remote signals or barrier semaphores. Data moves between devices by JAX's collectives and lax.ppermute only.
A program may use at most 128 MiB of HBM per device.

v0:
```python
import jax
import jax.numpy as jnp
from jax import lax
from jax.sharding import PartitionSpec as P

EXP_SPLIT = 8


norm_eps = 1e-05
residual_scale = 8.0**0.25


def split_up(array, dim, size):
    shape = array.shape
    blocks = array.reshape(*shape[:dim], size, shape[dim] // size, *shape[dim + 1 :])
    return jnp.moveaxis(blocks, dim, 0)


def sent_and_summed(array, axis, dim):
    blocks = split_up(array, dim, lax.axis_size(axis))
    arrived = lax.all_to_all(blocks, axis, split_axis=0, concat_axis=0, tiled=True)
    return arrived.sum(axis=0)


def in_one_piece(arrays, axis, dim, along):
    widths = [a.shape[along] for a in arrays]
    both = jnp.concatenate(arrays, axis=along)
    result = sent_and_summed(both, axis, dim)
    return tuple(jnp.split(result, [sum(widths[:k]) for k in range(1, len(widths))], axis=along))


def joined_along(blocks, dim):
    shape = list(blocks.shape[1:])
    shape[dim] *= blocks.shape[0]
    return jnp.moveaxis(blocks, 0, dim).reshape(shape)


def copy_for_each(array, axis):
    copies = jnp.broadcast_to(array, (lax.axis_size(axis), *array.shape))
    return lax.all_to_all(copies, axis, split_axis=0, concat_axis=0, tiled=True)


def gather_directly(array, axis, dim):
    return joined_along(copy_for_each(array, axis), dim)


def taken_together(array, axis):
    everything = copy_for_each(array, axis)
    return jnp.sum(everything, axis=0)


def together(arrays, axis):
    ends = [0]
    for a in arrays:
        ends.append(ends[-1] + a.size)
    so_far = taken_together(jnp.concatenate([a.ravel() for a in arrays]), axis)
    return tuple((so_far[b:e].reshape(a.shape) for a, b, e in zip(arrays, ends, ends[1:])))


def norm_rows(values, weights):
    center = jnp.mean(values, axis=-1, keepdims=True)
    second = jnp.mean(values * values, axis=-1, keepdims=True)
    return (
        (values - center)
        * lax.rsqrt(second - center * center + norm_eps)
        * weights.astype(jnp.float32)
    )


def attend(
    query,
    new_key,
    new_value,
    forget_pre,
    forget_bias,
    cache_keys,
    cache_values,
    cache_gates,
    lengths,
):
    seqs_here, width = query.shape
    heads = cache_gates.shape[2]
    head_size = width // heads
    cache_len = cache_keys.shape[1]
    query = query.reshape(seqs_here, heads, head_size)
    new_key = new_key.reshape(seqs_here, heads, head_size)
    new_value = new_value.reshape(seqs_here, heads, head_size)
    keys_all = cache_keys.reshape(seqs_here, cache_len, heads, head_size)
    values_all = cache_values.reshape(seqs_here, cache_len, heads, head_size)
    log_gate = jax.nn.log_sigmoid(forget_pre + forget_bias[None, :])
    position = jnp.arange(cache_len, dtype=jnp.int32)
    is_last = (position[None, :] == (lengths - 1)[:, None]).astype(jnp.float32)
    last_gate = jnp.sum(cache_gates * is_last[:, :, None], axis=1)
    bias = (last_gate + log_gate)[:, :, None] - jnp.transpose(cache_gates, (0, 2, 1))
    scale = head_size ** (-0.5)
    scores = (
        jnp.einsum("shd,slhd->shl", query, keys_all, preferred_element_type=jnp.float32) * scale
        + bias
    )
    valid = (position[None, :] < lengths[:, None])[:, None, :]
    scores = jnp.where(valid, scores, -jnp.inf)
    own_score = jnp.sum(query.astype(jnp.float32) * new_key.astype(jnp.float32), axis=-1) * scale
    top = jnp.maximum(jnp.max(scores, axis=-1), own_score)
    weights_cache = jnp.exp(scores - top[:, :, None])
    weight_own = jnp.exp(own_score - top)
    total = jnp.sum(weights_cache, axis=-1) + weight_own
    probs = (weights_cache / total[:, :, None]).astype(jnp.bfloat16)
    prob_own = (weight_own / total).astype(jnp.bfloat16)
    mixed = jnp.einsum("shl,slhd->shd", probs, values_all, preferred_element_type=jnp.float32)
    mixed = mixed + prob_own.astype(jnp.float32)[:, :, None] * new_value.astype(jnp.float32)
    return mixed.astype(jnp.bfloat16).reshape(seqs_here, width)


def shards(
    tokens,
    w_query,
    w_key,
    w_value,
    w_forget,
    forget_bias,
    cache_keys,
    cache_values,
    cache_gates,
    lengths,
    w_out,
    norm_gain,
    w_router,
    routes,
    dense_gate,
    dense_w_gate,
    dense_w_up,
    dense_w_down,
    expert_w_gate,
    expert_w_up,
    expert_w_down,
    final_gain,
):
    ranks = lax.axis_size("ep")
    rank = lax.axis_index("ep")
    seqs_all, feat_dev = tokens.shape
    offset = rank * feat_dev
    terms = (
        jnp.dot(tokens, w_query, preferred_element_type=jnp.float32),
        jnp.dot(tokens, w_key, preferred_element_type=jnp.float32),
        jnp.dot(tokens, w_value, preferred_element_type=jnp.float32),
        jnp.dot(tokens, w_forget, preferred_element_type=jnp.float32),
    )
    query_sum, key_sum, value_sum, forget_pre = in_one_piece(
        (terms[0], terms[1], terms[2], terms[3]), "ep", 0, 1
    )
    attn = attend(
        query_sum.astype(jnp.bfloat16),
        key_sum.astype(jnp.bfloat16),
        value_sum.astype(jnp.bfloat16),
        forget_pre,
        forget_bias,
        cache_keys,
        cache_values,
        cache_gates,
        lengths,
    )
    head_cols = lax.all_to_all(attn, "ep", split_axis=1, concat_axis=0, tiled=True)
    partial_sum = jnp.dot(head_cols, w_out, preferred_element_type=jnp.float32)
    residual = residual_scale * tokens.astype(jnp.float32)
    placed = lax.dynamic_slice_in_dim(partial_sum, offset, feat_dev, 1) + residual
    mixed_own = sent_and_summed(
        lax.dynamic_update_slice_in_dim(partial_sum, placed, offset, 1), "ep", 0
    )
    normed_own = norm_rows(mixed_own, norm_gain).astype(jnp.bfloat16)
    normed = gather_directly(normed_own, "ep", 0)
    logits = jnp.dot(normed, w_router, preferred_element_type=jnp.float32)
    expert_count = w_router.shape[1]
    picks = (routes[:, :, None] == jnp.arange(expert_count, dtype=jnp.int32)[None, None, :]).astype(
        jnp.float32
    )
    chosen = jnp.sum(logits[:, None, :] * picks, axis=-1)
    route_weight = jax.nn.softmax(chosen, axis=-1)
    expert_id = rank // EXP_SPLIT
    mine = jnp.sum(route_weight * (routes == expert_id).astype(jnp.float32), axis=1)
    expert_gate_part = jnp.dot(normed, expert_w_gate, preferred_element_type=jnp.float32)
    expert_up_part = jnp.dot(normed, expert_w_up, preferred_element_type=jnp.float32)
    expert_hidden = (mine[:, None] * jax.nn.silu(expert_gate_part) * expert_up_part).astype(
        jnp.bfloat16
    )
    dense_scale = jax.nn.sigmoid(jnp.dot(normed, dense_gate, preferred_element_type=jnp.float32))
    dense_gate_part = jnp.dot(normed, dense_w_gate, preferred_element_type=jnp.float32)
    dense_up_part = jnp.dot(normed, dense_w_up, preferred_element_type=jnp.float32)
    dense_hidden = (dense_scale[:, None] * jax.nn.silu(dense_gate_part) * dense_up_part).astype(
        jnp.bfloat16
    )
    width_all = feat_dev * ranks
    dims = (((0,), (1,)), ((), ()))
    branch_part = sent_and_summed(
        lax.dot_general(expert_w_down, expert_hidden, dims, preferred_element_type=jnp.float32)
        + lax.dot_general(dense_w_down, dense_hidden, dims, preferred_element_type=jnp.float32),
        "ep",
        0,
    )
    own_cols = lax.dynamic_slice_in_dim(normed, offset, feat_dev, 1).astype(jnp.float32)
    final_part = residual_scale * jnp.transpose(own_cols) + branch_part
    row_sum, row_squares = together(
        (jnp.sum(final_part, axis=0), jnp.sum(final_part * final_part, axis=0)), "ep"
    )
    center = row_sum / width_all
    second = row_squares / width_all
    unit_part = (final_part - center[None, :]) * lax.rsqrt(second - center * center + norm_eps)[
        None, :
    ]
    result = jnp.transpose(unit_part) * final_gain.astype(jnp.float32)[None, :]
    return result.astype(jnp.bfloat16)


def solution(mesh):
    placed = (
        P("grp", "ep"),
        P("ep", None),
        P("ep", None),
        P("ep", None),
        P("ep", None),
        P(),
        P(("grp", "ep"), None, None),
        P(("grp", "ep"), None, None),
        P(("grp", "ep"), None, None),
        P(("grp", "ep")),
        P("ep", None),
        P(),
        P(),
        P("grp", None),
        P(),
        P(None, "ep"),
        P(None, "ep"),
        P("ep", None),
        P(None, "ep"),
        P(None, "ep"),
        P("ep", None),
        P("ep"),
    )
    return jax.shard_map(
        shards, mesh=mesh, in_specs=placed, out_specs=P("grp", "ep"), check_vma=False
    )
```

profile of v0, /device:TPU:69, one launch (start us, length us, event | category | flops | bytes accessed | tf_op | source)
XLA Modules:
  0.0 239.3 jit_solution(12091949447478172159)
XLA Ops:
  0.0 1.2 fusion.46
  1.2 1.1 fusion.47
  2.3 1.1 fusion.48
  3.4 0.8 fusion.49
  4.3 0.1 pad_maximum_fusion
  4.3 1.4 reshape.129
  5.8 18.5 %all-to-all-start = ((f32[32,2,3088]{2,1,0:T(2,128)}), f32[32,2,3088]{2,1,0:T(2,128)S(1)}, u32[]{:S(2)}, u32[]{:S(2)}) async-start(f32[32,2,3088]{2,1,0:T(2,128)} %reshape.129), calls=%async_computation | async-start | bytes 1638400 | tf_op jit(solution)/shard_map/all_to_all | solution.py:21
  24.3 6.2 %copy.50 = bf16[2,1024,1024]{1,2,0:T(8,128)(2,1)} copy(bf16[2,1024,1024]{2,1,0:T(8,128)(2,1)} %param.28) | data formatting | bytes 8388608 | tf_op args[6]
  30.5 6.3 %copy.51 = bf16[2,1024,1024]{1,2,0:T(8,128)(2,1)} copy(bf16[2,1024,1024]{2,1,0:T(8,128)(2,1)} %param.29) | data formatting | bytes 8388608 | tf_op args[7]
  36.8 0.1 compare_convert_fusion
  36.9 0.1 multiply_reduce_fusion
  37.0 0.1 iota_compare_fusion
  37.0 33.0 %all-to-all-done = f32[32,2,3088]{2,1,0:T(2,128)S(1)} async-done(((f32[32,2,3088]{2,1,0:T(2,128)}), f32[32,2,3088]{2,1,0:T(2,128)S(1)}, u32[]{:S(2)}, u32[]{:S(2)}) %all-to-all-start) | async-done | bytes 790560 | tf_op jit(solution)/shard_map/all_to_all | solution.py:21
  70.1 0.2 reduce_sum.128
  70.3 0.1 reshape.130
  70.4 0.1 reshape.145
  70.5 0.1 reshape.136
  70.6 0.1 multiply_reduce_fusion.3
  70.7 2.9 %fusion.50 = f32[2,16,1,1024]{3,2,1,0:T(1,128)S(1)} fusion(bf16[2,16,64,1]{2,3,1,0:T(2,128)(2,1)S(1)} %reshape.145, bf16[2,1024,16,64]{1,3,2,0:T(8,128)(2,1)} %bitcast.82), kind=kOutput, calls=%fused_computation.89 | convolution fusion | flops 4194304 | bytes 4329472 | tf_op jit(solution)/shard_map/shd,slhd->shl/dot_general | solution.py:97
  73.6 0.2 fusion.44
  73.8 0.2 fusion.17
  74.0 0.1 fusion.26
  74.1 0.1 reshape.137
  74.2 3.4 %fusion.9 = f32[2,16,1,64]{3,2,1,0:T(1,128)S(1)} fusion(bf16[2,1024,16,64]{1,3,2,0:T(8,128)(2,1)} %bitcast.83, bf16[2,16,1024,1]{2,1,0,3:T(8,128)(2,1)S(1)} %fusion.26), kind=kOutput, calls=%fused_computation.16 | convolution fusion | flops 4194304 | bytes 4268032 | tf_op jit(solution)/shard_map/shl,slhd->shd/dot_general | solution.py:109
  77.6 0.1 add_convert_fusion
  77.6 0.1 all_to_all.31
  77.7 0.6 copy.52
  78.4 4.2 %all-to-all-start.1 = ((bf16[2,32,32]{2,0,1:T(2,128)(2,1)}), bf16[2,32,32]{2,0,1:T(2,128)(2,1)S(1)}, u32[]{:S(2)}, u32[]{:S(2)}) async-start(bf16[2,32,32]{2,0,1:T(2,128)(2,1)} %copy.52), calls=%async_computation.1 | async-start | bytes 32768 | tf_op jit(solution)/shard_map/all_to_all | solution.py:162
  82.6 11.8 %all-to-all-done.1 = bf16[2,32,32]{2,0,1:T(2,128)(2,1)S(1)} async-done(((bf16[2,32,32]{2,0,1:T(2,128)(2,1)}), bf16[2,32,32]{2,0,1:T(2,128)(2,1)S(1)}, u32[]{:S(2)}, u32[]{:S(2)}) %all-to-all-start.1) | async-done | bytes 4128 | tf_op jit(solution)/shard_map/all_to_all | solution.py:162
  94.4 0.2 fusion.51
  94.7 0.1 multiply_add_fusion
  94.8 0.6 dynamic_update_slice.3
  95.4 1.1 reshape.133
  96.5 4.5 %all-to-all-start.2 = ((f32[32,2,2048]{2,1,0:T(2,128)}), f32[32,2,2048]{2,1,0:T(2,128)S(1)}, u32[]{:S(2)}, u32[]{:S(2)}) async-start(f32[32,2,2048]{2,1,0:T(2,128)} %reshape.133), calls=%async_computation.2 | async-start | bytes 1048576 | tf_op jit(solution)/shard_map/all_to_all | solution.py:21
  101.0 33.4 %all-to-all-done.2 = f32[32,2,2048]{2,1,0:T(2,128)S(1)} async-done(((f32[32,2,2048]{2,1,0:T(2,128)}), f32[32,2,2048]{2,1,0:T(2,128)S(1)}, u32[]{:S(2)}, u32[]{:S(2)}) %all-to-all-start.2) | async-done | bytes 524320 | tf_op jit(solution)/shard_map/all_to_all | solution.py:21
  134.4 0.7 fusion.43
  135.0 0.1 multiply_reduce_fusion.2
  135.2 0.1 multiply_convert_fusion
  135.3 0.8 broadcast_in_dim.18
  136.1 5.2 %all-to-all-start.3 = ((bf16[32,2,2048]{2,1,0:T(2,128)(2,1)}), bf16[32,2,2048]{2,1,0:T(2,128)(2,1)}, u32[]{:S(2)}, u32[]{:S(2)}) async-start(bf16[32,2,2048]{2,1,0:T(2,128)(2,1)} %broadcast_in_dim.18), calls=%async_computation.3 | async-start | bytes 524288 | tf_op jit(solution)/shard_map/all_to_all | solution.py:40
  141.3 21.4 %all-to-all-done.3 = bf16[32,2,2048]{2,1,0:T(2,128)(2,1)} async-done(((bf16[32,2,2048]{2,1,0:T(2,128)(2,1)}), bf16[32,2,2048]{2,1,0:T(2,128)(2,1)}, u32[]{:S(2)}, u32[]{:S(2)}) %all-to-all-start.3) | async-done | bytes 262176 | tf_op jit(solution)/shard_map/all_to_all | solution.py:40
  162.8 1.0 reshape.134
  163.8 0.2 fusion.52
  164.1 2.1 fusion.53
  166.2 0.9 fusion.54
  167.1 0.2 fusion.7
  167.2 0.7 fusion.37
  168.0 2.5 %fusion.2 = f32[64,2048]{1,0:T(8,128)S(1)} fusion(bf16[512,2048]{1,0:T(8,128)(2,1)S(1)} %copy-done, bf16[64,2048]{1,0:T(8,128)(2,1)S(1)} %reshape.134, bf16[2048,512]{1,0:T(8,128)(2,1)} %param.41, f32[64,512]{1,0:T(8,128)S(1)} %fusion.53, f32[64]{0:T(128)S(1)} %fusion.37), kind=kOutput, calls=%fused_computation.4 | convolution fusion | flops 268664832 | bytes 5112064 | tf_op jit(solution)/shard_map/dot_general | solution.py:194
  170.5 3.1 %fusion = f32[2048,64]{0,1:T(8,128)} fusion(f32[64,2048]{1,0:T(8,128)S(1)} %fusion.2, bf16[256,2048]{1,0:T(8,128)(2,1)} %param.39, bf16[64,2048]{1,0:T(8,128)(2,1)S(1)} %reshape.134, bf16[2048,256]{1,0:T(8,128)(2,1)} %param.38, f32[64,256]{1,0:T(8,128)S(1)} %copy-done.4, f32[64]{0:T(128)S(1)} %fusion.7), kind=kOutput, calls=%fused_computation.1 | convolution fusion | flops 134463488 | bytes 3473664 | tf_op jit(solution)/shard_map/dot_general | solution.py:195
  173.7 1.5 reshape.135
  175.1 1.6 copy.65
  176.7 1.9 reshape.146
  178.6 37.9 %all_to_all.45 = f32[32,1,4096]{2,1,0:T(1,128)S(1)} all-to-all(f32[32,1,4096]{2,1,0:T(1,128)S(1)} %reshape.146), channel_id=1, replica_groups=mesh['grp'=4,'ep'=32] {'ep'}, dimensions={0} | all-to-all | bytes 1048576 | tf_op jit(solution)/shard_map/all_to_all | solution.py:21
  216.5 0.5 broadcast.131
  217.0 2.8 %reduce.2 = f32[32,4096]{1,0:T(8,128)} reduce(f32[32,1,4096]{2,1,0:T(1,128)S(1)} %all_to_all.45, f32[]{:T(128)} %broadcast.131), dimensions={1}, to_apply=%all_to_all.37.reduce_sub_computation | reduce | bytes 1048580 | tf_op jit(solution)/shard_map/all_to_all | solution.py:21
  219.8 1.5 reshape.147
  221.2 0.1 bitcast_reduce_fusion
  221.3 0.2 fusion.33
  221.5 0.1 pad_maximum_fusion.1
  221.6 0.6 broadcast_in_dim.19
  222.2 4.5 %all-to-all-start.5 = ((f32[32,1,128]{2,1,0:T(1,128)}), f32[32,1,128]{2,1,0:T(1,128)S(1)}, u32[]{:S(2)}, u32[]{:S(2)}) async-start(f32[32,1,128]{2,1,0:T(1,128)} %broadcast_in_dim.19), calls=%async_computation.5 | async-start | bytes 32768 | tf_op jit(solution)/shard_map/all_to_all | solution.py:40
  226.7 11.8 %all-to-all-done.5 = f32[32,1,128]{2,1,0:T(1,128)S(1)} async-done(((f32[32,1,128]{2,1,0:T(1,128)}), f32[32,1,128]{2,1,0:T(1,128)S(1)}, u32[]{:S(2)}, u32[]{:S(2)}) %all-to-all-start.5) | async-done | bytes 16416 | tf_op jit(solution)/shard_map/all_to_all | solution.py:40
  238.6 0.1 slice_multiply_fusion
  238.6 0.7 fusion.30
  (40 shorter events, 0.2 us)
Async XLA Ops:
  0.0 168.0 %copy-start = (bf16[512,2048]{1,0:T(8,128)(2,1)S(1)}, bf16[512,2048]{1,0:T(8,128)(2,1)}, u32[]{:S(2)}) copy-start(bf16[512,2048]{1,0:T(8,128)(2,1)} %param.42) | copy-start | bytes 6291460
  5.8 64.3 %all-to-all-start = ((f32[32,2,3088]{2,1,0:T(2,128)}), f32[32,2,3088]{2,1,0:T(2,128)S(1)}, u32[]{:S(2)}, u32[]{:S(2)}) async-start(f32[32,2,3088]{2,1,0:T(2,128)} %reshape.129), calls=%async_computation | async-start | bytes 1638400 | tf_op jit(solution)/shard_map/all_to_all | solution.py:21
  30.5 6.3 %copy-start.10 = (s32[2]{0:T(128)S(1)}, s32[2]{0:T(128)}, u32[]{:S(2)}) copy-start(s32[2]{0:T(128)} %param.31) | copy-start | bytes 28
  30.5 6.4 %copy-start.2 = (f32[2,1024,16]{1,2,0:T(8,128)S(1)}, f32[2,1024,16]{1,2,0:T(8,128)}, u32[]{:S(2)}) copy-start(f32[2,1024,16]{1,2,0:T(8,128)} %param.30) | copy-start | bytes 393220
  70.7 2.9 %copy-start.11 = (f32[16]{0:T(128)S(1)}, f32[16]{0:T(128)}, u32[]{:S(2)}) copy-start(f32[16]{0:T(128)} %param.27) | copy-start | bytes 196
  74.2 20.3 %copy-start.5 = (bf16[32,2048]{1,0:T(8,128)(2,1)S(1)}, bf16[32,2048]{1,0:T(8,128)(2,1)}, u32[]{:S(2)}) copy-start(bf16[32,2048]{1,0:T(8,128)(2,1)} %param.32) | copy-start | bytes 393220
  74.2 20.5 %copy-start.3 = (bf16[64,64]{1,0:T(8,128)(2,1)S(1)}, bf16[64,64]{1,0:T(8,128)(2,1)}, u32[]{:S(2)}) copy-start(bf16[64,64]{1,0:T(8,128)(2,1)} %param.22) | copy-start | bytes 24580
  77.6 23.4 %copy-start.7 = (bf16[2048]{0:T(1024)(128)(2,1)S(1)}, bf16[2048]{0:T(1024)(128)(2,1)}, u32[]{:S(2)}) copy-start(bf16[2048]{0:T(1024)(128)(2,1)} %param.33) | copy-start | bytes 12292
  78.4 16.1 %all-to-all-start.1 = ((bf16[2,32,32]{2,0,1:T(2,128)(2,1)}), bf16[2,32,32]{2,0,1:T(2,128)(2,1)S(1)}, u32[]{:S(2)}, u32[]{:S(2)}) async-start(bf16[2,32,32]{2,0,1:T(2,128)(2,1)} %copy.52), calls=%async_computation.1 | async-start | bytes 32768 | tf_op jit(solution)/shard_map/all_to_all | solution.py:162
  94.4 46.8 %copy-start.8 = (bf16[2048]{0:T(1024)(128)(2,1)S(1)}, bf16[2048]{0:T(1024)(128)(2,1)}, u32[]{:S(2)}) copy-start(bf16[2048]{0:T(1024)(128)(2,1)} %param.36) | copy-start | bytes 12292
  94.7 69.1 %copy-start.6 = (bf16[2048,4]{0,1:T(4,128)(2,1)S(1)}, bf16[2048,4]{0,1:T(4,128)(2,1)}, u32[]{:S(2)}) copy-start(bf16[2048,4]{0,1:T(4,128)(2,1)} %param.34) | copy-start | bytes 49156
  95.3 68.7 %copy-start.9 = (s32[64,2]{0,1:T(2,128)S(1)}, s32[64,2]{0,1:T(2,128)}, u32[]{:S(2)}) copy-start(s32[64,2]{0,1:T(2,128)} %param.35) | copy-start | bytes 1540
  96.5 37.9 %all-to-all-start.2 = ((f32[32,2,2048]{2,1,0:T(2,128)}), f32[32,2,2048]{2,1,0:T(2,128)S(1)}, u32[]{:S(2)}, u32[]{:S(2)}) async-start(f32[32,2,2048]{2,1,0:T(2,128)} %reshape.133), calls=%async_computation.2 | async-start | bytes 1048576 | tf_op jit(solution)/shard_map/all_to_all | solution.py:21
  135.0 31.1 %copy-start.1 = (bf16[2048,256]{1,0:T(8,128)(2,1)S(1)}, bf16[2048,256]{1,0:T(8,128)(2,1)}, u32[]{:S(2)}) copy-start(bf16[2048,256]{1,0:T(8,128)(2,1)} %param.37) | copy-start | bytes 3145732
  136.1 26.7 %all-to-all-start.3 = ((bf16[32,2,2048]{2,1,0:T(2,128)(2,1)}), bf16[32,2,2048]{2,1,0:T(2,128)(2,1)}, u32[]{:S(2)}, u32[]{:S(2)}) async-start(bf16[32,2,2048]{2,1,0:T(2,128)(2,1)} %broadcast_in_dim.18), calls=%async_computation.3 | async-start | bytes 524288 | tf_op jit(solution)/shard_map/all_to_all | solution.py:40
  168.0 2.6 %copy-start.4 = (f32[64,256]{1,0:T(8,128)S(1)}, f32[64,256]{1,0:T(8,128)}, u32[]{:S(2)}) copy-start(f32[64,256]{1,0:T(8,128)} %fusion.54) | copy-start | bytes 196612
  216.5 10.2 %copy-start.12 = (bf16[64]{0:T(256)(128)(2,1)S(1)}, bf16[64]{0:T(256)(128)(2,1)}, u32[]{:S(2)}) copy-start(bf16[64]{0:T(256)(128)(2,1)} %param.43) | copy-start | bytes 388
  222.2 16.3 %all-to-all-start.5 = ((f32[32,1,128]{2,1,0:T(1,128)}), f32[32,1,128]{2,1,0:T(1,128)S(1)}, u32[]{:S(2)}, u32[]{:S(2)}) async-start(f32[32,1,128]{2,1,0:T(1,128)} %broadcast_in_dim.19), calls=%async_computation.5 | async-start | bytes 32768 | tf_op jit(solution)/shard_map/all_to_all | solution.py:40
where the time goes:
time: 241 us; the launch traced here: 239 us
  waiting for transfers between devices  112 us (46%)
  blocking collectives  37.9 us (16%)
  starting transfers between devices  36.9 us (15%)
  local copies, waits for them, and re-layouts  26.1 us (11%)
  matrix products  19.7 us (8%)
  other arithmetic  6.93 us (3%)
    all_to_all x2, waiting for transfers between devices, sent_and_summed(): lax.all_to_all(blocks, axis, split_axis=0, concat_axis=0, tiled=True)  66.4 us
    all_to_all x1, blocking collectives, sent_and_summed(): lax.all_to_all(blocks, axis, split_axis=0, concat_axis=0, tiled=True)  37.9 us
    all_to_all x2, waiting for transfers between devices, copy_for_each(): return lax.all_to_all(copies, axis, split_axis=0, concat_axis=0, tiled=True)  33.3 us
    all_to_all x2, starting transfers between devices, sent_and_summed(): lax.all_to_all(blocks, axis, split_axis=0, concat_axis=0, tiled=True)  23 us
    unnamed x31, local copies, waits for them, and re-layouts  15.9 us
    all_to_all x1, waiting for transfers between devices, shards(): lax.all_to_all(attn, 'ep', split_axis=1, concat_axis=0, tiled=True)  11.8 us
    all_to_all x2, starting transfers between devices, copy_for_each(): return lax.all_to_all(copies, axis, split_axis=0, concat_axis=0, tiled=True)  9.64 us
    reshape x4, local copies, waits for them, and re-layouts, split_up(): array.reshape(*shape[:dim], size, shape[dim] // size, *shape[dim + 1:])  5.58 us
  transfers between devices with their start and end apart: 5, of which 5 were waited for; matrix products, arithmetic and copies ran while one was open for 5% of the time, Pallas kernels for 0%

commit v1 on v0

v1 whole, which is shorter than its diff:
```python
import functools

import jax
import jax.numpy as jnp
from jax import lax
from jax.experimental import pallas as pl
from jax.experimental.pallas import tpu as pltpu
from jax.sharding import PartitionSpec as P

norm_eps = 1e-05
residual_scale = 8.0**0.25
CORES = 2
LANES = 128
bf16 = jnp.bfloat16
f32 = jnp.float32
VM = pltpu.VMEM


def whole(space=VM):
    return pl.BlockSpec(memory_space=space)


def call(kernel, outs, ins, scratch=(), limit=None, cost=None):
    return pl.pallas_call(
        kernel,
        out_shape=outs,
        in_specs=ins,
        out_specs=jax.tree.map(lambda _: whole(), outs),
        scratch_shapes=list(scratch),
        cost_estimate=cost,
        compiler_params=pltpu.CompilerParams(vmem_limit_bytes=limit),
    )


def iota(shape, dim):
    return lax.broadcasted_iota(jnp.int32, shape, dim)


def nt(a, b):
    return lax.dot_general(a, b, (((1,), (1,)), ((), ())), preferred_element_type=f32)


def mm(a, b):
    return jnp.dot(a, b, preferred_element_type=f32)


def project(tok, tokp, wq, wk, wv, wf, pq, pk, pv, pf, wout, out, tok_out, wout_out):
    core = lax.rem(lax.axis_index("ep"), CORES)
    seqs = tok.shape[0]
    rows = seqs // CORES
    here = out.shape[1]
    r = iota((rows, seqs), 0)
    source = (r // here) * (CORES * here) + core * here + lax.rem(r, here)
    pick = (iota((rows, seqs), 1) == source).astype(f32).astype(bf16)
    own = mm(pick, tok[...]).astype(bf16)
    other = mm(pick, tokp[...]).astype(bf16)
    width = wq.shape[1]
    dest = rows // here
    for k, (w, p) in enumerate(((wq, pq), (wk, pk), (wv, pv))):
        term = mm(own, w[...]) + mm(other, p[...])
        out[:, :, k * width : (k + 1) * width] = term.reshape(dest, here, width).astype(bf16)
    heads = wf.shape[0]
    forget = nt(own, wf[...]) + nt(other, pf[...])
    high = forget.astype(bf16).astype(f32)
    low = forget - high
    pad = jnp.zeros((rows, LANES - 2 * heads), f32)
    both = jnp.concatenate([high, low, pad], axis=1)
    out[:, :, 3 * width : 3 * width + LANES] = both.reshape(dest, here, LANES).astype(bf16)
    feats = tok.shape[1]
    first = jnp.where(core == 0, own.astype(f32), other.astype(f32))
    second = jnp.where(core == 0, other.astype(f32), own.astype(f32))
    tok_out[...] = jnp.concatenate([first, second], axis=1)
    for z in range(dest):
        wout_out[z] = wout[:, z * LANES : (z + 1) * LANES]


def attention(got, gates, bias, lengths, keys, values, out):
    dest, here, _ = got.shape
    heads, places = gates.shape[1:]
    width = keys.shape[2]
    size = width // heads
    total = got[0].astype(f32)
    for z in range(1, dest):
        total = total + got[z].astype(f32)
    mine = iota((heads, width), 1) // size == iota((heads, width), 0)
    lane = iota((heads, LANES), 1)
    sub = iota((heads, LANES), 0)
    position = iota((heads, places), 1)
    scale = size**-0.5
    soft = []
    for j in range(here):
        row = total[j : j + 1]
        query = jnp.where(mine, row[:, :width].astype(bf16).astype(f32), 0.0)
        new_key = row[:, width : 2 * width].astype(bf16).astype(f32)
        tail = row[:, 3 * width : 3 * width + LANES]
        forget = jnp.sum(
            jnp.where((lane == sub) | (lane == sub + heads), tail, 0.0), axis=1, keepdims=True
        )
        x = forget + bias[...]
        log_gate = -(jnp.maximum(-x, 0.0) + jnp.log1p(jnp.exp(-jnp.abs(x))))
        gate = gates[j]
        length = lengths[j]
        last = jnp.sum(jnp.where(position == length - 1, gate, 0.0), axis=1, keepdims=True)
        own = jnp.sum(query * new_key, axis=1, keepdims=True) * scale
        scores = nt(query.astype(bf16), keys[j]) * scale + ((last + log_gate) - gate)
        scores = jnp.where(position < length, scores, -jnp.inf)
        top = jnp.maximum(jnp.max(scores, axis=1, keepdims=True), own)
        weights = jnp.exp(scores - top)
        weight_own = jnp.exp(own - top)
        sums = jnp.sum(weights, axis=1, keepdims=True) + weight_own
        soft.append(((weights / sums).astype(bf16), (weight_own / sums).astype(bf16).astype(f32)))
    rows = []
    for j in range(here):
        probs, prob_own = soft[j]
        new_value = total[j : j + 1, 2 * width : 3 * width].astype(bf16).astype(f32)
        mixed = mm(probs, values[j]) + prob_own * new_value
        rows.append(jnp.sum(jnp.where(mine, mixed, 0.0), axis=0, keepdims=True))
    attn = jnp.concatenate(rows, axis=0).astype(bf16)
    for z in range(dest):
        out[z] = attn


def out_project(got, wown, wpar, tok, out, wbuf):
    core = lax.rem(lax.axis_index("ep"), CORES)
    dest, here, width = got.shape
    part = wown.shape[1]
    for z in range(dest):
        wbuf[pl.ds(pl.multiple_of(z * CORES * part + core * part, part), part), :] = wown[z]
        wbuf[pl.ds(pl.multiple_of(z * CORES * part + (1 - core) * part, part), part), :] = wpar[z]
    attn = got[...].astype(f32).reshape(dest * here, width).astype(bf16)
    mixed = (mm(attn, wbuf[...]) + residual_scale * tok[...]).astype(bf16)
    for z in range(dest):
        out[z] = mixed


def feed_forward(
    xown, xpar, gain, small, routes, weg, weu, wdg, wdu, wed, wdd,
    keep, send, rest,
    xbuf,
):
    rank = lax.axis_index("ep")
    core = lax.rem(rank, CORES)
    chips, rows, lanes = xown.shape
    width = chips * lanes
    experts = small.shape[0] // 2
    for z in range(chips):
        at = slice(z * lanes, (z + 1) * lanes)
        xbuf[pl.ds(pl.multiple_of(core * rows, rows), rows), at] = xown[z]
        xbuf[pl.ds(pl.multiple_of((1 - core) * rows, rows), rows), at] = xpar[z]
    x = xbuf[...].astype(f32)
    center = jnp.sum(x, axis=1, keepdims=True) / width
    second = jnp.sum(x * x, axis=1, keepdims=True) / width
    normed = (x - center) * lax.rsqrt(second - center * center + norm_eps) * gain[...].astype(f32)
    normed = normed.astype(bf16)
    xbuf[...] = normed
    logits = nt(normed, small[...])
    slot = iota(logits.shape, 1)
    route0, route1 = routes[:, 0:1], routes[:, 1:2]
    logit0 = jnp.sum(jnp.where(slot == route0, logits, 0.0), axis=1, keepdims=True)
    logit1 = jnp.sum(jnp.where(slot == route1, logits, 0.0), axis=1, keepdims=True)
    peak = jnp.maximum(logit0, logit1)
    e0, e1 = jnp.exp(logit0 - peak), jnp.exp(logit1 - peak)
    expert = rank // (lax.axis_size("ep") // experts)
    weight = (jnp.where(route0 == expert, e0, 0.0) + jnp.where(route1 == expert, e1, 0.0)) / (e0 + e1)
    shut = jnp.sum(jnp.where(slot == experts, logits, 0.0), axis=1, keepdims=True)
    dense = 1.0 / (1.0 + jnp.exp(-shut))
    gate = mm(normed, weg[...])
    up = mm(normed, weu[...])
    hidden_e = (weight * (gate / (1.0 + jnp.exp(-gate))) * up).astype(bf16)
    gate = mm(normed, wdg[...])
    up = mm(normed, wdu[...])
    hidden_d = (dense * (gate / (1.0 + jnp.exp(-gate))) * up).astype(bf16)
    low = iota((rows, lanes), 1) < lanes // 2
    for z in range(chips):
        at = slice(z * lanes, (z + 1) * lanes)
        block = mm(hidden_e, wed[:, at]) + mm(hidden_d, wdd[:, at])
        above, below = block[:rows], block[rows:]
        zero = jnp.where(low, above, pltpu.roll(below, lanes // 2, 1))
        one = jnp.where(low, pltpu.roll(above, lanes // 2, 1), below)
        keep[z] = jnp.where(core == 0, zero, one)
        send[z] = jnp.where(core == 0, one, zero).astype(bf16)
    chip = rank // CORES
    own = xbuf[:, pl.ds(pl.multiple_of(chip * lanes, lanes), lanes)].astype(f32)
    above, below = own[:rows], own[rows:]
    zero = jnp.where(low, above, pltpu.roll(below, lanes // 2, 1))
    one = jnp.where(low, pltpu.roll(above, lanes // 2, 1), below)
    rest[...] = residual_scale * jnp.where(core == 0, zero, one)


def pair_sum(keep, got, out):
    out[...] = (keep[...] + got[...].astype(f32)).astype(bf16)


def gather_sums(got, rest, final, stats):
    chips, rows, lanes = got.shape
    total = rest[...]
    for z in range(chips):
        total = total + got[z].astype(f32)
    final[...] = total
    low = iota((rows, lanes), 1) < lanes // 2
    lane = iota((rows, lanes), 1)
    sub = iota((rows, lanes), 0)
    square = total * total
    line = jnp.zeros((1, lanes), f32)
    for k, v in enumerate(
        (
            jnp.where(low, total, 0.0),
            jnp.where(low, 0.0, total),
            jnp.where(low, square, 0.0),
            jnp.where(low, 0.0, square),
        )
    ):
        column = jnp.sum(v, axis=1, keepdims=True)
        line = line + jnp.sum(jnp.where(lane == sub + k * rows, column, 0.0), axis=0, keepdims=True)
    for d in range(stats.shape[0]):
        stats[d] = line


def finish(final, stats, gain, out):
    rows, lanes = final.shape
    ranks = stats.shape[0]
    line = stats[0]
    for d in range(1, ranks):
        line = line + stats[d]
    lane = iota((rows, lanes), 1)
    sub = iota((rows, lanes), 0)
    low = lane < lanes // 2
    width = ranks * (lanes // 2)
    columns = [
        jnp.sum(jnp.where(lane == sub + k * rows, line, 0.0), axis=1, keepdims=True) / width
        for k in range(4)
    ]
    center = jnp.where(low, columns[0], columns[1])
    second = jnp.where(low, columns[2], columns[3])
    unit = (final[...] - center) * lax.rsqrt(second - center * center + norm_eps)
    unit = (unit * gain[...].astype(f32)).astype(bf16)
    stacked = jnp.concatenate([unit[:, : lanes // 2], unit[:, lanes // 2 :]], axis=0)
    seqs = stacked.shape[0]
    here = seqs // ranks
    s = iota((seqs, seqs), 0)
    inside = lax.rem(s, CORES * here)
    source = (inside // here) * rows + (s // (CORES * here)) * here + lax.rem(inside, here)
    place = (iota((seqs, seqs), 1) == source).astype(f32).astype(bf16)
    out[...] = mm(place, stacked).astype(bf16)


def shards(
    tokens,
    w_query,
    w_key,
    w_value,
    w_forget,
    forget_bias,
    cache_keys,
    cache_values,
    cache_gates,
    lengths,
    w_out,
    norm_gain,
    w_router,
    routes,
    dense_gate,
    dense_w_gate,
    dense_w_up,
    dense_w_down,
    expert_w_gate,
    expert_w_up,
    expert_w_down,
    final_gain,
):
    ranks = lax.axis_size("ep")
    chips = ranks // CORES
    seqs, feats = tokens.shape
    here = seqs // ranks
    rows = seqs // CORES
    width = w_query.shape[1]
    heads = w_forget.shape[1]
    places = cache_keys.shape[1]
    model = w_out.shape[1]
    planes = [[CORES * z + c for z in range(chips)] for c in range(CORES)]
    pairs = [(i, i ^ 1) for i in range(ranks)]
    sds = jax.ShapeDtypeStruct

    def swap(a):
        return lax.ppermute(a, "ep", pairs)

    def exchange(a):
        return lax.all_to_all(
            a, "ep", split_axis=0, concat_axis=0, tiled=True, axis_index_groups=planes
        )

    wf = jnp.transpose(w_forget)
    sent = (tokens, w_query, w_key, w_value, wf)
    tokp, pq, pk, pv, pf = (swap(a) for a in sent)
    terms, tok, wcols = call(
        project,
        (
            sds((chips, here, 3 * width + LANES), bf16),
            sds((rows, LANES), f32),
            sds((chips, w_out.shape[0], LANES), bf16),
        ),
        [whole()] * 11,
        limit=8 << 20,
    )(tokens, tokp, w_query, w_key, w_value, wf, pq, pk, pv, pf, w_out)
    sums = exchange(terms)
    wown = exchange(wcols)
    attn = call(
        attention,
        sds((chips, here, width), bf16),
        [whole(), whole(), whole(), whole(pltpu.SMEM), whole(), whole()],
        limit=14 << 20,
    )(
        sums,
        jnp.transpose(cache_gates, (0, 2, 1)),
        forget_bias.reshape(heads, 1),
        lengths,
        cache_keys,
        cache_values,
    )
    attn_all = exchange(attn)
    wpar = swap(wown)
    mixed = call(
        out_project,
        sds((chips, rows, LANES), bf16),
        [whole()] * 4,
        [VM((width, LANES), bf16)],
        limit=4 << 20,
    )(attn_all, wown, wpar, tok)
    xown = exchange(mixed)
    xpar = swap(xown)
    experts = w_router.shape[1]
    small = jnp.concatenate(
        [
            jnp.transpose(w_router),
            dense_gate[None],
            jnp.zeros((experts - 1, model), bf16),
        ]
    )
    routes_planes = (
        routes.reshape(chips, CORES, here, routes.shape[1])
        .transpose(1, 0, 2, 3)
        .reshape(seqs, routes.shape[1])
    )
    weights = (expert_w_gate, expert_w_up, dense_w_gate, dense_w_up, expert_w_down, dense_w_down)
    keep, send, rest = call(
        feed_forward,
        (
            sds((chips, rows, LANES), f32),
            sds((chips, rows, LANES), bf16),
            sds((rows, LANES), f32),
        ),
        [whole()] * 11,
        [VM((seqs, model), bf16)],
        limit=18 << 20,
    )(xown, xpar, norm_gain[None], small, routes_planes, *weights)
    part = call(pair_sum, sds((chips, rows, LANES), bf16), [whole()] * 2, limit=4 << 20)(
        keep, swap(send)
    )
    final, stats = call(
        gather_sums,
        (sds((rows, LANES), f32), sds((ranks, 1, LANES), f32)),
        [whole()] * 2,
        limit=4 << 20,
    )(exchange(part), rest)
    stats = lax.all_to_all(stats, "ep", split_axis=0, concat_axis=0, tiled=True)
    gain2 = jnp.concatenate([final_gain, final_gain])[None]
    return call(finish, sds((seqs, feats), bf16), [whole()] * 3, limit=4 << 20)(
        final, stats, gain2
    )


def solution(mesh):
    placed = (
        P("grp", "ep"),
        P("ep", None),
        P("ep", None),
        P("ep", None),
        P("ep", None),
        P(),
        P(("grp", "ep"), None, None),
        P(("grp", "ep"), None, None),
        P(("grp", "ep"), None, None),
        P(("grp", "ep")),
        P("ep", None),
        P(),
        P(),
        P("grp", None),
        P(),
        P(None, "ep"),
        P(None, "ep"),
        P("ep", None),
        P(None, "ep"),
        P(None, "ep"),
        P("ep", None),
        P("ep"),
    )
    return jax.shard_map(
        shards, mesh=mesh, in_specs=placed, out_specs=P("grp", "ep"), check_vma=False
    )
```

time: 241 us -> 148 us (0.61)
  waiting for transfers between devices: 112 us -> 37.3 us
  matrix products: 19.7 us -> 0 us
  starting transfers between devices: 36.9 us -> 46.9 us
  Pallas kernels: 0 us -> 8.83 us
  local copies, waits for them, and re-layouts: 26.1 us -> 17.9 us
  other arithmetic: 6.93 us -> 0.15 us
    all_to_all x5 -> x4, waiting for transfers between devices: 112 us -> 33.8 us  [the longest x3 22.4 us: exchange(): lax.all_to_all(a, 'ep', split_axis=0, concat_axis=0, tiled=True, axis_ind...]
    dot_general x13 -> x0, matrix products: 19.7 us -> none  [the longest x1 3.41 us: attend(): jnp.einsum('shl,slhd->shd', probs, values_all, preferred_element_type=jnp...]
    ppermute x0 -> x8, starting transfers between devices: none -> 17.1 us  [swap(): return lax.ppermute(a, 'ep', pairs)]
    pallas_call x0 -> x7, Pallas kernels: none -> 8.83 us  [the longest x1 2.92 us: shards(): call(attention, sds((chips, here, width), bf16), [whole(), whole(), whole...]
    all_to_all x5 -> x4, starting transfers between devices: 36.9 us -> 29.8 us  [the longest x3 22.2 us: exchange(): lax.all_to_all(a, 'ep', split_axis=0, concat_axis=0, tiled=True, axis_ind...]
    reshape x7 -> x3, local copies, waits for them, and re-layouts: 6.8 us -> 1.16 us  [the longest x1 0.73 us: shards(): forget_bias.reshape(heads, 1)]
    ppermute x0 -> x8, waiting for transfers between devices: none -> 3.47 us  [swap(): return lax.ppermute(a, 'ep', pairs)]
    all_to_all x1 -> x0, other arithmetic: 2.75 us -> none  [sent_and_summed(): lax.all_to_all(blocks, axis, split_axis=0, concat_axis=0, tiled=True)]
  transfers between devices with their start and end apart: 5 -> 12, of which waited for: 5 -> 8; matrix products, arithmetic and copies ran while one was open for 5% -> 1% of each run, Pallas kernels for 0% -> 2%
where the time goes in v1:
time: 148 us
  starting transfers between devices  46.9 us (32%)
  waiting for transfers between devices  37.3 us (25%)
  blocking collectives  36.4 us (25%)
  local copies, waits for them, and re-layouts  17.9 us (12%)
  Pallas kernels  8.83 us (6%)
    all_to_all x2, blocking collectives, exchange(): lax.all_to_all(a, 'ep', split_axis=0, concat_axis=0, tiled=True, axis_ind...  36.4 us
    all_to_all x3, waiting for transfers between devices, exchange(): lax.all_to_all(a, 'ep', split_axis=0, concat_axis=0, tiled=True, axis_ind...  22.4 us
    all_to_all x3, starting transfers between devices, exchange(): lax.all_to_all(a, 'ep', split_axis=0, concat_axis=0, tiled=True, axis_ind...  22.2 us
    ppermute x8, starting transfers between devices, swap(): return lax.ppermute(a, 'ep', pairs)  17.1 us
    unnamed x42, local copies, waits for them, and re-layouts  16.6 us
    all_to_all x1, waiting for transfers between devices, shards(): stats = lax.all_to_all(stats, 'ep', split_axis=0, concat_axis=0, tiled=True)  11.4 us
    all_to_all x1, starting transfers between devices, shards(): stats = lax.all_to_all(stats, 'ep', split_axis=0, concat_axis=0, tiled=True)  7.67 us
    ppermute x8, waiting for transfers between devices, swap(): return lax.ppermute(a, 'ep', pairs)  3.47 us
  transfers between devices with their start and end apart: 12, of which 8 were waited for; matrix products, arithmetic and copies ran while one was open for 1% of the time, Pallas kernels for 2%

profile of v1, /device:TPU:69, one launch (start us, length us, event | category | flops | bytes accessed | tf_op | source)
XLA Modules:
  0.0 147.6 jit_solution(8425067447058195930)
XLA Ops:
  0.0 9.9 %collective-permute-start.1 = (bf16[64,1024]{1,0:T(8,128)(2,1)}, bf16[64,1024]{1,0:T(8,128)(2,1)S(1)}, u32[]{:S(2)}, u32[]{:S(2)}) collective-permute-start(bf16[64,1024]{1,0:T(8,128)(2,1)} %wq.1), channel_id=1, source_target_pairs={{0,1},{1,0},{2,3},{3,2},{4,5},{5,4},{6,7},{7,6},{8,9},{9,8},{10,11... | collective-permute-start | bytes 393224 | tf_op jit(solution)/shard_map/ppermute | solution.py:285
  9.9 0.0 collective-permute-start.2
  9.9 0.5 collective-permute-start.3
  10.4 0.0 collective-permute-start
  10.4 0.5 collective-permute-start.4
  10.9 1.0 collective-permute-done.4.pf
  12.0 0.0 collective-permute-done.tokp
  12.0 0.0 collective-permute-done.1.pq
  12.0 0.0 collective-permute-done.2.pk
  12.0 0.0 collective-permute-done.3.pv
  12.0 0.0 copy-start.9
  12.0 0.9 copy-done.9
  12.9 0.0 copy-start.10
  12.9 0.9 copy-done.10
  13.8 0.0 copy-start.11
  13.8 0.9 copy-done.11
  14.7 0.9 copy-done.12
  15.6 0.7 copy-done.13
  16.3 0.7 copy-done.14
  17.0 1.1 shard_map.208
  18.2 20.9 %all_to_all.30.got = bf16[16,2,3200]{2,1,0:T(2,128)(2,1)S(1)} all-to-all(bf16[16,2,3200]{2,1,0:T(2,128)(2,1)S(1)} %get-tuple-element.13), channel_id=1, replica_groups={{0,2,4,6,8,10,12,14,16,18,20,22,24,26,28,30},{1,3,5,7,9,11,13,15,17,19,..., dimensions={0} | all-to-all | bytes 409600 | tf_op jit(solution)/shard_map/all_to_all | solution.py:288
  39.0 8.9 %all-to-all-start.2 = ((bf16[16,32,128]{2,1,0:T(8,128)(2,1)}), bf16[16,32,128]{2,1,0:T(8,128)(2,1)S(1)}, u32[]{:S(2)}, u32[]{:S(2)}) async-start(bf16[16,32,128]{2,1,0:T(8,128)(2,1)} %get-tuple-element.14), calls=%async_computation.2 | async-start | bytes 262144 | tf_op jit(solution)/shard_map/all_to_all | solution.py:288
  47.9 0.7 copy.26.bias
  48.6 2.2 %copy-done = bf16[2,1024,1024]{2,1,0:T(8,128)(2,1)S(1)} copy-done((bf16[2,1024,1024]{2,1,0:T(8,128)(2,1)S(1)}, bf16[2,1024,1024]{2,1,0:T(8,128)(2,1)}, u32[]{:S(2)}) %copy-start) | copy-done | bytes 4194328
  50.8 2.2 %copy-done.1 = bf16[2,1024,1024]{2,1,0:T(8,128)(2,1)S(1)} copy-done((bf16[2,1024,1024]{2,1,0:T(8,128)(2,1)S(1)}, bf16[2,1024,1024]{2,1,0:T(8,128)(2,1)}, u32[]{:S(2)}) %copy-start.1) | copy-done | bytes 4194328
  53.0 0.9 copy-done.8
  53.9 0.7 copy-done.15
  54.6 0.0 copy-start.2
  54.6 0.0 copy-start.5
  54.6 2.9 %shard_map.209 = bf16[16,2,1024]{2,1,0:T(2,128)(2,1)} custom-call(bf16[16,2,3200]{2,1,0:T(2,128)(2,1)S(1)} %all_to_all.30.got, f32[2,16,1024]{2,1,0:T(8,128)S(1)} %bitcast.10, f32[16,1]{1,0:T(8,128)S(1)} %copy.26.bias, s32[2]{0:T(128)S(1)} %copy-done.15, bf16[2,1024,1024]{2,1,0:T(8,128)(2,1)S(1)} %copy-done, bf16[2,1024,1024]{2,1,0:T(8,128)(2,1)S(1)} %copy-done.1), custom_call_target="tpu_custom_call" | custom-call | tf_op jit(solution)/shard_map/pallas_call | solution.py:307
  57.5 2.1 %all-to-all-done.2.wown = bf16[16,32,128]{2,1,0:T(8,128)(2,1)S(1)} async-done(((bf16[16,32,128]{2,1,0:T(8,128)(2,1)}), bf16[16,32,128]{2,1,0:T(8,128)(2,1)S(1)}, u32[]{:S(2)}, u32[]{:S(2)}) %all-to-all-start.2) | async-done | bytes 131104 | tf_op jit(solution)/shard_map/all_to_all | solution.py:288
  59.7 9.3 %all-to-all-start.1 = ((bf16[16,2,1024]{2,1,0:T(2,128)(2,1)}), bf16[16,2,1024]{2,1,0:T(2,128)(2,1)S(1)}, u32[]{:S(2)}, u32[]{:S(2)}) async-start(bf16[16,2,1024]{2,1,0:T(2,128)(2,1)} %shard_map.209), calls=%async_computation.1 | async-start | bytes 131072 | tf_op jit(solution)/shard_map/all_to_all | solution.py:288
  69.0 1.7 %collective-permute-start.5 = (bf16[16,32,128]{2,1,0:T(8,128)(2,1)S(1)}, bf16[16,32,128]{2,1,0:T(8,128)(2,1)S(1)}, u32[]{:S(2)}, u32[]{:S(2)}) collective-permute-start(bf16[16,32,128]{2,1,0:T(8,128)(2,1)S(1)} %all-to-all-done.2.wown), channel_id=1, source_target_pairs={{0,1},{1,0},{2,3},{3,2},{4,5},{5,4},{6,7},{7,6},{8,9},{9,8},{10,11... | collective-permute-start | bytes 393224 | tf_op jit(solution)/shard_map/ppermute | solution.py:285
  70.7 1.0 collective-permute-done.5.wpar
  71.7 8.8 %all-to-all-done.1.got = bf16[16,2,1024]{2,1,0:T(2,128)(2,1)S(1)} async-done(((bf16[16,2,1024]{2,1,0:T(2,128)(2,1)}), bf16[16,2,1024]{2,1,0:T(2,128)(2,1)S(1)}, u32[]{:S(2)}, u32[]{:S(2)}) %all-to-all-start.1) | async-done | bytes 65568 | tf_op jit(solution)/shard_map/all_to_all | solution.py:288
  80.5 0.9 shard_map.210
  81.4 4.0 %all-to-all-start.3 = ((bf16[16,32,128]{2,1,0:T(8,128)(2,1)}), bf16[16,32,128]{2,1,0:T(8,128)(2,1)S(1)}, u32[]{:S(2)}, u32[]{:S(2)}) async-start(bf16[16,32,128]{2,1,0:T(8,128)(2,1)} %shard_map.210), calls=%async_computation.3 | async-start | bytes 262144 | tf_op jit(solution)/shard_map/all_to_all | solution.py:288
  85.3 0.0 copy-done.17
  85.4 0.1 pad.4.clone
  85.4 11.4 %all-to-all-done.3.xown = bf16[16,32,128]{2,1,0:T(8,128)(2,1)S(1)} async-done(((bf16[16,32,128]{2,1,0:T(8,128)(2,1)}), bf16[16,32,128]{2,1,0:T(8,128)(2,1)S(1)}, u32[]{:S(2)}, u32[]{:S(2)}) %all-to-all-start.3) | async-done | bytes 131104 | tf_op jit(solution)/shard_map/all_to_all | solution.py:288
  96.9 4.1 %collective-permute-start.6 = (bf16[16,32,128]{2,1,0:T(8,128)(2,1)S(1)}, bf16[16,32,128]{2,1,0:T(8,128)(2,1)S(1)}, u32[]{:S(2)}, u32[]{:S(2)}) collective-permute-start(bf16[16,32,128]{2,1,0:T(8,128)(2,1)S(1)} %all-to-all-done.3.xown), channel_id=1, source_target_pairs={{0,1},{1,0},{2,3},{3,2},{4,5},{5,4},{6,7},{7,6},{8,9},{9,8},{10,11... | collective-permute-start | bytes 393224 | tf_op jit(solution)/shard_map/ppermute | solution.py:285
  100.9 0.0 copy-done.16
  100.9 0.1 maximum_maximum_fusion.small
  101.0 0.0 copy-done.19
  101.0 0.1 reshape.10
  101.1 0.3 copy.29
  101.4 0.0 copy-done.18
  101.5 0.5 collective-permute-done.6.xpar
  101.9 0.0 copy-done.2
  101.9 0.0 copy-done.5
  101.9 1.6 %copy-done.3 = bf16[2048,512]{1,0:T(8,128)(2,1)S(1)} copy-done((bf16[2048,512]{1,0:T(8,128)(2,1)S(1)}, bf16[2048,512]{1,0:T(8,128)(2,1)}, u32[]{:S(2)}) %copy-start.3) | copy-done | bytes 2097176
  103.5 1.6 %copy-done.4 = bf16[512,2048]{1,0:T(8,128)(2,1)S(1)} copy-done((bf16[512,2048]{1,0:T(8,128)(2,1)S(1)}, bf16[512,2048]{1,0:T(8,128)(2,1)}, u32[]{:S(2)}) %copy-start.4) | copy-done | bytes 2097176
  105.1 1.2 copy-done.6
  106.3 1.2 copy-done.7
  107.6 2.2 %shard_map.211 = (f32[16,32,128]{2,1,0:T(8,128)S(1)}, bf16[16,32,128]{2,1,0:T(8,128)(2,1)S(1)}, f32[32,128]{1,0:T(8,128)S(1)}) custom-call(bf16[16,32,128]{2,1,0:T(8,128)(2,1)S(1)} %all-to-all-done.3.xown, bf16[16,32,128]{2,1,0:T(8,128)(2,1)S(1)} %collective-permute-done.6.xpar, bf16[1,2048]{1,0:T(2,128)(2,1)S(1)} %broadcast_in_dim.12.gain, ...), custom_call_target="tpu_custom_call" | custom-call | tf_op jit(solution)/shard_map/pallas_call | solution.py:345
  109.8 0.5 collective-permute-start.7
  110.2 1.0 collective-permute-done.7.got
  111.3 15.5 %all_to_all.31.got = bf16[16,32,128]{2,1,0:T(8,128)(2,1)S(1)} all-to-all(bf16[16,32,128]{2,1,0:T(8,128)(2,1)S(1)} %shard_map.212), channel_id=1, replica_groups={{0,2,4,6,8,10,12,14,16,18,20,22,24,26,28,30},{1,3,5,7,9,11,13,15,17,19,..., dimensions={0} | all-to-all | bytes 262144 | tf_op jit(solution)/shard_map/all_to_all | solution.py:288
  126.8 0.7 shard_map.213
  127.5 7.7 %all-to-all-start.5 = ((f32[32,1,128]{2,1,0:T(1,128)}), f32[32,1,128]{2,1,0:T(1,128)S(1)}, u32[]{:S(2)}, u32[]{:S(2)}) async-start(f32[32,1,128]{2,1,0:T(1,128)} %get-tuple-element.20), calls=%async_computation.5 | async-start | bytes 32768 | tf_op jit(solution)/shard_map/all_to_all | solution.py:365
  135.2 0.0 copy-done.20
  135.2 0.1 maximum_bitcast_fusion.gain
  135.3 11.4 %all-to-all-done.5.stats = f32[32,1,128]{2,1,0:T(1,128)S(1)} async-done(((f32[32,1,128]{2,1,0:T(1,128)}), f32[32,1,128]{2,1,0:T(1,128)S(1)}, u32[]{:S(2)}, u32[]{:S(2)}) %all-to-all-start.5) | async-done | bytes 16416 | tf_op jit(solution)/shard_map/all_to_all | solution.py:365
  146.7 0.9 shard_map.214
  (20 shorter events, 0.1 us)
Async XLA Ops:
  0.0 12.0 %collective-permute-start.1 = (bf16[64,1024]{1,0:T(8,128)(2,1)}, bf16[64,1024]{1,0:T(8,128)(2,1)S(1)}, u32[]{:S(2)}, u32[]{:S(2)}) collective-permute-start(bf16[64,1024]{1,0:T(8,128)(2,1)} %wq.1), channel_id=1, source_target_pairs={{0,1},{1,0},{2,3},{3,2},{4,5},{5,4},{6,7},{7,6},{8,9},{9,8},{10,11... | collective-permute-start | bytes 393224 | tf_op jit(solution)/shard_map/ppermute | solution.py:285
  9.9 2.1 %collective-permute-start.2 = (bf16[64,1024]{1,0:T(8,128)(2,1)}, bf16[64,1024]{1,0:T(8,128)(2,1)S(1)}, u32[]{:S(2)}, u32[]{:S(2)}) collective-permute-start(bf16[64,1024]{1,0:T(8,128)(2,1)} %wk.1), channel_id=1, source_target_pairs={{0,1},{1,0},{2,3},{3,2},{4,5},{5,4},{6,7},{7,6},{8,9},{9,8},{10,11... | collective-permute-start | bytes 393224 | tf_op jit(solution)/shard_map/ppermute | solution.py:285
  9.9 2.1 %collective-permute-start.3 = (bf16[64,1024]{1,0:T(8,128)(2,1)}, bf16[64,1024]{1,0:T(8,128)(2,1)S(1)}, u32[]{:S(2)}, u32[]{:S(2)}) collective-permute-start(bf16[64,1024]{1,0:T(8,128)(2,1)} %wv.1), channel_id=1, source_target_pairs={{0,1},{1,0},{2,3},{3,2},{4,5},{5,4},{6,7},{7,6},{8,9},{9,8},{10,11... | collective-permute-start | bytes 393224 | tf_op jit(solution)/shard_map/ppermute | solution.py:285
  10.4 1.5 %collective-permute-start = (bf16[64,64]{1,0:T(8,128)(2,1)}, bf16[64,64]{1,0:T(8,128)(2,1)S(1)}, u32[]{:S(2)}, u32[]{:S(2)}) collective-permute-start(bf16[64,64]{1,0:T(8,128)(2,1)} %tok.1), channel_id=1, source_target_pairs={{0,1},{1,0},{2,3},{3,2},{4,5},{5,4},{6,7},{7,6},{8,9},{9,8},{10,11... | collective-permute-start | bytes 24584 | tf_op jit(solution)/shard_map/ppermute | solution.py:285
  10.4 1.5 %collective-permute-start.4 = (bf16[16,64]{1,0:T(8,128)(2,1)}, bf16[16,64]{1,0:T(8,128)(2,1)S(1)}, u32[]{:S(2)}, u32[]{:S(2)}) collective-permute-start(bf16[16,64]{1,0:T(8,128)(2,1)} %bitcast.12), channel_id=1, source_target_pairs={{0,1},{1,0},{2,3},{3,2},{4,5},{5,4},{6,7},{7,6},{8,9},{9,8},{10,11... | collective-permute-start | bytes 6152 | tf_op jit(solution)/shard_map/ppermute | solution.py:285
  12.0 0.9 copy-start.9
  12.9 0.9 copy-start.10
  13.8 0.9 copy-start.11
  14.7 0.9 copy-start.12
  15.6 0.7 copy-start.13
  16.3 0.7 copy-start.14
  39.0 20.7 %all-to-all-start.2 = ((bf16[16,32,128]{2,1,0:T(8,128)(2,1)}), bf16[16,32,128]{2,1,0:T(8,128)(2,1)S(1)}, u32[]{:S(2)}, u32[]{:S(2)}) async-start(bf16[16,32,128]{2,1,0:T(8,128)(2,1)} %get-tuple-element.14), calls=%async_computation.2 | async-start | bytes 262144 | tf_op jit(solution)/shard_map/all_to_all | solution.py:288
  48.6 2.2 %copy-start = (bf16[2,1024,1024]{2,1,0:T(8,128)(2,1)S(1)}, bf16[2,1024,1024]{2,1,0:T(8,128)(2,1)}, u32[]{:S(2)}) copy-start(bf16[2,1024,1024]{2,1,0:T(8,128)(2,1)} %keys.1) | copy-start | bytes 12582916
  50.8 2.2 %copy-start.1 = (bf16[2,1024,1024]{2,1,0:T(8,128)(2,1)S(1)}, bf16[2,1024,1024]{2,1,0:T(8,128)(2,1)}, u32[]{:S(2)}) copy-start(bf16[2,1024,1024]{2,1,0:T(8,128)(2,1)} %values.1) | copy-start | bytes 12582916
  53.0 0.9 copy-start.8
  53.9 0.7 copy-start.15
  54.6 30.7 %copy-start.17 = (bf16[2048]{0:T(1024)(128)(2,1)S(1)}, bf16[2048]{0:T(1024)(128)(2,1)}, u32[]{:S(2)}) copy-start(bf16[2048]{0:T(1024)(128)(2,1)} %param.36) | copy-start | bytes 12292
  54.6 46.3 %copy-start.16 = (bf16[2048,4]{0,1:T(4,128)(2,1)S(1)}, bf16[2048,4]{0,1:T(4,128)(2,1)}, u32[]{:S(2)}) copy-start(bf16[2048,4]{0,1:T(4,128)(2,1)} %param.34) | copy-start | bytes 49156
  54.6 46.4 %copy-start.19 = (s32[64,2]{0,1:T(2,128)S(1)}, s32[64,2]{0,1:T(2,128)}, u32[]{:S(2)}) copy-start(s32[64,2]{0,1:T(2,128)} %param.35) | copy-start | bytes 1540
  54.6 46.9 %copy-start.18 = (bf16[2048]{0:T(1024)(128)(2,1)S(1)}, bf16[2048]{0:T(1024)(128)(2,1)}, u32[]{:S(2)}) copy-start(bf16[2048]{0:T(1024)(128)(2,1)} %param.33) | copy-start | bytes 12292
  54.6 47.3 %copy-start.2 = (bf16[2048,512]{1,0:T(8,128)(2,1)S(1)}, bf16[2048,512]{1,0:T(8,128)(2,1)}, u32[]{:S(2)}) copy-start(bf16[2048,512]{1,0:T(8,128)(2,1)} %weg.1) | copy-start | bytes 6291460
  54.6 47.3 %copy-start.5 = (bf16[2048,256]{1,0:T(8,128)(2,1)S(1)}, bf16[2048,256]{1,0:T(8,128)(2,1)}, u32[]{:S(2)}) copy-start(bf16[2048,256]{1,0:T(8,128)(2,1)} %wdg.1) | copy-start | bytes 3145732
  59.7 20.8 %all-to-all-start.1 = ((bf16[16,2,1024]{2,1,0:T(2,128)(2,1)}), bf16[16,2,1024]{2,1,0:T(2,128)(2,1)S(1)}, u32[]{:S(2)}, u32[]{:S(2)}) async-start(bf16[16,2,1024]{2,1,0:T(2,128)(2,1)} %shard_map.209), calls=%async_computation.1 | async-start | bytes 131072 | tf_op jit(solution)/shard_map/all_to_all | solution.py:288
  69.0 2.6 %collective-permute-start.5 = (bf16[16,32,128]{2,1,0:T(8,128)(2,1)S(1)}, bf16[16,32,128]{2,1,0:T(8,128)(2,1)S(1)}, u32[]{:S(2)}, u32[]{:S(2)}) collective-permute-start(bf16[16,32,128]{2,1,0:T(8,128)(2,1)S(1)} %all-to-all-done.2.wown), channel_id=1, source_target_pairs={{0,1},{1,0},{2,3},{3,2},{4,5},{5,4},{6,7},{7,6},{8,9},{9,8},{10,11... | collective-permute-start | bytes 393224 | tf_op jit(solution)/shard_map/ppermute | solution.py:285
  81.4 15.5 %all-to-all-start.3 = ((bf16[16,32,128]{2,1,0:T(8,128)(2,1)}), bf16[16,32,128]{2,1,0:T(8,128)(2,1)S(1)}, u32[]{:S(2)}, u32[]{:S(2)}) async-start(bf16[16,32,128]{2,1,0:T(8,128)(2,1)} %shard_map.210), calls=%async_computation.3 | async-start | bytes 262144 | tf_op jit(solution)/shard_map/all_to_all | solution.py:288
  96.9 5.0 %collective-permute-start.6 = (bf16[16,32,128]{2,1,0:T(8,128)(2,1)S(1)}, bf16[16,32,128]{2,1,0:T(8,128)(2,1)S(1)}, u32[]{:S(2)}, u32[]{:S(2)}) collective-permute-start(bf16[16,32,128]{2,1,0:T(8,128)(2,1)S(1)} %all-to-all-done.3.xown), channel_id=1, source_target_pairs={{0,1},{1,0},{2,3},{3,2},{4,5},{5,4},{6,7},{7,6},{8,9},{9,8},{10,11... | collective-permute-start | bytes 393224 | tf_op jit(solution)/shard_map/ppermute | solution.py:285
  101.9 1.6 %copy-start.3 = (bf16[2048,512]{1,0:T(8,128)(2,1)S(1)}, bf16[2048,512]{1,0:T(8,128)(2,1)}, u32[]{:S(2)}) copy-start(bf16[2048,512]{1,0:T(8,128)(2,1)} %weu.1) | copy-start | bytes 6291460
  103.5 1.6 %copy-start.4 = (bf16[512,2048]{1,0:T(8,128)(2,1)S(1)}, bf16[512,2048]{1,0:T(8,128)(2,1)}, u32[]{:S(2)}) copy-start(bf16[512,2048]{1,0:T(8,128)(2,1)} %wed.1) | copy-start | bytes 6291460
  105.1 1.2 copy-start.6
  106.3 1.2 copy-start.7
  107.6 27.7 %copy-start.20 = (bf16[64]{0:T(256)(128)(2,1)S(1)}, bf16[64]{0:T(256)(128)(2,1)}, u32[]{:S(2)}) copy-start(bf16[64]{0:T(256)(128)(2,1)} %param.43) | copy-start | bytes 388
  109.8 1.5 collective-permute-start.7
  127.5 19.2 %all-to-all-start.5 = ((f32[32,1,128]{2,1,0:T(1,128)}), f32[32,1,128]{2,1,0:T(1,128)S(1)}, u32[]{:S(2)}, u32[]{:S(2)}) async-start(f32[32,1,128]{2,1,0:T(1,128)} %get-tuple-element.20), calls=%async_computation.5 | async-start | bytes 32768 | tf_op jit(solution)/shard_map/all_to_all | solution.py:365

commit v2 on v1

--- a/solution.py
+++ b/solution.py
@@ -1,11 +1,10 @@
-import functools
-
 import jax
 import jax.numpy as jnp
 from jax import lax
 from jax.experimental import pallas as pl
 from jax.experimental.pallas import tpu as pltpu
 from jax.sharding import PartitionSpec as P
+
 
 norm_eps = 1e-05
 residual_scale = 8.0**0.25
@@ -14,20 +13,20 @@
 bf16 = jnp.bfloat16
 f32 = jnp.float32
 VM = pltpu.VMEM
+HBM = pltpu.HBM
 
 
 def whole(space=VM):
     return pl.BlockSpec(memory_space=space)
 
 
-def call(kernel, outs, ins, scratch=(), limit=None, cost=None):
+def call(kernel, outs, ins, scratch=(), limit=None):
     return pl.pallas_call(
         kernel,
         out_shape=outs,
         in_specs=ins,
         out_specs=jax.tree.map(lambda _: whole(), outs),
         scratch_shapes=list(scratch),
-        cost_estimate=cost,
         compiler_params=pltpu.CompilerParams(vmem_limit_bytes=limit),
     )
 
@@ -44,7 +43,25 @@
     return jnp.dot(a, b, preferred_element_type=f32)
 
 
-def project(tok, tokp, wq, wk, wv, wf, pq, pk, pv, pf, wout, out, tok_out, wout_out):
+def project(
+    tokp, pq, pk, pv, pf, tok_hbm, wq_hbm, wk_hbm, wv_hbm, wf_hbm, wout_hbm,
+    out, tok_out, tok, wq, wk, wv, wf, wout, pairs, sems,
+):
+    copies = [
+        pltpu.make_async_copy(src, dst, sems.at[k])
+        for k, (src, dst) in enumerate(
+            (
+                (tok_hbm, tok),
+                (wq_hbm, wq),
+                (wk_hbm, wk),
+                (wv_hbm, wv),
+                (wf_hbm, wf),
+                (wout_hbm, wout),
+            )
+        )
+    ]
+    for c in copies:
+        c.start()
     core = lax.rem(lax.axis_index("ep"), CORES)
     seqs = tok.shape[0]
     rows = seqs // CORES
@@ -52,41 +69,104 @@
     r = iota((rows, seqs), 0)
     source = (r // here) * (CORES * here) + core * here + lax.rem(r, here)
     pick = (iota((rows, seqs), 1) == source).astype(f32).astype(bf16)
+    other = mm(pick, tokp[...]).astype(bf16)
+    copies[0].wait()
     own = mm(pick, tok[...]).astype(bf16)
-    other = mm(pick, tokp[...]).astype(bf16)
     width = wq.shape[1]
     dest = rows // here
     for k, (w, p) in enumerate(((wq, pq), (wk, pk), (wv, pv))):
+        copies[k + 1].wait()
         term = mm(own, w[...]) + mm(other, p[...])
         out[:, :, k * width : (k + 1) * width] = term.reshape(dest, here, width).astype(bf16)
     heads = wf.shape[0]
+    copies[4].wait()
     forget = nt(own, wf[...]) + nt(other, pf[...])
     high = forget.astype(bf16).astype(f32)
     low = forget - high
     pad = jnp.zeros((rows, LANES - 2 * heads), f32)
     both = jnp.concatenate([high, low, pad], axis=1)
     out[:, :, 3 * width : 3 * width + LANES] = both.reshape(dest, here, LANES).astype(bf16)
-    feats = tok.shape[1]
     first = jnp.where(core == 0, own.astype(f32), other.astype(f32))
     second = jnp.where(core == 0, other.astype(f32), own.astype(f32))
     tok_out[...] = jnp.concatenate([first, second], axis=1)
+    copies[5].wait()
+    steps = pairs.shape[0]
+    pairs[...] = wout[...].reshape(pairs.shape)
+    base = 3 * width + LANES
     for z in range(dest):
-        wout_out[z] = wout[:, z * LANES : (z + 1) * LANES]
-
-
-def attention(got, gates, bias, lengths, keys, values, out):
+        for t in range(steps):
+            out[z, :, base + t * LANES : base + (t + 1) * LANES] = pairs[
+                t, :, z * LANES : (z + 1) * LANES
+            ]
+
+
+def unpack_columns(got, out):
     dest, here, _ = got.shape
-    heads, places = gates.shape[1:]
-    width = keys.shape[2]
+    steps = out.shape[1] // here
+    base = got.shape[2] - steps * LANES
+    for z in range(dest):
+        out[z] = jnp.concatenate(
+            [
+                got[z, :, base + t * LANES : base + (t + 1) * LANES].astype(f32)
+                for t in range(steps)
+            ],
+            axis=0,
+        ).astype(bf16)
+
+
+def load_cache(lengths, keys_hbm, gates_hbm, keys, bias, gates, sems):
+    copies = [
+        pltpu.make_async_copy(gates_hbm, gates, sems.at[0]),
+        pltpu.make_async_copy(keys_hbm.at[0], keys, sems.at[1]),
+    ]
+    for c in copies:
+        c.start()
+    copies[0].wait()
+    for j in range(gates.shape[0]):
+        gate = gates[j]
+        length = lengths[j]
+        position = iota(gate.shape, 1)
+        last = jnp.sum(jnp.where(position == length - 1, gate, 0.0), axis=1, keepdims=True)
+        bias[j] = jnp.where(position < length, last - gate, -jnp.inf)
+    copies[1].wait()
+
+
+def load_all(*refs):
+    count = len(refs) // 2
+    sems = refs[-1]
+    copies = [
+        pltpu.make_async_copy(refs[k], refs[count + k], sems.at[k]) for k in range(count)
+    ]
+    for c in copies:
+        c.start()
+    for c in copies:
+        c.wait()
+
+
+def attention(
+    got, bias, forget_bias, first, keys_hbm, values_hbm, out, keys, values, sems
+):
+    dest, here, _ = got.shape
+    heads = bias.shape[1]
+    width = first.shape[1]
+    kcopy = [
+        pltpu.make_async_copy(keys_hbm.at[j], keys.at[j - 1], sems.at[0, j]) for j in range(1, here)
+    ]
+    vcopy = [
+        pltpu.make_async_copy(values_hbm.at[j], values.at[j], sems.at[1, j]) for j in range(here)
+    ]
+    for c in kcopy + vcopy:
+        c.start()
     size = width // heads
-    total = got[0].astype(f32)
+    used = 3 * width + LANES
+    total = got[0, :, :used].astype(f32)
     for z in range(1, dest):
-        total = total + got[z].astype(f32)
+        total = total + got[z, :, :used].astype(f32)
     mine = iota((heads, width), 1) // size == iota((heads, width), 0)
     lane = iota((heads, LANES), 1)
     sub = iota((heads, LANES), 0)
-    position = iota((heads, places), 1)
     scale = size**-0.5
+    added = jnp.sum(jnp.where(lane == sub, forget_bias[...], 0.0), axis=1, keepdims=True)
     soft = []
     for j in range(here):
         row = total[j : j + 1]
@@ -96,14 +176,13 @@
         forget = jnp.sum(
             jnp.where((lane == sub) | (lane == sub + heads), tail, 0.0), axis=1, keepdims=True
         )
-        x = forget + bias[...]
+        x = forget + added
         log_gate = -(jnp.maximum(-x, 0.0) + jnp.log1p(jnp.exp(-jnp.abs(x))))
-        gate = gates[j]
-        length = lengths[j]
-        last = jnp.sum(jnp.where(position == length - 1, gate, 0.0), axis=1, keepdims=True)
         own = jnp.sum(query * new_key, axis=1, keepdims=True) * scale
-        scores = nt(query.astype(bf16), keys[j]) * scale + ((last + log_gate) - gate)
-        scores = jnp.where(position < length, scores, -jnp.inf)
+        if j > 0:
+            kcopy[j - 1].wait()
+        keys_here = first[...] if j == 0 else keys[j - 1]
+        scores = nt(query.astype(bf16), keys_here) * scale + (bias[j] + log_gate)
         top = jnp.maximum(jnp.max(scores, axis=1, keepdims=True), own)
         weights = jnp.exp(scores - top)
         weight_own = jnp.exp(own - top)
@@ -113,6 +192,7 @@
     for j in range(here):
         probs, prob_own = soft[j]
         new_value = total[j : j + 1, 2 * width : 3 * width].astype(bf16).astype(f32)
+        vcopy[j].wait()
         mixed = mm(probs, values[j]) + prob_own * new_value
         rows.append(jnp.sum(jnp.where(mine, mixed, 0.0), axis=0, keepdims=True))
     attn = jnp.concatenate(rows, axis=0).astype(bf16)
@@ -134,43 +214,72 @@
 
 
 def feed_forward(
-    xown, xpar, gain, small, routes, weg, weu, wdg, wdu, wed, wdd,
+    xown, xpar, gain, shutter, router, routes, weg, wdg,
+    weu_hbm, wdu_hbm, wed_hbm, wdd_hbm,
     keep, send, rest,
-    xbuf,
+    xbuf, weu, wdu, wed, wdd, sems,
 ):
     rank = lax.axis_index("ep")
+    ranks = lax.axis_size("ep")
     core = lax.rem(rank, CORES)
+    copies = [
+        pltpu.make_async_copy(src, dst, sems.at[k])
+        for k, (src, dst) in enumerate(
+            ((weu_hbm, weu), (wdu_hbm, wdu), (wed_hbm, wed), (wdd_hbm, wdd))
+        )
+    ]
+    for c in copies:
+        c.start()
     chips, rows, lanes = xown.shape
     width = chips * lanes
-    experts = small.shape[0] // 2
-    for z in range(chips):
-        at = slice(z * lanes, (z + 1) * lanes)
-        xbuf[pl.ds(pl.multiple_of(core * rows, rows), rows), at] = xown[z]
-        xbuf[pl.ds(pl.multiple_of((1 - core) * rows, rows), rows), at] = xpar[z]
-    x = xbuf[...].astype(f32)
-    center = jnp.sum(x, axis=1, keepdims=True) / width
-    second = jnp.sum(x * x, axis=1, keepdims=True) / width
-    normed = (x - center) * lax.rsqrt(second - center * center + norm_eps) * gain[...].astype(f32)
-    normed = normed.astype(bf16)
-    xbuf[...] = normed
-    logits = nt(normed, small[...])
+    seqs = CORES * rows
+    here = seqs // ranks
+    experts = router.shape[0]
+    low = iota((rows, lanes), 1) < lanes // 2
+    chip = rank // CORES
+    for half, ref in ((core, xown), (1 - core, xpar)):
+        x = ref[...].astype(f32)
+        ones = jnp.sum(x, axis=0)
+        squares = jnp.sum(x * x, axis=0)
+        center = jnp.sum(ones, axis=1, keepdims=True) / width
+        second = jnp.sum(squares, axis=1, keepdims=True) / width
+        factor = lax.rsqrt(second - center * center + norm_eps)
+        for z in range(chips):
+            block = (x[z] - center) * factor * gain[z : z + 1, :].astype(f32)
+            xbuf[pl.ds(pl.multiple_of(half * rows, rows), rows), z * lanes : (z + 1) * lanes] = (
+                block.astype(bf16)
+            )
+    normed = xbuf[...]
+    logits = nt(normed, router[...])
     slot = iota(logits.shape, 1)
-    route0, route1 = routes[:, 0:1], routes[:, 1:2]
+    r = iota((seqs, seqs), 0)
+    inside = lax.rem(r, rows)
+    source = (inside // here) * (CORES * here) + (r // rows) * here + lax.rem(inside, here)
+    same = iota((seqs, seqs), 1) == source
+    route0 = jnp.sum(jnp.where(same, routes[0:1, :], 0), axis=1, keepdims=True)
+    route1 = jnp.sum(jnp.where(same, routes[1:2, :], 0), axis=1, keepdims=True)
     logit0 = jnp.sum(jnp.where(slot == route0, logits, 0.0), axis=1, keepdims=True)
     logit1 = jnp.sum(jnp.where(slot == route1, logits, 0.0), axis=1, keepdims=True)
     peak = jnp.maximum(logit0, logit1)
     e0, e1 = jnp.exp(logit0 - peak), jnp.exp(logit1 - peak)
-    expert = rank // (lax.axis_size("ep") // experts)
+    expert = rank // (ranks // experts)
     weight = (jnp.where(route0 == expert, e0, 0.0) + jnp.where(route1 == expert, e1, 0.0)) / (e0 + e1)
-    shut = jnp.sum(jnp.where(slot == experts, logits, 0.0), axis=1, keepdims=True)
+    shut = jnp.zeros((seqs, lanes), f32)
+    for z in range(chips):
+        block = xbuf[:, z * lanes : (z + 1) * lanes].astype(f32)
+        shut = shut + block * shutter[z : z + 1, :].astype(f32)
+    shut = jnp.sum(shut, axis=1, keepdims=True)
     dense = 1.0 / (1.0 + jnp.exp(-shut))
-    gate = mm(normed, weg[...])
-    up = mm(normed, weu[...])
-    hidden_e = (weight * (gate / (1.0 + jnp.exp(-gate))) * up).astype(bf16)
-    gate = mm(normed, wdg[...])
-    up = mm(normed, wdu[...])
-    hidden_d = (dense * (gate / (1.0 + jnp.exp(-gate))) * up).astype(bf16)
-    low = iota((rows, lanes), 1) < lanes // 2
+    gate_e = mm(normed, weg[...])
+    gate_d = mm(normed, wdg[...])
+    copies[0].wait()
+    up_e = mm(normed, weu[...])
+    hidden_e = (weight * (gate_e / (1.0 + jnp.exp(-gate_e))) * up_e).astype(bf16)
+    copies[1].wait()
+    up_d = mm(normed, wdu[...])
+    hidden_d = (dense * (gate_d / (1.0 + jnp.exp(-gate_d))) * up_d).astype(bf16)
+    copies[2].wait()
+    copies[3].wait()
     for z in range(chips):
         at = slice(z * lanes, (z + 1) * lanes)
         block = mm(hidden_e, wed[:, at]) + mm(hidden_d, wdd[:, at])
@@ -179,7 +288,6 @@
         one = jnp.where(low, pltpu.roll(above, lanes // 2, 1), below)
         keep[z] = jnp.where(core == 0, zero, one)
         send[z] = jnp.where(core == 0, one, zero).astype(bf16)
-    chip = rank // CORES
     own = xbuf[:, pl.ds(pl.multiple_of(chip * lanes, lanes), lanes)].astype(f32)
     above, below = own[:rows], own[rows:]
     zero = jnp.where(low, above, pltpu.roll(below, lanes // 2, 1))
@@ -233,8 +341,8 @@
     center = jnp.where(low, columns[0], columns[1])
     second = jnp.where(low, columns[2], columns[3])
     unit = (final[...] - center) * lax.rsqrt(second - center * center + norm_eps)
-    unit = (unit * gain[...].astype(f32)).astype(bf16)
     stacked = jnp.concatenate([unit[:, : lanes // 2], unit[:, lanes // 2 :]], axis=0)
+    stacked = (stacked * gain[...].reshape(1, lanes // 2).astype(f32)).astype(bf16)
     seqs = stacked.shape[0]
     here = seqs // ranks
     s = iota((seqs, seqs), 0)
@@ -281,6 +389,9 @@
     pairs = [(i, i ^ 1) for i in range(ranks)]
     sds = jax.ShapeDtypeStruct
 
+    def far(arrays):
+        return tuple(pltpu.with_memory_space_constraint(a, HBM) for a in arrays)
+
     def swap(a):
         return lax.ppermute(a, "ep", pairs)
 
@@ -289,34 +400,49 @@
             a, "ep", split_axis=0, concat_axis=0, tiled=True, axis_index_groups=planes
         )
 
+    dma = pltpu.SemaphoreType.DMA
     wf = jnp.transpose(w_forget)
     sent = (tokens, w_query, w_key, w_value, wf)
-    tokp, pq, pk, pv, pf = (swap(a) for a in sent)
-    terms, tok, wcols = call(
+    arrived = tuple(swap(a) for a in sent)
+    terms, tok = call(
         project,
         (
-            sds((chips, here, 3 * width + LANES), bf16),
+            sds((chips, here, 3 * width + LANES + w_out.shape[0] // here * LANES), bf16),
             sds((rows, LANES), f32),
-            sds((chips, w_out.shape[0], LANES), bf16),
         ),
-        [whole()] * 11,
+        [whole()] * 5 + [whole(HBM)] * 6,
+        [VM(a.shape, bf16) for a in (*sent, w_out)]
+        + [VM((w_out.shape[0] // here, here, model), bf16), dma((6,))],
         limit=8 << 20,
-    )(tokens, tokp, w_query, w_key, w_value, wf, pq, pk, pv, pf, w_out)
+    )(*arrived, *far((*sent, w_out)))
     sums = exchange(terms)
-    wown = exchange(wcols)
+    wown = call(
+        unpack_columns,
+        sds((chips, w_out.shape[0], LANES), bf16),
+        [whole()],
+        limit=4 << 20,
+    )(sums)
+    gates = jnp.transpose(cache_gates, (0, 2, 1))
+    far_keys, far_values, gates = far((cache_keys, cache_values, gates))
+    first, bias = call(
+        load_cache,
+        (VM(cache_keys.shape[1:], bf16), VM(gates.shape, f32)),
+        [whole(pltpu.SMEM)] + [whole(HBM)] * 2,
+        [VM(gates.shape, f32), dma((2,))],
+        limit=4 << 20,
+    )(lengths, far_keys, gates)
+    forget_row = jnp.pad(forget_bias, (0, LANES - heads))[None]
     attn = call(
         attention,
         sds((chips, here, width), bf16),
-        [whole(), whole(), whole(), whole(pltpu.SMEM), whole(), whole()],
+        [whole()] * 4 + [whole(HBM)] * 2,
+        [
+            VM((here - 1, places, width), bf16),
+            VM((here, places, width), bf16),
+            dma((2, here)),
+        ],
         limit=14 << 20,
-    )(
-        sums,
-        jnp.transpose(cache_gates, (0, 2, 1)),
-        forget_bias.reshape(heads, 1),
-        lengths,
-        cache_keys,
-        cache_values,
-    )
+    )(sums, bias, forget_row, first, far_keys, far_values)
     attn_all = exchange(attn)
     wpar = swap(wown)
     mixed = call(
@@ -328,20 +454,16 @@
     )(attn_all, wown, wpar, tok)
     xown = exchange(mixed)
     xpar = swap(xown)
-    experts = w_router.shape[1]
-    small = jnp.concatenate(
-        [
-            jnp.transpose(w_router),
-            dense_gate[None],
-            jnp.zeros((experts - 1, model), bf16),
-        ]
-    )
-    routes_planes = (
-        routes.reshape(chips, CORES, here, routes.shape[1])
-        .transpose(1, 0, 2, 3)
-        .reshape(seqs, routes.shape[1])
-    )
-    weights = (expert_w_gate, expert_w_up, dense_w_gate, dense_w_up, expert_w_down, dense_w_down)
+    weights = far(
+        (expert_w_gate, dense_w_gate, expert_w_up, dense_w_up, expert_w_down, dense_w_down)
+    )
+    first = call(
+        load_all,
+        tuple(VM(w.shape, bf16) for w in weights[:2]),
+        [whole(HBM)] * 2,
+        [dma((2,))],
+        limit=4 << 20,
+    )(*weights[:2])
     keep, send, rest = call(
         feed_forward,
         (
@@ -349,10 +471,19 @@
             sds((chips, rows, LANES), bf16),
             sds((rows, LANES), f32),
         ),
-        [whole()] * 11,
-        [VM((seqs, model), bf16)],
+        [whole()] * 8 + [whole(HBM)] * 4,
+        [VM((seqs, model), bf16)] + [VM(w.shape, bf16) for w in weights[2:]] + [dma((4,))],
         limit=18 << 20,
-    )(xown, xpar, norm_gain[None], small, routes_planes, *weights)
+    )(
+        xown,
+        xpar,
+        norm_gain.reshape(chips, LANES),
+        dense_gate.reshape(chips, LANES),
+        jnp.transpose(w_router),
+        jnp.transpose(routes),
+        *first,
+        *weights[2:],
+    )
     part = call(pair_sum, sds((chips, rows, LANES), bf16), [whole()] * 2, limit=4 << 20)(
         keep, swap(send)
     )
@@ -363,9 +494,8 @@
         limit=4 << 20,
     )(exchange(part), rest)
     stats = lax.all_to_all(stats, "ep", split_axis=0, concat_axis=0, tiled=True)
-    gain2 = jnp.concatenate([final_gain, final_gain])[None]
     return call(finish, sds((seqs, feats), bf16), [whole()] * 3, limit=4 << 20)(
-        final, stats, gain2
+        final, stats, final_gain
     )
 
 
@@ -394,6 +524,7 @@
         P("ep", None),
         P("ep"),
     )
+
     return jax.shard_map(
         shards, mesh=mesh, in_specs=placed, out_specs=P("grp", "ep"), check_vma=False
     )

time: 148 us -> 129 us (0.87)
  local copies, waits for them, and re-layouts: 17.9 us -> 0.69 us
  blocking collectives: 36.4 us -> 50.1 us
  waiting for transfers between devices: 37.3 us -> 25.1 us
  starting transfers between devices: 46.9 us -> 36 us
  Pallas kernels: 8.83 us -> 16.4 us
    all_to_all x0 -> x1, blocking collectives: none -> 19 us  [shards(): stats = lax.all_to_all(stats, 'ep', split_axis=0, concat_axis=0, tiled=True)]
    unnamed x42 -> x14, local copies, waits for them, and re-layouts: 16.6 us -> 0.69 us
    all_to_all x1 -> x0, waiting for transfers between devices: 11.4 us -> none  [shards(): stats = lax.all_to_all(stats, 'ep', split_axis=0, concat_axis=0, tiled=True)]
    all_to_all x1 -> x0, starting transfers between devices: 7.67 us -> none  [shards(): stats = lax.all_to_all(stats, 'ep', split_axis=0, concat_axis=0, tiled=True)]
    pallas_call x2 -> x5, Pallas kernels: 4.07 us -> 10.8 us  [the longest x1 3.94 us: shards(): call(attention, sds((chips, here, width), bf16), [whole()] * 4 + [whole(H...]
    all_to_all x2, blocking collectives: 36.4 us -> 31.1 us  [exchange(): lax.all_to_all(a, 'ep', split_axis=0, concat_axis=0, tiled=True, axis_ind...]
    pallas_call x1, Pallas kernels: 2.2 us -> 4.26 us  [shards(): call(feed_forward, (sds((chips, rows, LANES), f32), sds((chips, rows, LAN...]
    all_to_all x3 -> x2, starting transfers between devices: 22.2 us -> 20.3 us  [exchange(): lax.all_to_all(a, 'ep', split_axis=0, concat_axis=0, tiled=True, axis_ind...]
  transfers between devices with their start and end apart: 12 -> 10, of which waited for: 8 -> 5; matrix products, arithmetic and copies ran while one was open for 1% -> 0% of each run, Pallas kernels for 2% -> 3%
where the time goes in v2:
time: 129 us; the launch traced here: 128 us
  blocking collectives  50.1 us (39%)
  starting transfers between devices  36 us (28%)
  waiting for transfers between devices  25.1 us (19%)
  Pallas kernels  16.4 us (13%)
    all_to_all x2, blocking collectives, exchange(): lax.all_to_all(a, 'ep', split_axis=0, concat_axis=0, tiled=True, axis_ind...  31.1 us
    all_to_all x2, waiting for transfers between devices, exchange(): lax.all_to_all(a, 'ep', split_axis=0, concat_axis=0, tiled=True, axis_ind...  21.7 us
    all_to_all x2, starting transfers between devices, exchange(): lax.all_to_all(a, 'ep', split_axis=0, concat_axis=0, tiled=True, axis_ind...  20.3 us
    all_to_all x1, blocking collectives, shards(): stats = lax.all_to_all(stats, 'ep', split_axis=0, concat_axis=0, tiled=True)  19 us
    ppermute x8, starting transfers between devices, swap(): return lax.ppermute(a, 'ep', pairs)  15.7 us
    pallas_call x1, Pallas kernels, shards(): call(feed_forward, (sds((chips, rows, LANES), f32), sds((chips, rows, LAN...  4.26 us
    pallas_call x1, Pallas kernels, shards(): call(attention, sds((chips, here, width), bf16), [whole()] * 4 + [whole(H...  3.94 us
    ppermute x8, waiting for transfers between devices, swap(): return lax.ppermute(a, 'ep', pairs)  3.35 us
  transfers between devices with their start and end apart: 10, of which 5 were waited for; matrix products, arithmetic and copies ran while one was open for 0% of the time, Pallas kernels for 3%

profile of v2, /device:TPU:69, one launch (start us, length us, event | category | flops | bytes accessed | tf_op | source)
XLA Modules:
  0.0 128.5 jit_solution(1325171931024801534)
XLA Ops:
  0.0 9.9 %collective-permute-start.1 = (bf16[64,1024]{1,0:T(8,128)(2,1)}, bf16[64,1024]{1,0:T(8,128)(2,1)S(1)}, u32[]{:S(2)}, u32[]{:S(2)}) collective-permute-start(bf16[64,1024]{1,0:T(8,128)(2,1)} %wq_hbm.1), channel_id=1, source_target_pairs={{0,1},{1,0},{2,3},{3,2},{4,5},{5,4},{6,7},{7,6},{8,9},{9,8},{10,11... | collective-permute-start | bytes 393224 | tf_op jit(solution)/shard_map/ppermute | solution.py:396
  9.9 0.0 collective-permute-start.2
  9.9 0.5 collective-permute-start.3
  10.4 0.0 collective-permute-start
  10.4 0.5 collective-permute-start.4
  10.9 1.0 collective-permute-done.4.pf
  12.0 0.0 collective-permute-done.tokp
  12.0 0.0 collective-permute-done.1.pq
  12.0 0.0 collective-permute-done.2.pk
  12.0 0.0 collective-permute-done.3.pv
  12.0 2.7 %shard_map.208 = (bf16[16,2,5248]{2,1,0:T(2,128)(2,1)}, f32[32,128]{1,0:T(8,128)S(1)}) custom-call(bf16[64,64]{1,0:T(8,128)(2,1)S(1)} %collective-permute-done.tokp, bf16[64,1024]{1,0:T(8,128)(2,1)S(1)} %collective-permute-done.1.pq, bf16[64,1024]{1,0:T(8,128)(2,1)S(1)} %collective-permute-done.2.pk, bf16[64,1024]{1,0:T(8,128)(2,1)S(1)} %collective-permute-done.3.pv, ...), custom_call_target="tpu_custom_call" | custom-call | tf_op jit(solution)/shard_map/pallas_call | solution.py:407
  14.7 8.3 %all-to-all-start = ((bf16[16,2,5248]{2,1,0:T(2,128)(2,1)}), bf16[16,2,5248]{2,1,0:T(2,128)(2,1)S(1)}, u32[]{:S(2)}, u32[]{:S(2)}) async-start(bf16[16,2,5248]{2,1,0:T(2,128)(2,1)} %get-tuple-element.16), calls=%async_computation | async-start | bytes 671744 | tf_op jit(solution)/shard_map/all_to_all | solution.py:399
  22.9 0.0 copy-start.4
  23.0 0.6 copy-done.4
  23.6 0.0 copy-start.6
  23.6 2.2 %shard_map.209 = (bf16[1024,1024]{1,0:T(8,128)(2,1)S(1)}, f32[2,16,1024]{2,1,0:T(8,128)S(1)}) custom-call(s32[2]{0:T(128)S(1)} %copy-done.4, bf16[2,1024,1024]{2,1,0:T(8,128)(2,1)} %keys_hbm.3, f32[2,16,1024]{2,1,0:T(8,128)} %bitcast.12), custom_call_target="tpu_custom_call" | custom-call | tf_op jit(solution)/shard_map/pallas_call | solution.py:427
  25.8 0.0 copy-done.6
  25.9 12.5 %all-to-all-done.got = bf16[16,2,5248]{2,1,0:T(2,128)(2,1)S(1)} async-done(((bf16[16,2,5248]{2,1,0:T(2,128)(2,1)}), bf16[16,2,5248]{2,1,0:T(2,128)(2,1)S(1)}, u32[]{:S(2)}, u32[]{:S(2)}) %all-to-all-start) | async-done | bytes 335904 | tf_op jit(solution)/shard_map/all_to_all | solution.py:399
  38.4 3.9 %shard_map.210 = bf16[16,2,1024]{2,1,0:T(2,128)(2,1)} custom-call(bf16[16,2,5248]{2,1,0:T(2,128)(2,1)S(1)} %all-to-all-done.got, f32[2,16,1024]{2,1,0:T(8,128)S(1)} %get-tuple-element.17.bias, f32[1,128]{1,0:T(1,128)S(1)} %pad_bitcast_fusion.forget_bias, bf16[1024,1024]{1,0:T(8,128)(2,1)S(1)} %get-tuple-element.18.first, bf16[2,1024,1024]{2,1,0:T(8,128)(2,1)} %keys_hbm.3, ...), custom_call_target="tpu_custom_call" | custom-call | tf_op jit(solution)/shard_map/pallas_call | solution.py:435
  42.3 12.0 %all-to-all-start.1 = ((bf16[16,2,1024]{2,1,0:T(2,128)(2,1)}), bf16[16,2,1024]{2,1,0:T(2,128)(2,1)S(1)}, u32[]{:S(2)}, u32[]{:S(2)}) async-start(bf16[16,2,1024]{2,1,0:T(2,128)(2,1)} %shard_map.210), calls=%async_computation.1 | async-start | bytes 131072 | tf_op jit(solution)/shard_map/all_to_all | solution.py:399
  54.3 0.0 copy-start
  54.3 0.0 copy-start.1
  54.3 0.0 copy-start.2
  54.3 0.0 copy-start.3
  54.4 0.1 shard_map.211.wown
  54.5 1.0 collective-permute-start.5
  55.5 1.0 collective-permute-done.5.wpar
  56.5 9.2 %all-to-all-done.1.got = bf16[16,2,1024]{2,1,0:T(2,128)(2,1)S(1)} async-done(((bf16[16,2,1024]{2,1,0:T(2,128)(2,1)}), bf16[16,2,1024]{2,1,0:T(2,128)(2,1)S(1)}, u32[]{:S(2)}, u32[]{:S(2)}) %all-to-all-start.1) | async-done | bytes 65568 | tf_op jit(solution)/shard_map/all_to_all | solution.py:399
  65.7 0.2 shard_map.212
  65.9 15.6 %all_to_all.25.xown = bf16[16,32,128]{2,1,0:T(8,128)(2,1)S(1)} all-to-all(bf16[16,32,128]{2,1,0:T(8,128)(2,1)S(1)} %shard_map.212), channel_id=1, replica_groups={{0,2,4,6,8,10,12,14,16,18,20,22,24,26,28,30},{1,3,5,7,9,11,13,15,17,19,..., dimensions={0} | all-to-all | bytes 262144 | tf_op jit(solution)/shard_map/all_to_all | solution.py:399
  81.5 3.7 %collective-permute-start.6 = (bf16[16,32,128]{2,1,0:T(8,128)(2,1)S(1)}, bf16[16,32,128]{2,1,0:T(8,128)(2,1)S(1)}, u32[]{:S(2)}, u32[]{:S(2)}) collective-permute-start(bf16[16,32,128]{2,1,0:T(8,128)(2,1)S(1)} %all_to_all.25.xown), channel_id=1, source_target_pairs={{0,1},{1,0},{2,3},{3,2},{4,5},{5,4},{6,7},{7,6},{8,9},{9,8},{10,11... | collective-permute-start | bytes 393224 | tf_op jit(solution)/shard_map/ppermute | solution.py:396
  85.2 1.9 %shard_map.213 = (bf16[2048,512]{1,0:T(8,128)(2,1)S(1)}, bf16[2048,256]{1,0:T(8,128)(2,1)S(1)}) custom-call(bf16[2048,512]{1,0:T(8,128)(2,1)} %refs_0_.1, bf16[2048,256]{1,0:T(8,128)(2,1)} %refs_1_.1), custom_call_target="tpu_custom_call" | custom-call | tf_op jit(solution)/shard_map/pallas_call | solution.py:460
  87.1 0.0 collective-permute-done.6.xpar
  87.1 0.0 copy-done
  87.1 0.0 copy-done.1
  87.1 0.0 copy-done.2
  87.1 0.0 copy-done.3
  87.1 0.0 copy-start.5
  87.1 4.3 %shard_map.214 = (f32[16,32,128]{2,1,0:T(8,128)S(1)}, bf16[16,32,128]{2,1,0:T(8,128)(2,1)S(1)}, f32[32,128]{1,0:T(8,128)S(1)}) custom-call(bf16[16,32,128]{2,1,0:T(8,128)(2,1)S(1)} %all_to_all.25.xown, bf16[16,32,128]{2,1,0:T(8,128)(2,1)S(1)} %collective-permute-done.6.xpar, bf16[16,128]{1,0:T(8,128)(2,1)S(1)} %bitcast.9, bf16[16,128]{1,0:T(8,128)(2,1)S(1)} %bitcast.10, ...), custom_call_target="tpu_custom_call" | custom-call | tf_op jit(solution)/shard_map/pallas_call | solution.py:467
  91.4 0.1 collective-permute-start.7
  91.5 1.3 %collective-permute-done.7.got = bf16[16,32,128]{2,1,0:T(8,128)(2,1)S(1)} collective-permute-done((bf16[16,32,128]{2,1,0:T(8,128)(2,1)S(1)}, bf16[16,32,128]{2,1,0:T(8,128)(2,1)S(1)}, u32[]{:S(2)}, u32[]{:S(2)}) %collective-permute-start.7) | collective-permute-done | bytes 131104 | tf_op jit(solution)/shard_map/ppermute | solution.py:396
  92.9 15.5 %all_to_all.26.got = bf16[16,32,128]{2,1,0:T(8,128)(2,1)S(1)} all-to-all(bf16[16,32,128]{2,1,0:T(8,128)(2,1)S(1)} %shard_map.215), channel_id=1, replica_groups={{0,2,4,6,8,10,12,14,16,18,20,22,24,26,28,30},{1,3,5,7,9,11,13,15,17,19,..., dimensions={0} | all-to-all | bytes 262144 | tf_op jit(solution)/shard_map/all_to_all | solution.py:399
  108.4 0.1 shard_map.216
  108.5 19.0 %all_to_all.27.stats = f32[32,1,128]{2,1,0:T(1,128)S(1)} all-to-all(f32[32,1,128]{2,1,0:T(1,128)S(1)} %get-tuple-element.26), channel_id=1, replica_groups=mesh['grp'=4,'ep'=32] {'ep'}, dimensions={0} | all-to-all | bytes 32768 | tf_op jit(solution)/shard_map/all_to_all | solution.py:496
  127.5 0.0 copy-done.5
  127.5 0.9 shard_map.217
  (2 shorter events, 0.0 us)
Async XLA Ops:
  0.0 12.0 %collective-permute-start.1 = (bf16[64,1024]{1,0:T(8,128)(2,1)}, bf16[64,1024]{1,0:T(8,128)(2,1)S(1)}, u32[]{:S(2)}, u32[]{:S(2)}) collective-permute-start(bf16[64,1024]{1,0:T(8,128)(2,1)} %wq_hbm.1), channel_id=1, source_target_pairs={{0,1},{1,0},{2,3},{3,2},{4,5},{5,4},{6,7},{7,6},{8,9},{9,8},{10,11... | collective-permute-start | bytes 393224 | tf_op jit(solution)/shard_map/ppermute | solution.py:396
  9.9 2.1 %collective-permute-start.2 = (bf16[64,1024]{1,0:T(8,128)(2,1)}, bf16[64,1024]{1,0:T(8,128)(2,1)S(1)}, u32[]{:S(2)}, u32[]{:S(2)}) collective-permute-start(bf16[64,1024]{1,0:T(8,128)(2,1)} %wk_hbm.1), channel_id=1, source_target_pairs={{0,1},{1,0},{2,3},{3,2},{4,5},{5,4},{6,7},{7,6},{8,9},{9,8},{10,11... | collective-permute-start | bytes 393224 | tf_op jit(solution)/shard_map/ppermute | solution.py:396
  9.9 2.1 %collective-permute-start.3 = (bf16[64,1024]{1,0:T(8,128)(2,1)}, bf16[64,1024]{1,0:T(8,128)(2,1)S(1)}, u32[]{:S(2)}, u32[]{:S(2)}) collective-permute-start(bf16[64,1024]{1,0:T(8,128)(2,1)} %wv_hbm.1), channel_id=1, source_target_pairs={{0,1},{1,0},{2,3},{3,2},{4,5},{5,4},{6,7},{7,6},{8,9},{9,8},{10,11... | collective-permute-start | bytes 393224 | tf_op jit(solution)/shard_map/ppermute | solution.py:396
  10.4 1.5 %collective-permute-start = (bf16[64,64]{1,0:T(8,128)(2,1)}, bf16[64,64]{1,0:T(8,128)(2,1)S(1)}, u32[]{:S(2)}, u32[]{:S(2)}) collective-permute-start(bf16[64,64]{1,0:T(8,128)(2,1)} %tok_hbm.1), channel_id=1, source_target_pairs={{0,1},{1,0},{2,3},{3,2},{4,5},{5,4},{6,7},{7,6},{8,9},{9,8},{10,11... | collective-permute-start | bytes 24584 | tf_op jit(solution)/shard_map/ppermute | solution.py:396
  10.4 1.5 %collective-permute-start.4 = (bf16[16,64]{1,0:T(8,128)(2,1)}, bf16[16,64]{1,0:T(8,128)(2,1)S(1)}, u32[]{:S(2)}, u32[]{:S(2)}) collective-permute-start(bf16[16,64]{1,0:T(8,128)(2,1)} %bitcast.13), channel_id=1, source_target_pairs={{0,1},{1,0},{2,3},{3,2},{4,5},{5,4},{6,7},{7,6},{8,9},{9,8},{10,11... | collective-permute-start | bytes 6152 | tf_op jit(solution)/shard_map/ppermute | solution.py:396
  14.7 23.7 %all-to-all-start = ((bf16[16,2,5248]{2,1,0:T(2,128)(2,1)}), bf16[16,2,5248]{2,1,0:T(2,128)(2,1)S(1)}, u32[]{:S(2)}, u32[]{:S(2)}) async-start(bf16[16,2,5248]{2,1,0:T(2,128)(2,1)} %get-tuple-element.16), calls=%async_computation | async-start | bytes 671744 | tf_op jit(solution)/shard_map/all_to_all | solution.py:399
  22.9 0.7 copy-start.4
  23.6 2.2 %copy-start.6 = (f32[16]{0:T(128)S(1)}, f32[16]{0:T(128)}, u32[]{:S(2)}) copy-start(f32[16]{0:T(128)} %param.27) | copy-start | bytes 196
  42.3 23.4 %all-to-all-start.1 = ((bf16[16,2,1024]{2,1,0:T(2,128)(2,1)}), bf16[16,2,1024]{2,1,0:T(2,128)(2,1)S(1)}, u32[]{:S(2)}, u32[]{:S(2)}) async-start(bf16[16,2,1024]{2,1,0:T(2,128)(2,1)} %shard_map.210), calls=%async_computation.1 | async-start | bytes 131072 | tf_op jit(solution)/shard_map/all_to_all | solution.py:399
  54.3 32.8 %copy-start = (bf16[2048,4]{0,1:T(4,128)(2,1)S(1)}, bf16[2048,4]{0,1:T(4,128)(2,1)}, u32[]{:S(2)}) copy-start(bf16[2048,4]{0,1:T(4,128)(2,1)} %param.34) | copy-start | bytes 49156
  54.3 32.8 %copy-start.1 = (bf16[2048]{0:T(1024)(128)(2,1)S(1)}, bf16[2048]{0:T(1024)(128)(2,1)}, u32[]{:S(2)}) copy-start(bf16[2048]{0:T(1024)(128)(2,1)} %param.33) | copy-start | bytes 12292
  54.3 32.8 %copy-start.2 = (bf16[2048]{0:T(1024)(128)(2,1)S(1)}, bf16[2048]{0:T(1024)(128)(2,1)}, u32[]{:S(2)}) copy-start(bf16[2048]{0:T(1024)(128)(2,1)} %param.36) | copy-start | bytes 12292
  54.3 32.8 %copy-start.3 = (s32[64,2]{0,1:T(2,128)S(1)}, s32[64,2]{0,1:T(2,128)}, u32[]{:S(2)}) copy-start(s32[64,2]{0,1:T(2,128)} %param.35) | copy-start | bytes 1540
  54.5 2.0 %collective-permute-start.5 = (bf16[16,32,128]{2,1,0:T(8,128)(2,1)S(1)}, bf16[16,32,128]{2,1,0:T(8,128)(2,1)S(1)}, u32[]{:S(2)}, u32[]{:S(2)}) collective-permute-start(bf16[16,32,128]{2,1,0:T(8,128)(2,1)S(1)} %shard_map.211.wown), channel_id=1, source_target_pairs={{0,1},{1,0},{2,3},{3,2},{4,5},{5,4},{6,7},{7,6},{8,9},{9,8},{10,11... | collective-permute-start | bytes 393224 | tf_op jit(solution)/shard_map/ppermute | solution.py:396
  81.5 5.6 %collective-permute-start.6 = (bf16[16,32,128]{2,1,0:T(8,128)(2,1)S(1)}, bf16[16,32,128]{2,1,0:T(8,128)(2,1)S(1)}, u32[]{:S(2)}, u32[]{:S(2)}) collective-permute-start(bf16[16,32,128]{2,1,0:T(8,128)(2,1)S(1)} %all_to_all.25.xown), channel_id=1, source_target_pairs={{0,1},{1,0},{2,3},{3,2},{4,5},{5,4},{6,7},{7,6},{8,9},{9,8},{10,11... | collective-permute-start | bytes 393224 | tf_op jit(solution)/shard_map/ppermute | solution.py:396
  87.1 40.4 %copy-start.5 = (bf16[64]{0:T(256)(128)(2,1)S(1)}, bf16[64]{0:T(256)(128)(2,1)}, u32[]{:S(2)}) copy-start(bf16[64]{0:T(256)(128)(2,1)} %gain.1) | copy-start | bytes 388
  91.4 1.5 %collective-permute-start.7 = (bf16[16,32,128]{2,1,0:T(8,128)(2,1)S(1)}, bf16[16,32,128]{2,1,0:T(8,128)(2,1)S(1)}, u32[]{:S(2)}, u32[]{:S(2)}) collective-permute-start(bf16[16,32,128]{2,1,0:T(8,128)(2,1)S(1)} %get-tuple-element.23), channel_id=1, source_target_pairs={{0,1},{1,0},{2,3},{3,2},{4,5},{5,4},{6,7},{7,6},{8,9},{9,8},{10,11... | collective-permute-start | bytes 393224 | tf_op jit(solution)/shard_map/ppermute | solution.py:396

commit v3 on v2

--- a/solution.py
+++ b/solution.py
@@ -43,9 +43,16 @@
     return jnp.dot(a, b, preferred_element_type=f32)
 
 
-def project(
-    tokp, pq, pk, pv, pf, tok_hbm, wq_hbm, wk_hbm, wv_hbm, wf_hbm, wout_hbm,
-    out, tok_out, tok, wq, wk, wv, wf, wout, pairs, sems,
+def plane_rows(rows, seqs, here):
+    core = lax.rem(lax.axis_index("ep"), CORES)
+    r = iota((rows, seqs), 0)
+    source = (r // here) * (CORES * here) + core * here + lax.rem(r, here)
+    return (iota((rows, seqs), 1) == source).astype(f32).astype(bf16)
+
+
+def project_own(
+    tok_hbm, wq_hbm, wk_hbm, wv_hbm, wf_hbm, wout_hbm,
+    partial, own_out, pairs, tok, wq, wk, wv, wf, wout, sems,
 ):
     copies = [
         pltpu.make_async_copy(src, dst, sems.at[k])
@@ -62,39 +69,47 @@
     ]
     for c in copies:
         c.start()
+    rows = own_out.shape[0]
+    pick = plane_rows(rows, tok.shape[0], pairs.shape[1])
+    for c in copies:
+        c.wait()
+    own = mm(pick, tok[...]).astype(bf16)
+    own_out[...] = own
+    width = wq.shape[1]
+    for k, w in enumerate((wq, wk, wv)):
+        partial[:, k * width : (k + 1) * width] = mm(own, w[...])
+    forget = nt(own, wf[...])
+    heads = wf.shape[0]
+    pad = jnp.zeros((rows, LANES - 2 * heads), f32)
+    partial[:, 3 * width :] = jnp.concatenate([forget, forget, pad], axis=1)
+    pairs[...] = wout[...].reshape(pairs.shape)
+
+
+def project_pair(partial, own, pairs, tokp, pq, pk, pv, pf, out, tok_out):
     core = lax.rem(lax.axis_index("ep"), CORES)
-    seqs = tok.shape[0]
-    rows = seqs // CORES
-    here = out.shape[1]
-    r = iota((rows, seqs), 0)
-    source = (r // here) * (CORES * here) + core * here + lax.rem(r, here)
-    pick = (iota((rows, seqs), 1) == source).astype(f32).astype(bf16)
-    other = mm(pick, tokp[...]).astype(bf16)
-    copies[0].wait()
-    own = mm(pick, tok[...]).astype(bf16)
-    width = wq.shape[1]
-    dest = rows // here
-    for k, (w, p) in enumerate(((wq, pq), (wk, pk), (wv, pv))):
-        copies[k + 1].wait()
-        term = mm(own, w[...]) + mm(other, p[...])
-        out[:, :, k * width : (k + 1) * width] = term.reshape(dest, here, width).astype(bf16)
-    heads = wf.shape[0]
-    copies[4].wait()
-    forget = nt(own, wf[...]) + nt(other, pf[...])
-    high = forget.astype(bf16).astype(f32)
-    low = forget - high
+    dest, here, _ = out.shape
+    rows = own.shape[0]
+    other = mm(plane_rows(rows, tokp.shape[0], here), tokp[...]).astype(bf16)
+    width = pq.shape[1]
+    for k, p in enumerate((pq, pk, pv)):
+        at = slice(k * width, (k + 1) * width)
+        term = partial[:, at] + mm(other, p[...])
+        out[:, :, at] = term.reshape(dest, here, width).astype(bf16)
+    heads = pf.shape[0]
+    forget = nt(other, pf[...])
     pad = jnp.zeros((rows, LANES - 2 * heads), f32)
-    both = jnp.concatenate([high, low, pad], axis=1)
+    both = partial[:, 3 * width :] + jnp.concatenate([forget, forget, pad], axis=1)
+    high = both.astype(bf16).astype(f32)
+    both = jnp.where(iota(both.shape, 1) < heads, high, both - high)
     out[:, :, 3 * width : 3 * width + LANES] = both.reshape(dest, here, LANES).astype(bf16)
-    first = jnp.where(core == 0, own.astype(f32), other.astype(f32))
-    second = jnp.where(core == 0, other.astype(f32), own.astype(f32))
+    mine = own[...].astype(f32)
+    other = other.astype(f32)
+    first = jnp.where(core == 0, mine, other)
+    second = jnp.where(core == 0, other, mine)
     tok_out[...] = jnp.concatenate([first, second], axis=1)
-    copies[5].wait()
-    steps = pairs.shape[0]
-    pairs[...] = wout[...].reshape(pairs.shape)
     base = 3 * width + LANES
     for z in range(dest):
-        for t in range(steps):
+        for t in range(pairs.shape[0]):
             out[z, :, base + t * LANES : base + (t + 1) * LANES] = pairs[
                 t, :, z * LANES : (z + 1) * LANES
             ]
@@ -114,23 +129,6 @@
         ).astype(bf16)
 
 
-def load_cache(lengths, keys_hbm, gates_hbm, keys, bias, gates, sems):
-    copies = [
-        pltpu.make_async_copy(gates_hbm, gates, sems.at[0]),
-        pltpu.make_async_copy(keys_hbm.at[0], keys, sems.at[1]),
-    ]
-    for c in copies:
-        c.start()
-    copies[0].wait()
-    for j in range(gates.shape[0]):
-        gate = gates[j]
-        length = lengths[j]
-        position = iota(gate.shape, 1)
-        last = jnp.sum(jnp.where(position == length - 1, gate, 0.0), axis=1, keepdims=True)
-        bias[j] = jnp.where(position < length, last - gate, -jnp.inf)
-    copies[1].wait()
-
-
 def load_all(*refs):
     count = len(refs) // 2
     sems = refs[-1]
@@ -144,18 +142,21 @@
 
 
 def attention(
-    got, bias, forget_bias, first, keys_hbm, values_hbm, out, keys, values, sems
+    got, forget_bias, lengths_hbm, gates_hbm, keys_hbm, values_hbm, out,
+    lengths, gates, keys, values, sems,
 ):
     dest, here, _ = got.shape
-    heads = bias.shape[1]
-    width = first.shape[1]
-    kcopy = [
-        pltpu.make_async_copy(keys_hbm.at[j], keys.at[j - 1], sems.at[0, j]) for j in range(1, here)
+    heads, places = gates.shape[1:]
+    width = keys.shape[2]
+    small = [
+        pltpu.make_async_copy(lengths_hbm, lengths, sems.at[2, 0]),
+        pltpu.make_async_copy(gates_hbm, gates, sems.at[2, 1]),
     ]
+    kcopy = [pltpu.make_async_copy(keys_hbm.at[j], keys.at[j], sems.at[0, j]) for j in range(here)]
     vcopy = [
         pltpu.make_async_copy(values_hbm.at[j], values.at[j], sems.at[1, j]) for j in range(here)
     ]
-    for c in kcopy + vcopy:
+    for c in small + kcopy + vcopy:
         c.start()
     size = width // heads
     used = 3 * width + LANES
@@ -166,7 +167,16 @@
     lane = iota((heads, LANES), 1)
     sub = iota((heads, LANES), 0)
     scale = size**-0.5
-    added = jnp.sum(jnp.where(lane == sub, forget_bias[...], 0.0), axis=1, keepdims=True)
+    position = iota((heads, places), 1)
+    added = jnp.sum(
+        jnp.where(
+            iota((heads, heads), 1) == iota((heads, heads), 0), forget_bias[...], 0.0
+        ),
+        axis=1,
+        keepdims=True,
+    )
+    for c in small:
+        c.wait()
     soft = []
     for j in range(here):
         row = total[j : j + 1]
@@ -179,10 +189,12 @@
         x = forget + added
         log_gate = -(jnp.maximum(-x, 0.0) + jnp.log1p(jnp.exp(-jnp.abs(x))))
         own = jnp.sum(query * new_key, axis=1, keepdims=True) * scale
-        if j > 0:
-            kcopy[j - 1].wait()
-        keys_here = first[...] if j == 0 else keys[j - 1]
-        scores = nt(query.astype(bf16), keys_here) * scale + (bias[j] + log_gate)
+        gate = gates[j]
+        length = lengths[j]
+        last = jnp.sum(jnp.where(position == length - 1, gate, 0.0), axis=1, keepdims=True)
+        bias = jnp.where(position < length, (last + log_gate) - gate, -jnp.inf)
+        kcopy[j].wait()
+        scores = nt(query.astype(bf16), keys[j]) * scale + bias
         top = jnp.maximum(jnp.max(scores, axis=1, keepdims=True), own)
         weights = jnp.exp(scores - top)
         weight_own = jnp.exp(own - top)
@@ -191,8 +203,8 @@
     rows = []
     for j in range(here):
         probs, prob_own = soft[j]
+        vcopy[j].wait()
         new_value = total[j : j + 1, 2 * width : 3 * width].astype(bf16).astype(f32)
-        vcopy[j].wait()
         mixed = mm(probs, values[j]) + prob_own * new_value
         rows.append(jnp.sum(jnp.where(mine, mixed, 0.0), axis=0, keepdims=True))
     attn = jnp.concatenate(rows, axis=0).astype(bf16)
@@ -214,10 +226,10 @@
 
 
 def feed_forward(
-    xown, xpar, gain, shutter, router, routes, weg, wdg,
-    weu_hbm, wdu_hbm, wed_hbm, wdd_hbm,
+    xown, xpar, gain, shutter, router, routes, weg, wdg, weu, wdu,
+    wed_hbm, wdd_hbm,
     keep, send, rest,
-    xbuf, weu, wdu, wed, wdd, sems,
+    xbuf, wed, wdd, sems,
 ):
     rank = lax.axis_index("ep")
     ranks = lax.axis_size("ep")
@@ -225,7 +237,7 @@
     copies = [
         pltpu.make_async_copy(src, dst, sems.at[k])
         for k, (src, dst) in enumerate(
-            ((weu_hbm, weu), (wdu_hbm, wdu), (wed_hbm, wed), (wdd_hbm, wdd))
+            ((wed_hbm, wed), (wdd_hbm, wdd))
         )
     ]
     for c in copies:
@@ -272,14 +284,12 @@
     dense = 1.0 / (1.0 + jnp.exp(-shut))
     gate_e = mm(normed, weg[...])
     gate_d = mm(normed, wdg[...])
-    copies[0].wait()
     up_e = mm(normed, weu[...])
     hidden_e = (weight * (gate_e / (1.0 + jnp.exp(-gate_e))) * up_e).astype(bf16)
-    copies[1].wait()
     up_d = mm(normed, wdu[...])
     hidden_d = (dense * (gate_d / (1.0 + jnp.exp(-gate_d))) * up_d).astype(bf16)
-    copies[2].wait()
-    copies[3].wait()
+    copies[0].wait()
+    copies[1].wait()
     for z in range(chips):
         at = slice(z * lanes, (z + 1) * lanes)
         block = mm(hidden_e, wed[:, at]) + mm(hidden_d, wdd[:, at])
@@ -404,17 +414,26 @@
     wf = jnp.transpose(w_forget)
     sent = (tokens, w_query, w_key, w_value, wf)
     arrived = tuple(swap(a) for a in sent)
+    partial, own, w_pairs = call(
+        project_own,
+        (
+            sds((rows, 3 * width + LANES), f32),
+            sds((rows, feats), bf16),
+            sds((w_out.shape[0] // here, here, model), bf16),
+        ),
+        [whole(HBM)] * 6,
+        [VM(a.shape, bf16) for a in (*sent, w_out)] + [dma((6,))],
+        limit=6 << 20,
+    )(*far((*sent, w_out)))
     terms, tok = call(
-        project,
+        project_pair,
         (
             sds((chips, here, 3 * width + LANES + w_out.shape[0] // here * LANES), bf16),
             sds((rows, LANES), f32),
         ),
-        [whole()] * 5 + [whole(HBM)] * 6,
-        [VM(a.shape, bf16) for a in (*sent, w_out)]
-        + [VM((w_out.shape[0] // here, here, model), bf16), dma((6,))],
-        limit=8 << 20,
-    )(*arrived, *far((*sent, w_out)))
+        [whole()] * 8,
+        limit=6 << 20,
+    )(partial, own, w_pairs, *arrived)
     sums = exchange(terms)
     wown = call(
         unpack_columns,
@@ -422,27 +441,23 @@
         [whole()],
         limit=4 << 20,
     )(sums)
-    gates = jnp.transpose(cache_gates, (0, 2, 1))
-    far_keys, far_values, gates = far((cache_keys, cache_values, gates))
-    first, bias = call(
-        load_cache,
-        (VM(cache_keys.shape[1:], bf16), VM(gates.shape, f32)),
-        [whole(pltpu.SMEM)] + [whole(HBM)] * 2,
-        [VM(gates.shape, f32), dma((2,))],
-        limit=4 << 20,
-    )(lengths, far_keys, gates)
-    forget_row = jnp.pad(forget_bias, (0, LANES - heads))[None]
     attn = call(
         attention,
         sds((chips, here, width), bf16),
-        [whole()] * 4 + [whole(HBM)] * 2,
+        [whole()] * 2 + [whole(HBM)] * 4,
         [
-            VM((here - 1, places, width), bf16),
+            pltpu.SMEM((here,), jnp.int32),
+            VM((here, heads, places), f32),
             VM((here, places, width), bf16),
-            dma((2, here)),
+            VM((here, places, width), bf16),
+            dma((3, 2)),
         ],
         limit=14 << 20,
-    )(sums, bias, forget_row, first, far_keys, far_values)
+    )(
+        sums,
+        forget_bias[None],
+        *far((lengths, jnp.transpose(cache_gates, (0, 2, 1)), cache_keys, cache_values)),
+    )
     attn_all = exchange(attn)
     wpar = swap(wown)
     mixed = call(
@@ -464,6 +479,13 @@
         [dma((2,))],
         limit=4 << 20,
     )(*weights[:2])
+    ups = call(
+        load_all,
+        tuple(VM(w.shape, bf16) for w in weights[2:4]),
+        [whole(HBM)] * 2,
+        [dma((2,))],
+        limit=4 << 20,
+    )(*weights[2:4])
     keep, send, rest = call(
         feed_forward,
         (
@@ -471,8 +493,8 @@
             sds((chips, rows, LANES), bf16),
             sds((rows, LANES), f32),
         ),
-        [whole()] * 8 + [whole(HBM)] * 4,
-        [VM((seqs, model), bf16)] + [VM(w.shape, bf16) for w in weights[2:]] + [dma((4,))],
+        [whole()] * 10 + [whole(HBM)] * 2,
+        [VM((seqs, model), bf16)] + [VM(w.shape, bf16) for w in weights[4:]] + [dma((2,))],
         limit=18 << 20,
     )(
         xown,
@@ -482,7 +504,8 @@
         jnp.transpose(w_router),
         jnp.transpose(routes),
         *first,
-        *weights[2:],
+        *ups,
+        *weights[4:],
     )
     part = call(pair_sum, sds((chips, rows, LANES), bf16), [whole()] * 2, limit=4 << 20)(
         keep, swap(send)

time: 129 us -> 129 us (level)
  blocking collectives: 50.1 us -> 73.8 us
  waiting for transfers between devices: 25.1 us -> 11.7 us
  starting transfers between devices: 36 us -> 27.7 us
    all_to_all x2 -> x3, blocking collectives: 31.1 us -> 54.8 us  [exchange(): lax.all_to_all(a, 'ep', split_axis=0, concat_axis=0, tiled=True, axis_ind...]
    all_to_all x2 -> x1, waiting for transfers between devices: 21.7 us -> 9.35 us  [exchange(): lax.all_to_all(a, 'ep', split_axis=0, concat_axis=0, tiled=True, axis_ind...]
    all_to_all x2 -> x1, starting transfers between devices: 20.3 us -> 12 us  [exchange(): lax.all_to_all(a, 'ep', split_axis=0, concat_axis=0, tiled=True, axis_ind...]
    pallas_call x3 -> x4, Pallas kernels: 8.83 us -> 8.82 us  [the longest x1 4.84 us: shards(): call(attention, sds((chips, here, width), bf16), [whole()] * 2 + [whole(H...]
  transfers between devices with their start and end apart: 10 -> 9, of which waited for: 5 -> 3; matrix products, arithmetic and copies ran while one was open for 0% -> 0% of each run, Pallas kernels for 3% -> 4%
where the time goes in v3:
time: 129 us
  blocking collectives  73.8 us (57%)
  starting transfers between devices  27.7 us (21%)
  Pallas kernels  15.4 us (12%)
  waiting for transfers between devices  11.7 us (9%)
    all_to_all x3, blocking collectives, exchange(): lax.all_to_all(a, 'ep', split_axis=0, concat_axis=0, tiled=True, axis_ind...  54.8 us
    all_to_all x1, blocking collectives, shards(): stats = lax.all_to_all(stats, 'ep', split_axis=0, concat_axis=0, tiled=True)  19 us
    ppermute x8, starting transfers between devices, swap(): return lax.ppermute(a, 'ep', pairs)  15.7 us
    all_to_all x1, starting transfers between devices, exchange(): lax.all_to_all(a, 'ep', split_axis=0, concat_axis=0, tiled=True, axis_ind...  12 us
    all_to_all x1, waiting for transfers between devices, exchange(): lax.all_to_all(a, 'ep', split_axis=0, concat_axis=0, tiled=True, axis_ind...  9.35 us
    pallas_call x1, Pallas kernels, shards(): call(attention, sds((chips, here, width), bf16), [whole()] * 2 + [whole(H...  4.84 us
    pallas_call x1, Pallas kernels, shards(): call(feed_forward, (sds((chips, rows, LANES), f32), sds((chips, rows, LAN...  3.3 us
  transfers between devices with their start and end apart: 9, of which 3 were waited for; matrix products, arithmetic and copies ran while one was open for 0% of the time, Pallas kernels for 4%

profile of v3, /device:TPU:69, one launch (start us, length us, event | category | flops | bytes accessed | tf_op | source)
XLA Modules:
  0.0 128.8 jit_solution(16039387829530649330)
XLA Ops:
  0.0 0.0 copy-start.4
  0.0 9.9 %collective-permute-start.1 = (bf16[64,1024]{1,0:T(8,128)(2,1)}, bf16[64,1024]{1,0:T(8,128)(2,1)S(1)}, u32[]{:S(2)}, u32[]{:S(2)}) collective-permute-start(bf16[64,1024]{1,0:T(8,128)(2,1)} %wq_hbm.1), channel_id=1, source_target_pairs={{0,1},{1,0},{2,3},{3,2},{4,5},{5,4},{6,7},{7,6},{8,9},{9,8},{10,11... | collective-permute-start | bytes 393224 | tf_op jit(solution)/shard_map/ppermute | solution.py:406
  9.9 0.0 collective-permute-start.2
  9.9 0.5 collective-permute-start.3
  10.4 0.0 collective-permute-start
  10.4 0.5 collective-permute-start.4
  10.9 1.6 %shard_map.208 = (f32[32,3200]{1,0:T(8,128)S(1)}, bf16[32,64]{1,0:T(8,128)(2,1)S(1)}, bf16[16,2,2048]{2,1,0:T(2,128)(2,1)S(1)}) custom-call(bf16[64,64]{1,0:T(8,128)(2,1)} %tok_hbm.1, bf16[64,1024]{1,0:T(8,128)(2,1)} %wq_hbm.1, bf16[64,1024]{1,0:T(8,128)(2,1)} %wk_hbm.1, bf16[64,1024]{1,0:T(8,128)(2,1)} %wv_hbm.1, bf16[16,64]{1,0:T(8,128)(2,1)} %bitcast.14, ...), custom_call_target="tpu_custom_call" | custom-call | tf_op jit(solution)/shard_map/pallas_call | solution.py:417
  12.5 0.0 collective-permute-done.4.pf
  12.5 0.0 collective-permute-done.tokp
  12.5 0.0 collective-permute-done.1.pq
  12.5 0.0 collective-permute-done.2.pk
  12.5 0.0 collective-permute-done.3.pv
  12.6 0.5 shard_map.209
  13.1 23.6 %all_to_all.25.got = bf16[16,2,5248]{2,1,0:T(2,128)(2,1)S(1)} all-to-all(bf16[16,2,5248]{2,1,0:T(2,128)(2,1)S(1)} %get-tuple-element.22), channel_id=1, replica_groups={{0,2,4,6,8,10,12,14,16,18,20,22,24,26,28,30},{1,3,5,7,9,11,13,15,17,19,..., dimensions={0} | all-to-all | bytes 671744 | tf_op jit(solution)/shard_map/all_to_all | solution.py:409
  36.7 0.0 copy-done.4
  36.7 4.8 %shard_map.210 = bf16[16,2,1024]{2,1,0:T(2,128)(2,1)} custom-call(bf16[16,2,5248]{2,1,0:T(2,128)(2,1)S(1)} %all_to_all.25.got, f32[1,16]{1,0:T(1,128)S(1)} %bitcast.11, s32[2]{0:T(128)} %lengths_hbm.1, f32[2,16,1024]{2,1,0:T(8,128)} %bitcast.12, bf16[2,1024,1024]{2,1,0:T(8,128)(2,1)} %keys_hbm.1, bf16[2,1024,1024]{2,1,0:T(8,128)(2,1)} %values_hbm.1), custom_call_target="tpu_custom_call" | custom-call | tf_op jit(solution)/shard_map/pallas_call | solution.py:444
  41.5 12.0 %all-to-all-start.1 = ((bf16[16,2,1024]{2,1,0:T(2,128)(2,1)}), bf16[16,2,1024]{2,1,0:T(2,128)(2,1)S(1)}, u32[]{:S(2)}, u32[]{:S(2)}) async-start(bf16[16,2,1024]{2,1,0:T(2,128)(2,1)} %shard_map.210), calls=%async_computation.1 | async-start | bytes 131072 | tf_op jit(solution)/shard_map/all_to_all | solution.py:409
  53.5 0.1 shard_map.211.wown
  53.7 0.9 collective-permute-start.5
  54.6 1.0 collective-permute-done.5.wpar
  55.5 9.3 %all-to-all-done.1.got = bf16[16,2,1024]{2,1,0:T(2,128)(2,1)S(1)} async-done(((bf16[16,2,1024]{2,1,0:T(2,128)(2,1)}), bf16[16,2,1024]{2,1,0:T(2,128)(2,1)S(1)}, u32[]{:S(2)}, u32[]{:S(2)}) %all-to-all-start.1) | async-done | bytes 65568 | tf_op jit(solution)/shard_map/all_to_all | solution.py:409
  64.9 0.2 shard_map.212
  65.1 15.7 %all_to_all.26.xown = bf16[16,32,128]{2,1,0:T(8,128)(2,1)S(1)} all-to-all(bf16[16,32,128]{2,1,0:T(8,128)(2,1)S(1)} %shard_map.212), channel_id=1, replica_groups={{0,2,4,6,8,10,12,14,16,18,20,22,24,26,28,30},{1,3,5,7,9,11,13,15,17,19,..., dimensions={0} | all-to-all | bytes 262144 | tf_op jit(solution)/shard_map/all_to_all | solution.py:409
  80.9 3.7 %collective-permute-start.6 = (bf16[16,32,128]{2,1,0:T(8,128)(2,1)S(1)}, bf16[16,32,128]{2,1,0:T(8,128)(2,1)S(1)}, u32[]{:S(2)}, u32[]{:S(2)}) collective-permute-start(bf16[16,32,128]{2,1,0:T(8,128)(2,1)S(1)} %all_to_all.26.xown), channel_id=1, source_target_pairs={{0,1},{1,0},{2,3},{3,2},{4,5},{5,4},{6,7},{7,6},{8,9},{9,8},{10,11... | collective-permute-start | bytes 393224 | tf_op jit(solution)/shard_map/ppermute | solution.py:406
  84.6 1.9 %shard_map.213 = (bf16[2048,512]{1,0:T(8,128)(2,1)S(1)}, bf16[2048,256]{1,0:T(8,128)(2,1)S(1)}) custom-call(bf16[2048,512]{1,0:T(8,128)(2,1)} %refs_0_.2, bf16[2048,256]{1,0:T(8,128)(2,1)} %refs_1_.2), custom_call_target="tpu_custom_call" | custom-call | tf_op jit(solution)/shard_map/pallas_call | solution.py:475
  86.5 0.0 copy-start
  86.5 0.0 copy-start.1
  86.5 0.0 copy-start.2
  86.5 0.0 copy-start.3
  86.5 1.9 %shard_map.214 = (bf16[2048,512]{1,0:T(8,128)(2,1)S(1)}, bf16[2048,256]{1,0:T(8,128)(2,1)S(1)}) custom-call(bf16[2048,512]{1,0:T(8,128)(2,1)} %refs_0_.3, bf16[2048,256]{1,0:T(8,128)(2,1)} %refs_1_.3), custom_call_target="tpu_custom_call" | custom-call | tf_op jit(solution)/shard_map/pallas_call | solution.py:482
  88.4 0.0 collective-permute-done.6.xpar
  88.4 0.0 copy-done
  88.4 0.0 copy-done.1
  88.4 0.0 copy-done.2
  88.4 0.0 copy-done.3
  88.5 0.0 copy-start.5
  88.5 3.3 %shard_map.215 = (f32[16,32,128]{2,1,0:T(8,128)S(1)}, bf16[16,32,128]{2,1,0:T(8,128)(2,1)S(1)}, f32[32,128]{1,0:T(8,128)S(1)}) custom-call(bf16[16,32,128]{2,1,0:T(8,128)(2,1)S(1)} %all_to_all.26.xown, bf16[16,32,128]{2,1,0:T(8,128)(2,1)S(1)} %collective-permute-done.6.xpar, bf16[16,128]{1,0:T(8,128)(2,1)S(1)} %bitcast.8, bf16[16,128]{1,0:T(8,128)(2,1)S(1)} %bitcast.9, ...), custom_call_target="tpu_custom_call" | custom-call | tf_op jit(solution)/shard_map/pallas_call | solution.py:489
  91.8 0.1 collective-permute-start.7
  91.9 1.3 %collective-permute-done.7.got = bf16[16,32,128]{2,1,0:T(8,128)(2,1)S(1)} collective-permute-done((bf16[16,32,128]{2,1,0:T(8,128)(2,1)S(1)}, bf16[16,32,128]{2,1,0:T(8,128)(2,1)S(1)}, u32[]{:S(2)}, u32[]{:S(2)}) %collective-permute-start.7) | collective-permute-done | bytes 131104 | tf_op jit(solution)/shard_map/ppermute | solution.py:406
  93.3 15.4 %all_to_all.27.got = bf16[16,32,128]{2,1,0:T(8,128)(2,1)S(1)} all-to-all(bf16[16,32,128]{2,1,0:T(8,128)(2,1)S(1)} %shard_map.216), channel_id=1, replica_groups={{0,2,4,6,8,10,12,14,16,18,20,22,24,26,28,30},{1,3,5,7,9,11,13,15,17,19,..., dimensions={0} | all-to-all | bytes 262144 | tf_op jit(solution)/shard_map/all_to_all | solution.py:409
  108.7 0.1 shard_map.217
  108.8 19.0 %all_to_all.28.stats = f32[32,1,128]{2,1,0:T(1,128)S(1)} all-to-all(f32[32,1,128]{2,1,0:T(1,128)S(1)} %get-tuple-element.32), channel_id=1, replica_groups=mesh['grp'=4,'ep'=32] {'ep'}, dimensions={0} | all-to-all | bytes 32768 | tf_op jit(solution)/shard_map/all_to_all | solution.py:519
  127.9 0.0 copy-done.5
  127.9 0.9 shard_map.218
  (1 shorter events, 0.0 us)
Async XLA Ops:
  0.0 36.7 %copy-start.4 = (f32[16]{0:T(128)S(1)}, f32[16]{0:T(128)}, u32[]{:S(2)}) copy-start(f32[16]{0:T(128)} %param.27) | copy-start | bytes 196
  0.0 12.5 %collective-permute-start.1 = (bf16[64,1024]{1,0:T(8,128)(2,1)}, bf16[64,1024]{1,0:T(8,128)(2,1)S(1)}, u32[]{:S(2)}, u32[]{:S(2)}) collective-permute-start(bf16[64,1024]{1,0:T(8,128)(2,1)} %wq_hbm.1), channel_id=1, source_target_pairs={{0,1},{1,0},{2,3},{3,2},{4,5},{5,4},{6,7},{7,6},{8,9},{9,8},{10,11... | collective-permute-start | bytes 393224 | tf_op jit(solution)/shard_map/ppermute | solution.py:406
  9.9 2.6 %collective-permute-start.2 = (bf16[64,1024]{1,0:T(8,128)(2,1)}, bf16[64,1024]{1,0:T(8,128)(2,1)S(1)}, u32[]{:S(2)}, u32[]{:S(2)}) collective-permute-start(bf16[64,1024]{1,0:T(8,128)(2,1)} %wk_hbm.1), channel_id=1, source_target_pairs={{0,1},{1,0},{2,3},{3,2},{4,5},{5,4},{6,7},{7,6},{8,9},{9,8},{10,11... | collective-permute-start | bytes 393224 | tf_op jit(solution)/shard_map/ppermute | solution.py:406
  9.9 2.6 %collective-permute-start.3 = (bf16[64,1024]{1,0:T(8,128)(2,1)}, bf16[64,1024]{1,0:T(8,128)(2,1)S(1)}, u32[]{:S(2)}, u32[]{:S(2)}) collective-permute-start(bf16[64,1024]{1,0:T(8,128)(2,1)} %wv_hbm.1), channel_id=1, source_target_pairs={{0,1},{1,0},{2,3},{3,2},{4,5},{5,4},{6,7},{7,6},{8,9},{9,8},{10,11... | collective-permute-start | bytes 393224 | tf_op jit(solution)/shard_map/ppermute | solution.py:406
  10.4 2.1 %collective-permute-start = (bf16[64,64]{1,0:T(8,128)(2,1)}, bf16[64,64]{1,0:T(8,128)(2,1)S(1)}, u32[]{:S(2)}, u32[]{:S(2)}) collective-permute-start(bf16[64,64]{1,0:T(8,128)(2,1)} %tok_hbm.1), channel_id=1, source_target_pairs={{0,1},{1,0},{2,3},{3,2},{4,5},{5,4},{6,7},{7,6},{8,9},{9,8},{10,11... | collective-permute-start | bytes 24584 | tf_op jit(solution)/shard_map/ppermute | solution.py:406
  10.4 2.1 %collective-permute-start.4 = (bf16[16,64]{1,0:T(8,128)(2,1)}, bf16[16,64]{1,0:T(8,128)(2,1)S(1)}, u32[]{:S(2)}, u32[]{:S(2)}) collective-permute-start(bf16[16,64]{1,0:T(8,128)(2,1)} %bitcast.13), channel_id=1, source_target_pairs={{0,1},{1,0},{2,3},{3,2},{4,5},{5,4},{6,7},{7,6},{8,9},{9,8},{10,11... | collective-permute-start | bytes 6152 | tf_op jit(solution)/shard_map/ppermute | solution.py:406
  41.5 23.4 %all-to-all-start.1 = ((bf16[16,2,1024]{2,1,0:T(2,128)(2,1)}), bf16[16,2,1024]{2,1,0:T(2,128)(2,1)S(1)}, u32[]{:S(2)}, u32[]{:S(2)}) async-start(bf16[16,2,1024]{2,1,0:T(2,128)(2,1)} %shard_map.210), calls=%async_computation.1 | async-start | bytes 131072 | tf_op jit(solution)/shard_map/all_to_all | solution.py:409
  53.7 1.9 %collective-permute-start.5 = (bf16[16,32,128]{2,1,0:T(8,128)(2,1)S(1)}, bf16[16,32,128]{2,1,0:T(8,128)(2,1)S(1)}, u32[]{:S(2)}, u32[]{:S(2)}) collective-permute-start(bf16[16,32,128]{2,1,0:T(8,128)(2,1)S(1)} %shard_map.211.wown), channel_id=1, source_target_pairs={{0,1},{1,0},{2,3},{3,2},{4,5},{5,4},{6,7},{7,6},{8,9},{9,8},{10,11... | collective-permute-start | bytes 393224 | tf_op jit(solution)/shard_map/ppermute | solution.py:406
  80.9 7.6 %collective-permute-start.6 = (bf16[16,32,128]{2,1,0:T(8,128)(2,1)S(1)}, bf16[16,32,128]{2,1,0:T(8,128)(2,1)S(1)}, u32[]{:S(2)}, u32[]{:S(2)}) collective-permute-start(bf16[16,32,128]{2,1,0:T(8,128)(2,1)S(1)} %all_to_all.26.xown), channel_id=1, source_target_pairs={{0,1},{1,0},{2,3},{3,2},{4,5},{5,4},{6,7},{7,6},{8,9},{9,8},{10,11... | collective-permute-start | bytes 393224 | tf_op jit(solution)/shard_map/ppermute | solution.py:406
  86.5 2.0 %copy-start = (bf16[2048,4]{0,1:T(4,128)(2,1)S(1)}, bf16[2048,4]{0,1:T(4,128)(2,1)}, u32[]{:S(2)}) copy-start(bf16[2048,4]{0,1:T(4,128)(2,1)} %param.34) | copy-start | bytes 49156
  86.5 2.0 %copy-start.1 = (bf16[2048]{0:T(1024)(128)(2,1)S(1)}, bf16[2048]{0:T(1024)(128)(2,1)}, u32[]{:S(2)}) copy-start(bf16[2048]{0:T(1024)(128)(2,1)} %param.33) | copy-start | bytes 12292
  86.5 2.0 %copy-start.2 = (bf16[2048]{0:T(1024)(128)(2,1)S(1)}, bf16[2048]{0:T(1024)(128)(2,1)}, u32[]{:S(2)}) copy-start(bf16[2048]{0:T(1024)(128)(2,1)} %param.36) | copy-start | bytes 12292
  86.5 2.0 %copy-start.3 = (s32[64,2]{0,1:T(2,128)S(1)}, s32[64,2]{0,1:T(2,128)}, u32[]{:S(2)}) copy-start(s32[64,2]{0,1:T(2,128)} %param.35) | copy-start | bytes 1540
  88.5 39.4 %copy-start.5 = (bf16[64]{0:T(256)(128)(2,1)S(1)}, bf16[64]{0:T(256)(128)(2,1)}, u32[]{:S(2)}) copy-start(bf16[64]{0:T(256)(128)(2,1)} %gain.1) | copy-start | bytes 388
  91.8 1.5 %collective-permute-start.7 = (bf16[16,32,128]{2,1,0:T(8,128)(2,1)S(1)}, bf16[16,32,128]{2,1,0:T(8,128)(2,1)S(1)}, u32[]{:S(2)}, u32[]{:S(2)}) collective-permute-start(bf16[16,32,128]{2,1,0:T(8,128)(2,1)S(1)} %get-tuple-element.29), channel_id=1, source_target_pairs={{0,1},{1,0},{2,3},{3,2},{4,5},{5,4},{6,7},{7,6},{8,9},{9,8},{10,11... | collective-permute-start | bytes 393224 | tf_op jit(solution)/shard_map/ppermute | solution.py:406

commit v4 on v3

--- a/solution.py
+++ b/solution.py
@@ -43,6 +43,10 @@
     return jnp.dot(a, b, preferred_element_type=f32)
 
 
+def my_half():
+    return lax.rem(lax.axis_index("grp"), 2)
+
+
 def plane_rows(rows, seqs, here):
     core = lax.rem(lax.axis_index("ep"), CORES)
     r = iota((rows, seqs), 0)
@@ -54,6 +58,7 @@
     tok_hbm, wq_hbm, wk_hbm, wv_hbm, wf_hbm, wout_hbm,
     partial, own_out, pairs, tok, wq, wk, wv, wf, wout, sems,
 ):
+    share = wout.shape[0]
     copies = [
         pltpu.make_async_copy(src, dst, sems.at[k])
         for k, (src, dst) in enumerate(
@@ -63,7 +68,7 @@
                 (wk_hbm, wk),
                 (wv_hbm, wv),
                 (wf_hbm, wf),
-                (wout_hbm, wout),
+                (wout_hbm.at[pl.ds(pl.multiple_of(my_half() * share, share), share)], wout),
             )
         )
     ]
@@ -142,8 +147,8 @@
 
 
 def attention(
-    got, forget_bias, lengths_hbm, gates_hbm, keys_hbm, values_hbm, out,
-    lengths, gates, keys, values, sems,
+    got, forget_hbm, lengths_hbm, gates_hbm, keys_hbm, values_hbm, out,
+    forget_bias, lengths, gates, keys, values, sems,
 ):
     dest, here, _ = got.shape
     heads, places = gates.shape[1:]
@@ -151,6 +156,7 @@
     small = [
         pltpu.make_async_copy(lengths_hbm, lengths, sems.at[2, 0]),
         pltpu.make_async_copy(gates_hbm, gates, sems.at[2, 1]),
+        pltpu.make_async_copy(forget_hbm, forget_bias, sems.at[3, 0]),
     ]
     kcopy = [pltpu.make_async_copy(keys_hbm.at[j], keys.at[j], sems.at[0, j]) for j in range(here)]
     vcopy = [
@@ -168,15 +174,11 @@
     sub = iota((heads, LANES), 0)
     scale = size**-0.5
     position = iota((heads, places), 1)
-    added = jnp.sum(
-        jnp.where(
-            iota((heads, heads), 1) == iota((heads, heads), 0), forget_bias[...], 0.0
-        ),
-        axis=1,
-        keepdims=True,
-    )
     for c in small:
         c.wait()
+    added = jnp.zeros((heads, 1), f32)
+    for h in range(heads):
+        added = jnp.where(iota((heads, 1), 0) == h, forget_bias[h], added)
     soft = []
     for j in range(here):
         row = total[j : j + 1]
@@ -212,13 +214,16 @@
         out[z] = attn
 
 
-def out_project(got, wown, wpar, tok, out, wbuf):
+def out_project(got, own, other, own_par, other_par, tok, out, wbuf):
     core = lax.rem(lax.axis_index("ep"), CORES)
+    half = my_half()
     dest, here, width = got.shape
-    part = wown.shape[1]
+    part = own.shape[1]
     for z in range(dest):
-        wbuf[pl.ds(pl.multiple_of(z * CORES * part + core * part, part), part), :] = wown[z]
-        wbuf[pl.ds(pl.multiple_of(z * CORES * part + (1 - core) * part, part), part), :] = wpar[z]
+        for side, near, across in ((core, own, other), (1 - core, own_par, other_par)):
+            base = (z * CORES + side) * 2 * part
+            wbuf[pl.ds(pl.multiple_of(base + half * part, part), part), :] = near[z]
+            wbuf[pl.ds(pl.multiple_of(base + (1 - half) * part, part), part), :] = across[z]
     attn = got[...].astype(f32).reshape(dest * here, width).astype(bf16)
     mixed = (mm(attn, wbuf[...]) + residual_scale * tok[...]).astype(bf16)
     for z in range(dest):
@@ -398,6 +403,7 @@
     planes = [[CORES * z + c for z in range(chips)] for c in range(CORES)]
     pairs = [(i, i ^ 1) for i in range(ranks)]
     sds = jax.ShapeDtypeStruct
+    half_rows = w_out.shape[0] // 2
 
     def far(arrays):
         return tuple(pltpu.with_memory_space_constraint(a, HBM) for a in arrays)
@@ -419,16 +425,16 @@
         (
             sds((rows, 3 * width + LANES), f32),
             sds((rows, feats), bf16),
-            sds((w_out.shape[0] // here, here, model), bf16),
+            sds((half_rows // here, here, model), bf16),
         ),
         [whole(HBM)] * 6,
-        [VM(a.shape, bf16) for a in (*sent, w_out)] + [dma((6,))],
+        [VM(a.shape, bf16) for a in sent] + [VM((half_rows, model), bf16), dma((6,))],
         limit=6 << 20,
     )(*far((*sent, w_out)))
     terms, tok = call(
         project_pair,
         (
-            sds((chips, here, 3 * width + LANES + w_out.shape[0] // here * LANES), bf16),
+            sds((chips, here, 3 * width + LANES + half_rows // here * LANES), bf16),
             sds((rows, LANES), f32),
         ),
         [whole()] * 8,
@@ -437,36 +443,43 @@
     sums = exchange(terms)
     wown = call(
         unpack_columns,
-        sds((chips, w_out.shape[0], LANES), bf16),
+        sds((chips, half_rows, LANES), bf16),
         [whole()],
         limit=4 << 20,
     )(sums)
     attn = call(
         attention,
         sds((chips, here, width), bf16),
-        [whole()] * 2 + [whole(HBM)] * 4,
+        [whole()] + [whole(HBM)] * 5,
         [
+            pltpu.SMEM((heads,), f32),
             pltpu.SMEM((here,), jnp.int32),
             VM((here, heads, places), f32),
             VM((here, places, width), bf16),
             VM((here, places, width), bf16),
-            dma((3, 2)),
+            dma((4, here)),
         ],
         limit=14 << 20,
     )(
         sums,
-        forget_bias[None],
-        *far((lengths, jnp.transpose(cache_gates, (0, 2, 1)), cache_keys, cache_values)),
+        *far((forget_bias, lengths, jnp.transpose(cache_gates, (0, 2, 1)), cache_keys, cache_values)),
     )
     attn_all = exchange(attn)
+    groups = lax.axis_size("grp")
+    wother = lax.ppermute(wown, "grp", [(g, g ^ 1) for g in range(groups)])
+    wother_par = lax.ppermute(
+        wown,
+        ("grp", "ep"),
+        [(g * ranks + i, (g ^ 1) * ranks + (i ^ 1)) for g in range(groups) for i in range(ranks)],
+    )
     wpar = swap(wown)
     mixed = call(
         out_project,
         sds((chips, rows, LANES), bf16),
-        [whole()] * 4,
+        [whole()] * 6,
         [VM((width, LANES), bf16)],
         limit=4 << 20,
-    )(attn_all, wown, wpar, tok)
+    )(attn_all, wown, wother, wpar, wother_par, tok)
     xown = exchange(mixed)
     xpar = swap(xown)
     weights = far(

time: 129 us -> 128 us (level)
  waiting for transfers between devices: 11.7 us -> 10.2 us
    all_to_all x1, waiting for transfers between devices: 9.35 us -> 5.69 us  [exchange(): lax.all_to_all(a, 'ep', split_axis=0, concat_axis=0, tiled=True, axis_ind...]
    ppermute x0 -> x2, waiting for transfers between devices: none -> 3.21 us  [the longest x1 2.56 us: shards(): lax.ppermute(wown, ('grp', 'ep'), [(g * ranks + i, (g ^ 1) * ranks + (i ^...]
    ppermute x0 -> x2, starting transfers between devices: none -> 2.38 us  [the longest x1 2.13 us: shards(): lax.ppermute(wown, ('grp', 'ep'), [(g * ranks + i, (g ^ 1) * ranks + (i ^...]
    all_to_all x1, starting transfers between devices: 12 us -> 10.5 us  [exchange(): lax.all_to_all(a, 'ep', split_axis=0, concat_axis=0, tiled=True, axis_ind...]
  transfers between devices with their start and end apart: 9 -> 11, of which waited for: 3 -> 4; matrix products, arithmetic and copies ran while one was open for 0% -> 0% of each run, Pallas kernels for 4% -> 4%
where the time goes in v4:
time: 128 us
  blocking collectives  73.9 us (58%)
  starting transfers between devices  27.8 us (22%)
  Pallas kernels  15.4 us (12%)
  waiting for transfers between devices  10.2 us (8%)
    all_to_all x3, blocking collectives, exchange(): lax.all_to_all(a, 'ep', split_axis=0, concat_axis=0, tiled=True, axis_ind...  54.9 us
    all_to_all x1, blocking collectives, shards(): stats = lax.all_to_all(stats, 'ep', split_axis=0, concat_axis=0, tiled=True)  19 us
    ppermute x8, starting transfers between devices, swap(): return lax.ppermute(a, 'ep', pairs)  15 us
    all_to_all x1, starting transfers between devices, exchange(): lax.all_to_all(a, 'ep', split_axis=0, concat_axis=0, tiled=True, axis_ind...  10.5 us
    all_to_all x1, waiting for transfers between devices, exchange(): lax.all_to_all(a, 'ep', split_axis=0, concat_axis=0, tiled=True, axis_ind...  5.69 us
    pallas_call x1, Pallas kernels, shards(): call(attention, sds((chips, here, width), bf16), [whole()] + [whole(HBM)]...  4.86 us
    pallas_call x1, Pallas kernels, shards(): call(feed_forward, (sds((chips, rows, LANES), f32), sds((chips, rows, LAN...  3.3 us
  transfers between devices with their start and end apart: 11, of which 4 were waited for; matrix products, arithmetic and copies ran while one was open for 0% of the time, Pallas kernels for 4%

profile of v4, /device:TPU:69, one launch (start us, length us, event | category | flops | bytes accessed | tf_op | source)
XLA Modules:
  0.0 127.6 jit_solution(8576516954354366012)
XLA Ops:
  0.0 9.9 %collective-permute-start.1 = (bf16[64,1024]{1,0:T(8,128)(2,1)}, bf16[64,1024]{1,0:T(8,128)(2,1)S(1)}, u32[]{:S(2)}, u32[]{:S(2)}) collective-permute-start(bf16[64,1024]{1,0:T(8,128)(2,1)} %wq_hbm.1), channel_id=1, source_target_pairs={{0,1},{1,0},{2,3},{3,2},{4,5},{5,4},{6,7},{7,6},{8,9},{9,8},{10,11... | collective-permute-start | bytes 393224 | tf_op jit(solution)/shard_map/ppermute | solution.py:412
  9.9 0.0 collective-permute-start.2
  9.9 0.5 collective-permute-start.3
  10.4 0.0 collective-permute-start
  10.4 0.5 collective-permute-start.4
  10.9 1.5 %shard_map.208 = (f32[32,3200]{1,0:T(8,128)S(1)}, bf16[32,64]{1,0:T(8,128)(2,1)S(1)}, bf16[8,2,2048]{2,1,0:T(2,128)(2,1)S(1)}) custom-call(bf16[64,64]{1,0:T(8,128)(2,1)} %tok_hbm.1, bf16[64,1024]{1,0:T(8,128)(2,1)} %wq_hbm.1, bf16[64,1024]{1,0:T(8,128)(2,1)} %wk_hbm.1, bf16[64,1024]{1,0:T(8,128)(2,1)} %wv_hbm.1, bf16[16,64]{1,0:T(8,128)(2,1)} %bitcast.12, ...), custom_call_target="tpu_custom_call" | custom-call | tf_op jit(solution)/shard_map/pallas_call | solution.py:423
  12.4 0.0 collective-permute-done.4.pf
  12.4 0.0 collective-permute-done.tokp
  12.4 0.0 collective-permute-done.1.pq
  12.5 0.0 collective-permute-done.2.pk
  12.5 0.0 collective-permute-done.3.pv
  12.5 0.5 shard_map.209
  13.0 22.3 %all_to_all.25.got = bf16[16,2,4224]{2,1,0:T(2,128)(2,1)S(1)} all-to-all(bf16[16,2,4224]{2,1,0:T(2,128)(2,1)S(1)} %get-tuple-element.22), channel_id=1, replica_groups={{0,2,4,6,8,10,12,14,16,18,20,22,24,26,28,30},{1,3,5,7,9,11,13,15,17,19,..., dimensions={0} | all-to-all | bytes 540672 | tf_op jit(solution)/shard_map/all_to_all | solution.py:415
  35.3 4.9 %shard_map.210 = bf16[16,2,1024]{2,1,0:T(2,128)(2,1)} custom-call(bf16[16,2,4224]{2,1,0:T(2,128)(2,1)S(1)} %all_to_all.25.got, f32[16]{0:T(128)} %forget_hbm.1, s32[2]{0:T(128)} %lengths_hbm.1, f32[2,16,1024]{2,1,0:T(8,128)} %bitcast.10, bf16[2,1024,1024]{2,1,0:T(8,128)(2,1)} %keys_hbm.1, bf16[2,1024,1024]{2,1,0:T(8,128)(2,1)} %values_hbm.1), custom_call_target="tpu_custom_call" | custom-call | tf_op jit(solution)/shard_map/pallas_call | solution.py:450
  40.2 10.5 %all-to-all-start.1 = ((bf16[16,2,1024]{2,1,0:T(2,128)(2,1)}), bf16[16,2,1024]{2,1,0:T(2,128)(2,1)S(1)}, u32[]{:S(2)}, u32[]{:S(2)}) async-start(bf16[16,2,1024]{2,1,0:T(2,128)(2,1)} %shard_map.210), calls=%async_computation.1 | async-start | bytes 131072 | tf_op jit(solution)/shard_map/all_to_all | solution.py:415
  50.6 0.1 shard_map.211.own
  50.7 2.1 %collective-permute-start.7 = (bf16[16,16,128]{2,1,0:T(8,128)(2,1)S(1)}, bf16[16,16,128]{2,1,0:T(8,128)(2,1)S(1)}, u32[]{:S(2)}, u32[]{:S(2)}) collective-permute-start(bf16[16,16,128]{2,1,0:T(8,128)(2,1)S(1)} %shard_map.211.own), channel_id=1, source_target_pairs={{0,33},{1,32},{2,35},{3,34},{4,37},{5,36},{6,39},{7,38},{8,41},{9,... | collective-permute-start | bytes 196616 | tf_op jit(solution)/shard_map/ppermute | solution.py:470
  52.8 0.0 collective-permute-start.6
  52.8 0.3 collective-permute-start.5
  53.1 2.6 %collective-permute-done.7.other_par = bf16[16,16,128]{2,1,0:T(8,128)(2,1)S(1)} collective-permute-done((bf16[16,16,128]{2,1,0:T(8,128)(2,1)S(1)}, bf16[16,16,128]{2,1,0:T(8,128)(2,1)S(1)}, u32[]{:S(2)}, u32[]{:S(2)}) %collective-permute-start.7) | collective-permute-done | bytes 65568 | tf_op jit(solution)/shard_map/ppermute | solution.py:470
  55.6 0.0 collective-permute-done.6.own_par
  55.7 0.6 collective-permute-done.5.other
  56.3 5.7 %all-to-all-done.1.got = bf16[16,2,1024]{2,1,0:T(2,128)(2,1)S(1)} async-done(((bf16[16,2,1024]{2,1,0:T(2,128)(2,1)}), bf16[16,2,1024]{2,1,0:T(2,128)(2,1)S(1)}, u32[]{:S(2)}, u32[]{:S(2)}) %all-to-all-start.1) | async-done | bytes 65568 | tf_op jit(solution)/shard_map/all_to_all | solution.py:415
  62.0 0.3 shard_map.212
  62.3 17.4 %all_to_all.26.xown = bf16[16,32,128]{2,1,0:T(8,128)(2,1)S(1)} all-to-all(bf16[16,32,128]{2,1,0:T(8,128)(2,1)S(1)} %shard_map.212), channel_id=1, replica_groups={{0,2,4,6,8,10,12,14,16,18,20,22,24,26,28,30},{1,3,5,7,9,11,13,15,17,19,..., dimensions={0} | all-to-all | bytes 262144 | tf_op jit(solution)/shard_map/all_to_all | solution.py:415
  79.7 3.9 %collective-permute-start.8 = (bf16[16,32,128]{2,1,0:T(8,128)(2,1)S(1)}, bf16[16,32,128]{2,1,0:T(8,128)(2,1)S(1)}, u32[]{:S(2)}, u32[]{:S(2)}) collective-permute-start(bf16[16,32,128]{2,1,0:T(8,128)(2,1)S(1)} %all_to_all.26.xown), channel_id=1, source_target_pairs={{0,1},{1,0},{2,3},{3,2},{4,5},{5,4},{6,7},{7,6},{8,9},{9,8},{10,11... | collective-permute-start | bytes 393224 | tf_op jit(solution)/shard_map/ppermute | solution.py:412
  83.7 1.9 %shard_map.213 = (bf16[2048,512]{1,0:T(8,128)(2,1)S(1)}, bf16[2048,256]{1,0:T(8,128)(2,1)S(1)}) custom-call(bf16[2048,512]{1,0:T(8,128)(2,1)} %refs_0_.2, bf16[2048,256]{1,0:T(8,128)(2,1)} %refs_1_.2), custom_call_target="tpu_custom_call" | custom-call | tf_op jit(solution)/shard_map/pallas_call | solution.py:488
  85.6 0.0 copy-start
  85.6 0.0 copy-start.1
  85.6 0.0 copy-start.2
  85.6 0.0 copy-start.3
  85.6 1.9 %shard_map.214 = (bf16[2048,512]{1,0:T(8,128)(2,1)S(1)}, bf16[2048,256]{1,0:T(8,128)(2,1)S(1)}) custom-call(bf16[2048,512]{1,0:T(8,128)(2,1)} %refs_0_.3, bf16[2048,256]{1,0:T(8,128)(2,1)} %refs_1_.3), custom_call_target="tpu_custom_call" | custom-call | tf_op jit(solution)/shard_map/pallas_call | solution.py:495
  87.5 0.0 collective-permute-done.8.xpar
  87.5 0.0 copy-done
  87.5 0.0 copy-done.1
  87.5 0.0 copy-done.2
  87.5 0.0 copy-done.3
  87.6 0.0 copy-start.4
  87.6 3.3 %shard_map.215 = (f32[16,32,128]{2,1,0:T(8,128)S(1)}, bf16[16,32,128]{2,1,0:T(8,128)(2,1)S(1)}, f32[32,128]{1,0:T(8,128)S(1)}) custom-call(bf16[16,32,128]{2,1,0:T(8,128)(2,1)S(1)} %all_to_all.26.xown, bf16[16,32,128]{2,1,0:T(8,128)(2,1)S(1)} %collective-permute-done.8.xpar, bf16[16,128]{1,0:T(8,128)(2,1)S(1)} %bitcast.7, bf16[16,128]{1,0:T(8,128)(2,1)S(1)} %bitcast.8, ...), custom_call_target="tpu_custom_call" | custom-call | tf_op jit(solution)/shard_map/pallas_call | solution.py:502
  90.9 0.1 collective-permute-start.9
  91.0 1.3 %collective-permute-done.9.got = bf16[16,32,128]{2,1,0:T(8,128)(2,1)S(1)} collective-permute-done((bf16[16,32,128]{2,1,0:T(8,128)(2,1)S(1)}, bf16[16,32,128]{2,1,0:T(8,128)(2,1)S(1)}, u32[]{:S(2)}, u32[]{:S(2)}) %collective-permute-start.9) | collective-permute-done | bytes 131104 | tf_op jit(solution)/shard_map/ppermute | solution.py:412
  92.4 15.1 %all_to_all.27.got = bf16[16,32,128]{2,1,0:T(8,128)(2,1)S(1)} all-to-all(bf16[16,32,128]{2,1,0:T(8,128)(2,1)S(1)} %shard_map.216), channel_id=1, replica_groups={{0,2,4,6,8,10,12,14,16,18,20,22,24,26,28,30},{1,3,5,7,9,11,13,15,17,19,..., dimensions={0} | all-to-all | bytes 262144 | tf_op jit(solution)/shard_map/all_to_all | solution.py:415
  107.5 0.1 shard_map.217
  107.6 19.0 %all_to_all.28.stats = f32[32,1,128]{2,1,0:T(1,128)S(1)} all-to-all(f32[32,1,128]{2,1,0:T(1,128)S(1)} %get-tuple-element.32), channel_id=1, replica_groups=mesh['grp'=4,'ep'=32] {'ep'}, dimensions={0} | all-to-all | bytes 32768 | tf_op jit(solution)/shard_map/all_to_all | solution.py:532
  126.7 0.0 copy-done.4
  126.7 0.9 shard_map.218
  (1 shorter events, 0.0 us)
Async XLA Ops:
  0.0 12.5 %collective-permute-start.1 = (bf16[64,1024]{1,0:T(8,128)(2,1)}, bf16[64,1024]{1,0:T(8,128)(2,1)S(1)}, u32[]{:S(2)}, u32[]{:S(2)}) collective-permute-start(bf16[64,1024]{1,0:T(8,128)(2,1)} %wq_hbm.1), channel_id=1, source_target_pairs={{0,1},{1,0},{2,3},{3,2},{4,5},{5,4},{6,7},{7,6},{8,9},{9,8},{10,11... | collective-permute-start | bytes 393224 | tf_op jit(solution)/shard_map/ppermute | solution.py:412
  9.9 2.6 %collective-permute-start.2 = (bf16[64,1024]{1,0:T(8,128)(2,1)}, bf16[64,1024]{1,0:T(8,128)(2,1)S(1)}, u32[]{:S(2)}, u32[]{:S(2)}) collective-permute-start(bf16[64,1024]{1,0:T(8,128)(2,1)} %wk_hbm.1), channel_id=1, source_target_pairs={{0,1},{1,0},{2,3},{3,2},{4,5},{5,4},{6,7},{7,6},{8,9},{9,8},{10,11... | collective-permute-start | bytes 393224 | tf_op jit(solution)/shard_map/ppermute | solution.py:412
  9.9 2.6 %collective-permute-start.3 = (bf16[64,1024]{1,0:T(8,128)(2,1)}, bf16[64,1024]{1,0:T(8,128)(2,1)S(1)}, u32[]{:S(2)}, u32[]{:S(2)}) collective-permute-start(bf16[64,1024]{1,0:T(8,128)(2,1)} %wv_hbm.1), channel_id=1, source_target_pairs={{0,1},{1,0},{2,3},{3,2},{4,5},{5,4},{6,7},{7,6},{8,9},{9,8},{10,11... | collective-permute-start | bytes 393224 | tf_op jit(solution)/shard_map/ppermute | solution.py:412
  10.4 2.0 %collective-permute-start = (bf16[64,64]{1,0:T(8,128)(2,1)}, bf16[64,64]{1,0:T(8,128)(2,1)S(1)}, u32[]{:S(2)}, u32[]{:S(2)}) collective-permute-start(bf16[64,64]{1,0:T(8,128)(2,1)} %tok_hbm.1), channel_id=1, source_target_pairs={{0,1},{1,0},{2,3},{3,2},{4,5},{5,4},{6,7},{7,6},{8,9},{9,8},{10,11... | collective-permute-start | bytes 24584 | tf_op jit(solution)/shard_map/ppermute | solution.py:412
  10.4 2.0 %collective-permute-start.4 = (bf16[16,64]{1,0:T(8,128)(2,1)}, bf16[16,64]{1,0:T(8,128)(2,1)S(1)}, u32[]{:S(2)}, u32[]{:S(2)}) collective-permute-start(bf16[16,64]{1,0:T(8,128)(2,1)} %bitcast.11), channel_id=1, source_target_pairs={{0,1},{1,0},{2,3},{3,2},{4,5},{5,4},{6,7},{7,6},{8,9},{9,8},{10,11... | collective-permute-start | bytes 6152 | tf_op jit(solution)/shard_map/ppermute | solution.py:412
  40.2 21.8 %all-to-all-start.1 = ((bf16[16,2,1024]{2,1,0:T(2,128)(2,1)}), bf16[16,2,1024]{2,1,0:T(2,128)(2,1)S(1)}, u32[]{:S(2)}, u32[]{:S(2)}) async-start(bf16[16,2,1024]{2,1,0:T(2,128)(2,1)} %shard_map.210), calls=%async_computation.1 | async-start | bytes 131072 | tf_op jit(solution)/shard_map/all_to_all | solution.py:415
  50.7 4.9 %collective-permute-start.7 = (bf16[16,16,128]{2,1,0:T(8,128)(2,1)S(1)}, bf16[16,16,128]{2,1,0:T(8,128)(2,1)S(1)}, u32[]{:S(2)}, u32[]{:S(2)}) collective-permute-start(bf16[16,16,128]{2,1,0:T(8,128)(2,1)S(1)} %shard_map.211.own), channel_id=1, source_target_pairs={{0,33},{1,32},{2,35},{3,34},{4,37},{5,36},{6,39},{7,38},{8,41},{9,... | collective-permute-start | bytes 196616 | tf_op jit(solution)/shard_map/ppermute | solution.py:470
  52.8 2.8 %collective-permute-start.6 = (bf16[16,16,128]{2,1,0:T(8,128)(2,1)S(1)}, bf16[16,16,128]{2,1,0:T(8,128)(2,1)S(1)}, u32[]{:S(2)}, u32[]{:S(2)}) collective-permute-start(bf16[16,16,128]{2,1,0:T(8,128)(2,1)S(1)} %shard_map.211.own), channel_id=1, source_target_pairs={{0,1},{1,0},{2,3},{3,2},{4,5},{5,4},{6,7},{7,6},{8,9},{9,8},{10,11... | collective-permute-start | bytes 196616 | tf_op jit(solution)/shard_map/ppermute | solution.py:412
  52.8 3.5 %collective-permute-start.5 = (bf16[16,16,128]{2,1,0:T(8,128)(2,1)S(1)}, bf16[16,16,128]{2,1,0:T(8,128)(2,1)S(1)}, u32[]{:S(2)}, u32[]{:S(2)}) collective-permute-start(bf16[16,16,128]{2,1,0:T(8,128)(2,1)S(1)} %shard_map.211.own), channel_id=1, source_target_pairs={{0,32},{32,0},{64,96},{96,64},{1,33},{33,1},{65,97},{97,65},{2,34}... | collective-permute-start | bytes 196616 | tf_op jit(solution)/shard_map/ppermute | solution.py:469
  79.7 7.8 %collective-permute-start.8 = (bf16[16,32,128]{2,1,0:T(8,128)(2,1)S(1)}, bf16[16,32,128]{2,1,0:T(8,128)(2,1)S(1)}, u32[]{:S(2)}, u32[]{:S(2)}) collective-permute-start(bf16[16,32,128]{2,1,0:T(8,128)(2,1)S(1)} %all_to_all.26.xown), channel_id=1, source_target_pairs={{0,1},{1,0},{2,3},{3,2},{4,5},{5,4},{6,7},{7,6},{8,9},{9,8},{10,11... | collective-permute-start | bytes 393224 | tf_op jit(solution)/shard_map/ppermute | solution.py:412
  85.6 2.0 %copy-start = (bf16[2048,4]{0,1:T(4,128)(2,1)S(1)}, bf16[2048,4]{0,1:T(4,128)(2,1)}, u32[]{:S(2)}) copy-start(bf16[2048,4]{0,1:T(4,128)(2,1)} %param.34) | copy-start | bytes 49156
  85.6 2.0 %copy-start.1 = (bf16[2048]{0:T(1024)(128)(2,1)S(1)}, bf16[2048]{0:T(1024)(128)(2,1)}, u32[]{:S(2)}) copy-start(bf16[2048]{0:T(1024)(128)(2,1)} %param.33) | copy-start | bytes 12292
  85.6 2.0 %copy-start.2 = (bf16[2048]{0:T(1024)(128)(2,1)S(1)}, bf16[2048]{0:T(1024)(128)(2,1)}, u32[]{:S(2)}) copy-start(bf16[2048]{0:T(1024)(128)(2,1)} %param.36) | copy-start | bytes 12292
  85.6 2.0 %copy-start.3 = (s32[64,2]{0,1:T(2,128)S(1)}, s32[64,2]{0,1:T(2,128)}, u32[]{:S(2)}) copy-start(s32[64,2]{0,1:T(2,128)} %param.35) | copy-start | bytes 1540
  87.6 39.1 %copy-start.4 = (bf16[64]{0:T(256)(128)(2,1)S(1)}, bf16[64]{0:T(256)(128)(2,1)}, u32[]{:S(2)}) copy-start(bf16[64]{0:T(256)(128)(2,1)} %gain.1) | copy-start | bytes 388
  90.9 1.5 %collective-permute-start.9 = (bf16[16,32,128]{2,1,0:T(8,128)(2,1)S(1)}, bf16[16,32,128]{2,1,0:T(8,128)(2,1)S(1)}, u32[]{:S(2)}, u32[]{:S(2)}) collective-permute-start(bf16[16,32,128]{2,1,0:T(8,128)(2,1)S(1)} %get-tuple-element.29), channel_id=1, source_target_pairs={{0,1},{1,0},{2,3},{3,2},{4,5},{5,4},{6,7},{7,6},{8,9},{9,8},{10,11... | collective-permute-start | bytes 393224 | tf_op jit(solution)/shard_map/ppermute | solution.py:412

commit v5 on v4

--- a/solution.py
+++ b/solution.py
@@ -55,8 +55,8 @@
 
 
 def project_own(
-    tok_hbm, wq_hbm, wk_hbm, wv_hbm, wf_hbm, wout_hbm,
-    partial, own_out, pairs, tok, wq, wk, wv, wf, wout, sems,
+    tok_hbm, wq_hbm, wk_hbm, wv_hbm, wf_hbm, wout_hbm, keys_hbm,
+    partial, own_out, pairs, first, tok, wq, wk, wv, wf, wout, sems,
 ):
     share = wout.shape[0]
     copies = [
@@ -74,6 +74,8 @@
     ]
     for c in copies:
         c.start()
+    keys_copy = pltpu.make_async_copy(keys_hbm.at[0], first, sems.at[len(copies)])
+    keys_copy.start()
     rows = own_out.shape[0]
     pick = plane_rows(rows, tok.shape[0], pairs.shape[1])
     for c in copies:
@@ -88,6 +90,7 @@
     pad = jnp.zeros((rows, LANES - 2 * heads), f32)
     partial[:, 3 * width :] = jnp.concatenate([forget, forget, pad], axis=1)
     pairs[...] = wout[...].reshape(pairs.shape)
+    keys_copy.wait()
 
 
 def project_pair(partial, own, pairs, tokp, pq, pk, pv, pf, out, tok_out):
@@ -147,7 +150,7 @@
 
 
 def attention(
-    got, forget_hbm, lengths_hbm, gates_hbm, keys_hbm, values_hbm, out,
+    got, first, forget_hbm, lengths_hbm, gates_hbm, keys_hbm, values_hbm, out,
     forget_bias, lengths, gates, keys, values, sems,
 ):
     dest, here, _ = got.shape
@@ -158,7 +161,7 @@
         pltpu.make_async_copy(gates_hbm, gates, sems.at[2, 1]),
         pltpu.make_async_copy(forget_hbm, forget_bias, sems.at[3, 0]),
     ]
-    kcopy = [pltpu.make_async_copy(keys_hbm.at[j], keys.at[j], sems.at[0, j]) for j in range(here)]
+    kcopy = [pltpu.make_async_copy(keys_hbm.at[j], keys.at[j - 1], sems.at[0, j]) for j in range(1, here)]
     vcopy = [
         pltpu.make_async_copy(values_hbm.at[j], values.at[j], sems.at[1, j]) for j in range(here)
     ]
@@ -195,8 +198,10 @@
         length = lengths[j]
         last = jnp.sum(jnp.where(position == length - 1, gate, 0.0), axis=1, keepdims=True)
         bias = jnp.where(position < length, (last + log_gate) - gate, -jnp.inf)
-        kcopy[j].wait()
-        scores = nt(query.astype(bf16), keys[j]) * scale + bias
+        if j > 0:
+            kcopy[j - 1].wait()
+        keys_here = first[...] if j == 0 else keys[j - 1]
+        scores = nt(query.astype(bf16), keys_here) * scale + bias
         top = jnp.maximum(jnp.max(scores, axis=1, keepdims=True), own)
         weights = jnp.exp(scores - top)
         weight_own = jnp.exp(own - top)
@@ -420,17 +425,18 @@
     wf = jnp.transpose(w_forget)
     sent = (tokens, w_query, w_key, w_value, wf)
     arrived = tuple(swap(a) for a in sent)
-    partial, own, w_pairs = call(
+    partial, own, w_pairs, first_keys = call(
         project_own,
         (
             sds((rows, 3 * width + LANES), f32),
             sds((rows, feats), bf16),
             sds((half_rows // here, here, model), bf16),
+            VM(cache_keys.shape[1:], bf16),
         ),
-        [whole(HBM)] * 6,
-        [VM(a.shape, bf16) for a in sent] + [VM((half_rows, model), bf16), dma((6,))],
+        [whole(HBM)] * 7,
+        [VM(a.shape, bf16) for a in sent] + [VM((half_rows, model), bf16), dma((7,))],
         limit=6 << 20,
-    )(*far((*sent, w_out)))
+    )(*far((*sent, w_out, cache_keys)))
     terms, tok = call(
         project_pair,
         (
@@ -450,18 +456,19 @@
     attn = call(
         attention,
         sds((chips, here, width), bf16),
-        [whole()] + [whole(HBM)] * 5,
+        [whole()] * 2 + [whole(HBM)] * 5,
         [
             pltpu.SMEM((heads,), f32),
             pltpu.SMEM((here,), jnp.int32),
             VM((here, heads, places), f32),
-            VM((here, places, width), bf16),
+            VM((here - 1, places, width), bf16),
             VM((here, places, width), bf16),
             dma((4, here)),
         ],
         limit=14 << 20,
     )(
         sums,
+        first_keys,
         *far((forget_bias, lengths, jnp.transpose(cache_gates, (0, 2, 1)), cache_keys, cache_values)),
     )
     attn_all = exchange(attn)

time: 128 us -> 128 us (level)
  transfers between devices with their start and end apart: 11 -> 11, of which waited for: 4 -> 4; matrix products, arithmetic and copies ran while one was open for 0% -> 0% of each run, Pallas kernels for 4% -> 5%
where the time goes in v5:
time: 128 us; the launch traced here: 127 us
  blocking collectives  73.9 us (58%)
  starting transfers between devices  27.8 us (22%)
  Pallas kernels  15 us (12%)
  waiting for transfers between devices  10.2 us (8%)
    all_to_all x3, blocking collectives, exchange(): lax.all_to_all(a, 'ep', split_axis=0, concat_axis=0, tiled=True, axis_ind...  54.9 us
    all_to_all x1, blocking collectives, shards(): stats = lax.all_to_all(stats, 'ep', split_axis=0, concat_axis=0, tiled=True)  19 us
    ppermute x8, starting transfers between devices, swap(): return lax.ppermute(a, 'ep', pairs)  15 us
    all_to_all x1, starting transfers between devices, exchange(): lax.all_to_all(a, 'ep', split_axis=0, concat_axis=0, tiled=True, axis_ind...  10.5 us
    all_to_all x1, waiting for transfers between devices, exchange(): lax.all_to_all(a, 'ep', split_axis=0, concat_axis=0, tiled=True, axis_ind...  5.69 us
    pallas_call x1, Pallas kernels, shards(): call(attention, sds((chips, here, width), bf16), [whole()] * 2 + [whole(H...  4.1 us
    pallas_call x1, Pallas kernels, shards(): call(feed_forward, (sds((chips, rows, LANES), f32), sds((chips, rows, LAN...  3.29 us
  transfers between devices with their start and end apart: 11, of which 4 were waited for; matrix products, arithmetic and copies ran while one was open for 0% of the time, Pallas kernels for 5%

profile of v5, /device:TPU:69, one launch (start us, length us, event | category | flops | bytes accessed | tf_op | source)
XLA Modules:
  0.0 127.3 jit_solution(13904813549216192936)
XLA Ops:
  0.0 9.9 %collective-permute-start.1 = (bf16[64,1024]{1,0:T(8,128)(2,1)}, bf16[64,1024]{1,0:T(8,128)(2,1)S(1)}, u32[]{:S(2)}, u32[]{:S(2)}) collective-permute-start(bf16[64,1024]{1,0:T(8,128)(2,1)} %wq_hbm.1), channel_id=1, source_target_pairs={{0,1},{1,0},{2,3},{3,2},{4,5},{5,4},{6,7},{7,6},{8,9},{9,8},{10,11... | collective-permute-start | bytes 393224 | tf_op jit(solution)/shard_map/ppermute | solution.py:417
  9.9 0.0 collective-permute-start.2
  9.9 0.5 collective-permute-start.3
  10.4 0.0 collective-permute-start
  10.4 0.5 collective-permute-start.4
  10.9 1.9 %shard_map.208 = (f32[32,3200]{1,0:T(8,128)S(1)}, bf16[32,64]{1,0:T(8,128)(2,1)S(1)}, bf16[8,2,2048]{2,1,0:T(2,128)(2,1)S(1)}, bf16[1024,1024]{1,0:T(8,128)(2,1)S(1)}) custom-call(bf16[64,64]{1,0:T(8,128)(2,1)} %tok_hbm.1, bf16[64,1024]{1,0:T(8,128)(2,1)} %wq_hbm.1, bf16[64,1024]{1,0:T(8,128)(2,1)} %wk_hbm.1, bf16[64,1024]{1,0:T(8,128)(2,1)} %wv_hbm.1, ...), custom_call_target="tpu_custom_call" | custom-call | tf_op jit(solution)/shard_map/pallas_call | solution.py:428
  12.9 0.0 collective-permute-done.4.pf
  12.9 0.0 collective-permute-done.tokp
  12.9 0.0 collective-permute-done.1.pq
  12.9 0.0 collective-permute-done.2.pk
  12.9 0.0 collective-permute-done.3.pv
  12.9 0.5 shard_map.209
  13.4 22.3 %all_to_all.25.got = bf16[16,2,4224]{2,1,0:T(2,128)(2,1)S(1)} all-to-all(bf16[16,2,4224]{2,1,0:T(2,128)(2,1)S(1)} %get-tuple-element.23), channel_id=1, replica_groups={{0,2,4,6,8,10,12,14,16,18,20,22,24,26,28,30},{1,3,5,7,9,11,13,15,17,19,..., dimensions={0} | all-to-all | bytes 540672 | tf_op jit(solution)/shard_map/all_to_all | solution.py:420
  35.7 4.1 %shard_map.210 = bf16[16,2,1024]{2,1,0:T(2,128)(2,1)} custom-call(bf16[16,2,4224]{2,1,0:T(2,128)(2,1)S(1)} %all_to_all.25.got, bf16[1024,1024]{1,0:T(8,128)(2,1)S(1)} %get-tuple-element.24.first, f32[16]{0:T(128)} %forget_hbm.1, s32[2]{0:T(128)} %lengths_hbm.1, f32[2,16,1024]{2,1,0:T(8,128)} %bitcast.10, bf16[2,1024,1024]{2,1,0:T(8,128)(2,1)} %keys_hbm.3, ...), custom_call_target="tpu_custom_call" | custom-call | tf_op jit(solution)/shard_map/pallas_call | solution.py:456
  39.8 10.5 %all-to-all-start.1 = ((bf16[16,2,1024]{2,1,0:T(2,128)(2,1)}), bf16[16,2,1024]{2,1,0:T(2,128)(2,1)S(1)}, u32[]{:S(2)}, u32[]{:S(2)}) async-start(bf16[16,2,1024]{2,1,0:T(2,128)(2,1)} %shard_map.210), calls=%async_computation.1 | async-start | bytes 131072 | tf_op jit(solution)/shard_map/all_to_all | solution.py:420
  50.3 0.1 shard_map.211.own
  50.4 2.1 %collective-permute-start.7 = (bf16[16,16,128]{2,1,0:T(8,128)(2,1)S(1)}, bf16[16,16,128]{2,1,0:T(8,128)(2,1)S(1)}, u32[]{:S(2)}, u32[]{:S(2)}) collective-permute-start(bf16[16,16,128]{2,1,0:T(8,128)(2,1)S(1)} %shard_map.211.own), channel_id=1, source_target_pairs={{0,33},{1,32},{2,35},{3,34},{4,37},{5,36},{6,39},{7,38},{8,41},{9,... | collective-permute-start | bytes 196616 | tf_op jit(solution)/shard_map/ppermute | solution.py:477
  52.5 0.0 collective-permute-start.6
  52.5 0.3 collective-permute-start.5
  52.8 2.6 %collective-permute-done.7.other_par = bf16[16,16,128]{2,1,0:T(8,128)(2,1)S(1)} collective-permute-done((bf16[16,16,128]{2,1,0:T(8,128)(2,1)S(1)}, bf16[16,16,128]{2,1,0:T(8,128)(2,1)S(1)}, u32[]{:S(2)}, u32[]{:S(2)}) %collective-permute-start.7) | collective-permute-done | bytes 65568 | tf_op jit(solution)/shard_map/ppermute | solution.py:477
  55.3 0.0 collective-permute-done.6.own_par
  55.3 0.6 collective-permute-done.5.other
  56.0 5.7 %all-to-all-done.1.got = bf16[16,2,1024]{2,1,0:T(2,128)(2,1)S(1)} async-done(((bf16[16,2,1024]{2,1,0:T(2,128)(2,1)}), bf16[16,2,1024]{2,1,0:T(2,128)(2,1)S(1)}, u32[]{:S(2)}, u32[]{:S(2)}) %all-to-all-start.1) | async-done | bytes 65568 | tf_op jit(solution)/shard_map/all_to_all | solution.py:420
  61.7 0.3 shard_map.212
  62.0 17.4 %all_to_all.26.xown = bf16[16,32,128]{2,1,0:T(8,128)(2,1)S(1)} all-to-all(bf16[16,32,128]{2,1,0:T(8,128)(2,1)S(1)} %shard_map.212), channel_id=1, replica_groups={{0,2,4,6,8,10,12,14,16,18,20,22,24,26,28,30},{1,3,5,7,9,11,13,15,17,19,..., dimensions={0} | all-to-all | bytes 262144 | tf_op jit(solution)/shard_map/all_to_all | solution.py:420
  79.4 3.9 %collective-permute-start.8 = (bf16[16,32,128]{2,1,0:T(8,128)(2,1)S(1)}, bf16[16,32,128]{2,1,0:T(8,128)(2,1)S(1)}, u32[]{:S(2)}, u32[]{:S(2)}) collective-permute-start(bf16[16,32,128]{2,1,0:T(8,128)(2,1)S(1)} %all_to_all.26.xown), channel_id=1, source_target_pairs={{0,1},{1,0},{2,3},{3,2},{4,5},{5,4},{6,7},{7,6},{8,9},{9,8},{10,11... | collective-permute-start | bytes 393224 | tf_op jit(solution)/shard_map/ppermute | solution.py:417
  83.4 1.9 %shard_map.213 = (bf16[2048,512]{1,0:T(8,128)(2,1)S(1)}, bf16[2048,256]{1,0:T(8,128)(2,1)S(1)}) custom-call(bf16[2048,512]{1,0:T(8,128)(2,1)} %refs_0_.2, bf16[2048,256]{1,0:T(8,128)(2,1)} %refs_1_.2), custom_call_target="tpu_custom_call" | custom-call | tf_op jit(solution)/shard_map/pallas_call | solution.py:495
  85.2 0.0 copy-start
  85.2 0.0 copy-start.1
  85.3 0.0 copy-start.2
  85.3 0.0 copy-start.3
  85.3 1.9 %shard_map.214 = (bf16[2048,512]{1,0:T(8,128)(2,1)S(1)}, bf16[2048,256]{1,0:T(8,128)(2,1)S(1)}) custom-call(bf16[2048,512]{1,0:T(8,128)(2,1)} %refs_0_.3, bf16[2048,256]{1,0:T(8,128)(2,1)} %refs_1_.3), custom_call_target="tpu_custom_call" | custom-call | tf_op jit(solution)/shard_map/pallas_call | solution.py:502
  87.2 0.0 collective-permute-done.8.xpar
  87.2 0.0 copy-done
  87.2 0.0 copy-done.1
  87.2 0.0 copy-done.2
  87.2 0.0 copy-done.3
  87.2 0.0 copy-start.4
  87.2 3.3 %shard_map.215 = (f32[16,32,128]{2,1,0:T(8,128)S(1)}, bf16[16,32,128]{2,1,0:T(8,128)(2,1)S(1)}, f32[32,128]{1,0:T(8,128)S(1)}) custom-call(bf16[16,32,128]{2,1,0:T(8,128)(2,1)S(1)} %all_to_all.26.xown, bf16[16,32,128]{2,1,0:T(8,128)(2,1)S(1)} %collective-permute-done.8.xpar, bf16[16,128]{1,0:T(8,128)(2,1)S(1)} %bitcast.7, bf16[16,128]{1,0:T(8,128)(2,1)S(1)} %bitcast.8, ...), custom_call_target="tpu_custom_call" | custom-call | tf_op jit(solution)/shard_map/pallas_call | solution.py:509
  90.5 0.1 collective-permute-start.9
  90.7 1.3 %collective-permute-done.9.got = bf16[16,32,128]{2,1,0:T(8,128)(2,1)S(1)} collective-permute-done((bf16[16,32,128]{2,1,0:T(8,128)(2,1)S(1)}, bf16[16,32,128]{2,1,0:T(8,128)(2,1)S(1)}, u32[]{:S(2)}, u32[]{:S(2)}) %collective-permute-start.9) | collective-permute-done | bytes 131104 | tf_op jit(solution)/shard_map/ppermute | solution.py:417
  92.0 15.1 %all_to_all.27.got = bf16[16,32,128]{2,1,0:T(8,128)(2,1)S(1)} all-to-all(bf16[16,32,128]{2,1,0:T(8,128)(2,1)S(1)} %shard_map.216), channel_id=1, replica_groups={{0,2,4,6,8,10,12,14,16,18,20,22,24,26,28,30},{1,3,5,7,9,11,13,15,17,19,..., dimensions={0} | all-to-all | bytes 262144 | tf_op jit(solution)/shard_map/all_to_all | solution.py:420
  107.2 0.1 shard_map.217
  107.3 19.0 %all_to_all.28.stats = f32[32,1,128]{2,1,0:T(1,128)S(1)} all-to-all(f32[32,1,128]{2,1,0:T(1,128)S(1)} %get-tuple-element.34), channel_id=1, replica_groups=mesh['grp'=4,'ep'=32] {'ep'}, dimensions={0} | all-to-all | bytes 32768 | tf_op jit(solution)/shard_map/all_to_all | solution.py:539
  126.4 0.0 copy-done.4
  126.4 0.9 shard_map.218
  (1 shorter events, 0.0 us)
Async XLA Ops:
  0.0 12.9 %collective-permute-start.1 = (bf16[64,1024]{1,0:T(8,128)(2,1)}, bf16[64,1024]{1,0:T(8,128)(2,1)S(1)}, u32[]{:S(2)}, u32[]{:S(2)}) collective-permute-start(bf16[64,1024]{1,0:T(8,128)(2,1)} %wq_hbm.1), channel_id=1, source_target_pairs={{0,1},{1,0},{2,3},{3,2},{4,5},{5,4},{6,7},{7,6},{8,9},{9,8},{10,11... | collective-permute-start | bytes 393224 | tf_op jit(solution)/shard_map/ppermute | solution.py:417
  9.9 3.0 %collective-permute-start.2 = (bf16[64,1024]{1,0:T(8,128)(2,1)}, bf16[64,1024]{1,0:T(8,128)(2,1)S(1)}, u32[]{:S(2)}, u32[]{:S(2)}) collective-permute-start(bf16[64,1024]{1,0:T(8,128)(2,1)} %wk_hbm.1), channel_id=1, source_target_pairs={{0,1},{1,0},{2,3},{3,2},{4,5},{5,4},{6,7},{7,6},{8,9},{9,8},{10,11... | collective-permute-start | bytes 393224 | tf_op jit(solution)/shard_map/ppermute | solution.py:417
  9.9 3.0 %collective-permute-start.3 = (bf16[64,1024]{1,0:T(8,128)(2,1)}, bf16[64,1024]{1,0:T(8,128)(2,1)S(1)}, u32[]{:S(2)}, u32[]{:S(2)}) collective-permute-start(bf16[64,1024]{1,0:T(8,128)(2,1)} %wv_hbm.1), channel_id=1, source_target_pairs={{0,1},{1,0},{2,3},{3,2},{4,5},{5,4},{6,7},{7,6},{8,9},{9,8},{10,11... | collective-permute-start | bytes 393224 | tf_op jit(solution)/shard_map/ppermute | solution.py:417
  10.4 2.5 %collective-permute-start = (bf16[64,64]{1,0:T(8,128)(2,1)}, bf16[64,64]{1,0:T(8,128)(2,1)S(1)}, u32[]{:S(2)}, u32[]{:S(2)}) collective-permute-start(bf16[64,64]{1,0:T(8,128)(2,1)} %tok_hbm.1), channel_id=1, source_target_pairs={{0,1},{1,0},{2,3},{3,2},{4,5},{5,4},{6,7},{7,6},{8,9},{9,8},{10,11... | collective-permute-start | bytes 24584 | tf_op jit(solution)/shard_map/ppermute | solution.py:417
  10.4 2.5 %collective-permute-start.4 = (bf16[16,64]{1,0:T(8,128)(2,1)}, bf16[16,64]{1,0:T(8,128)(2,1)S(1)}, u32[]{:S(2)}, u32[]{:S(2)}) collective-permute-start(bf16[16,64]{1,0:T(8,128)(2,1)} %bitcast.11), channel_id=1, source_target_pairs={{0,1},{1,0},{2,3},{3,2},{4,5},{5,4},{6,7},{7,6},{8,9},{9,8},{10,11... | collective-permute-start | bytes 6152 | tf_op jit(solution)/shard_map/ppermute | solution.py:417
  39.8 21.8 %all-to-all-start.1 = ((bf16[16,2,1024]{2,1,0:T(2,128)(2,1)}), bf16[16,2,1024]{2,1,0:T(2,128)(2,1)S(1)}, u32[]{:S(2)}, u32[]{:S(2)}) async-start(bf16[16,2,1024]{2,1,0:T(2,128)(2,1)} %shard_map.210), calls=%async_computation.1 | async-start | bytes 131072 | tf_op jit(solution)/shard_map/all_to_all | solution.py:420
  50.4 4.9 %collective-permute-start.7 = (bf16[16,16,128]{2,1,0:T(8,128)(2,1)S(1)}, bf16[16,16,128]{2,1,0:T(8,128)(2,1)S(1)}, u32[]{:S(2)}, u32[]{:S(2)}) collective-permute-start(bf16[16,16,128]{2,1,0:T(8,128)(2,1)S(1)} %shard_map.211.own), channel_id=1, source_target_pairs={{0,33},{1,32},{2,35},{3,34},{4,37},{5,36},{6,39},{7,38},{8,41},{9,... | collective-permute-start | bytes 196616 | tf_op jit(solution)/shard_map/ppermute | solution.py:477
  52.5 2.8 %collective-permute-start.6 = (bf16[16,16,128]{2,1,0:T(8,128)(2,1)S(1)}, bf16[16,16,128]{2,1,0:T(8,128)(2,1)S(1)}, u32[]{:S(2)}, u32[]{:S(2)}) collective-permute-start(bf16[16,16,128]{2,1,0:T(8,128)(2,1)S(1)} %shard_map.211.own), channel_id=1, source_target_pairs={{0,1},{1,0},{2,3},{3,2},{4,5},{5,4},{6,7},{7,6},{8,9},{9,8},{10,11... | collective-permute-start | bytes 196616 | tf_op jit(solution)/shard_map/ppermute | solution.py:417
  52.5 3.5 %collective-permute-start.5 = (bf16[16,16,128]{2,1,0:T(8,128)(2,1)S(1)}, bf16[16,16,128]{2,1,0:T(8,128)(2,1)S(1)}, u32[]{:S(2)}, u32[]{:S(2)}) collective-permute-start(bf16[16,16,128]{2,1,0:T(8,128)(2,1)S(1)} %shard_map.211.own), channel_id=1, source_target_pairs={{0,32},{32,0},{64,96},{96,64},{1,33},{33,1},{65,97},{97,65},{2,34}... | collective-permute-start | bytes 196616 | tf_op jit(solution)/shard_map/ppermute | solution.py:476
  79.4 7.8 %collective-permute-start.8 = (bf16[16,32,128]{2,1,0:T(8,128)(2,1)S(1)}, bf16[16,32,128]{2,1,0:T(8,128)(2,1)S(1)}, u32[]{:S(2)}, u32[]{:S(2)}) collective-permute-start(bf16[16,32,128]{2,1,0:T(8,128)(2,1)S(1)} %all_to_all.26.xown), channel_id=1, source_target_pairs={{0,1},{1,0},{2,3},{3,2},{4,5},{5,4},{6,7},{7,6},{8,9},{9,8},{10,11... | collective-permute-start | bytes 393224 | tf_op jit(solution)/shard_map/ppermute | solution.py:417
  85.2 2.0 %copy-start = (bf16[2048,4]{0,1:T(4,128)(2,1)S(1)}, bf16[2048,4]{0,1:T(4,128)(2,1)}, u32[]{:S(2)}) copy-start(bf16[2048,4]{0,1:T(4,128)(2,1)} %param.34) | copy-start | bytes 49156
  85.2 2.0 %copy-start.1 = (bf16[2048]{0:T(1024)(128)(2,1)S(1)}, bf16[2048]{0:T(1024)(128)(2,1)}, u32[]{:S(2)}) copy-start(bf16[2048]{0:T(1024)(128)(2,1)} %param.33) | copy-start | bytes 12292
  85.3 2.0 %copy-start.2 = (bf16[2048]{0:T(1024)(128)(2,1)S(1)}, bf16[2048]{0:T(1024)(128)(2,1)}, u32[]{:S(2)}) copy-start(bf16[2048]{0:T(1024)(128)(2,1)} %param.36) | copy-start | bytes 12292
  85.3 2.0 %copy-start.3 = (s32[64,2]{0,1:T(2,128)S(1)}, s32[64,2]{0,1:T(2,128)}, u32[]{:S(2)}) copy-start(s32[64,2]{0,1:T(2,128)} %param.35) | copy-start | bytes 1540
  87.2 39.1 %copy-start.4 = (bf16[64]{0:T(256)(128)(2,1)S(1)}, bf16[64]{0:T(256)(128)(2,1)}, u32[]{:S(2)}) copy-start(bf16[64]{0:T(256)(128)(2,1)} %gain.1) | copy-start | bytes 388
  90.5 1.5 %collective-permute-start.9 = (bf16[16,32,128]{2,1,0:T(8,128)(2,1)S(1)}, bf16[16,32,128]{2,1,0:T(8,128)(2,1)S(1)}, u32[]{:S(2)}, u32[]{:S(2)}) collective-permute-start(bf16[16,32,128]{2,1,0:T(8,128)(2,1)S(1)} %get-tuple-element.31), channel_id=1, source_target_pairs={{0,1},{1,0},{2,3},{3,2},{4,5},{5,4},{6,7},{7,6},{8,9},{9,8},{10,11... | collective-permute-start | bytes 393224 | tf_op jit(solution)/shard_map/ppermute | solution.py:417
